TPU v7x, 512 devices: a whole 4x8x8 slice. The times are simulated.
512 devices in a mesh: ep: 32 (over z, x), tp: 16 (over y, core).
Axes of the slice: x: 4, y: 8, z: 8, core: 2. Of those that a mesh axis runs over, the one named last changes fastest.
Arguments:
- queries: bfloat16 [4096, 512], P('ep'), may hold values from -6 to 6
- key_vectors: bfloat16 [4096, 512], P('ep'), may hold values from -6 to 6
- values: bfloat16 [4096, 1024], P('ep', 'tp'), may hold values from -6 to 6
- out_gate: bfloat16 [4096, 1024], P('ep', 'tp'), may hold values from -6 to 6
- input_gate: float32 [4096, 2], P('ep'), may hold values from -8 to 130
- forget_gate: float32 [4096, 2], P('ep'), may hold values from -2 to 16
- mix_weight: bfloat16 [1024, 2048], P('tp'), may hold values from -0.1875 to 0.1875
- expert_input: bfloat16 [8192, 2048], P('ep'), may hold values from -6 to 6
- norm_gain: float32 [2048], replicated, may hold values from 0.1 to 1.9
- route_ids: int32 [8192, 4], P('ep'), may hold values from 0 to 63, all different within a row; in each aligned block of 256 rows (0 to 255, 256 to 511, ...) at most 32 rows name the same one
- route_weights: float32 [8192, 4], P('ep'), may hold values from 0.2 to 1.2
- expert_gate: bfloat16 [512, 2048, 128], P(('ep', 'tp')), may hold values from -0.125 to 0.125
- expert_up: bfloat16 [512, 2048, 128], P(('ep', 'tp')), may hold values from -0.125 to 0.125
- expert_down: bfloat16 [512, 128, 2048], P(('ep', 'tp')), may hold values from -0.1875 to 0.1875
- shared_gate: bfloat16 [2048, 512], P(None, 'tp'), may hold values from -0.125 to 0.125
- shared_up: bfloat16 [2048, 512], P(None, 'tp'), may hold values from -0.125 to 0.125
- shared_down: bfloat16 [512, 2048], P('tp'), may hold values from -0.25 to 0.25
Outputs:
- mixer_out: bfloat16 [4096, 2048], P('ep')
- expert_out: bfloat16 [8192, 2048], P('ep')
Inputs may be any that keep to these rules, and one draw needn't show every extreme that they name: `route_ids`: each row names 4 different experts. In each aligned block of 256 rows (the rows of one index of ep) no expert is named by more than 32 rows, and in some block one expert is named by exactly 32 rows.
All inputs are finite; a program needn't handle non-finite values.
Results may differ from a plain program's by a relative error of at most 0.01575.
Values may be sent and summed in bfloat16 or wider, within the bound.
No kernel may reach another device: no remote copies, remote signals or barrier semaphores. Data moves between devices by JAX's collectives and lax.ppermute only.
A program may use at most 64 MiB of HBM per device.

v0:
```python
import jax
import jax.numpy as jnp
from jax import lax
from jax.sharding import Mesh
from jax.sharding import PartitionSpec as P

D = 2048
MEMORY_HEADS = 2
KEY_DIM = 256
BLOCK = 128
FF = 1024
EP = ("ep_0", "ep_1")
EP_TP = ("ep_0", "ep_1", "tp")


epsilon = 1e-06
lowest = -1e30
den_floor = 4.0


def nothing_yet(array, identity):
    return jax.tree.map(
        lambda part, zero: jnp.zeros_like(part) + jnp.asarray(zero, part.dtype), array, identity
    )


def all_in_one(array, axis):
    leaves = jax.tree.leaves(array)
    order = sorted(range(len(leaves)), key=lambda k: -leaves[k].size)
    width = (1, *leaves[order[0]].shape)[-1]
    lines = [
        jnp.pad(leaves[k].reshape(-1), (0, -leaves[k].size % width)).reshape(-1, width)
        for k in order
    ]
    both, at, found = (lax.all_gather(jnp.concatenate(lines), axis), 0, {})
    for k, line in zip(order, lines):
        section = both[:, at : at + len(line)].reshape(len(both), -1)
        found[k] = section[:, : leaves[k].size].reshape(-1, *leaves[k].shape)
        at += len(line)
    numbers = iter(range(len(leaves)))
    return jax.tree.map(lambda _: found[next(numbers)], array)


def entering_2(array, axes, combine, identity):
    before = start = nothing_yet(array, identity)
    subtotal = array
    for axis in reversed(axes):
        count, place = (lax.axis_size(axis), lax.axis_index(axis))
        pieces = all_in_one(subtotal, axis)
        inside, subtotal = (start, start)
        for k in range(count):
            passed = k < place
            subtotal = combine(subtotal, jax.tree.map(lambda part: part[k], pieces))
            inside = jax.tree.map(lambda new, old: jnp.where(passed, new, old), subtotal, inside)
        before = combine(inside, before)
    return before


def in_blocks(array, dim, count):
    before, after = (array.shape[:dim], array.shape[dim + 1 :])
    return jnp.moveaxis(array.reshape(*before, count, -1, *after), dim, 0)


def summed_on_arrival(array, axis, dim):
    blocks = in_blocks(array, dim, lax.axis_size(axis))
    arrived = lax.all_to_all(blocks, axis, split_axis=0, concat_axis=0, tiled=True)
    return arrived.astype(jnp.float32).sum(axis=0)


def from_everyone(array, axis):
    copies = jnp.broadcast_to(array, (lax.axis_size(axis), *array.shape))
    return lax.all_to_all(copies, axis, split_axis=0, concat_axis=0, tiled=True)


def in_order(blocks, dim):
    blocks = jnp.moveaxis(blocks, 0, dim)
    shape = blocks.shape
    return blocks.reshape(*shape[:dim], shape[dim] * shape[dim + 1], *shape[dim + 2 :])


def collect(array, axis, dim):
    blocks = from_everyone(array, axis)
    return in_order(blocks, dim)


def combine_segments(earlier, later):
    first_decay, first_memory, first_normalizer, first_running = earlier
    second_decay, second_memory, second_normalizer, second_running = later
    running = jnp.maximum(second_decay + first_running, second_running)
    lead_scale = jnp.exp(second_decay + first_running - running)
    tail_scale = jnp.exp(second_running - running)
    return (
        first_decay + second_decay,
        lead_scale * first_memory + tail_scale * second_memory,
        lead_scale * first_normalizer + tail_scale * second_normalizer,
        running,
    )


def mixer_half(queries, key_vectors, values, out_gate, input_gate, forget_gate, mix_weight):
    tp_count = lax.axis_size("tp")
    tp_rank = lax.axis_index("tp")
    length = queries.shape[0]
    blocks = length // BLOCK
    channels = values.shape[1]
    factor = KEY_DIM ** (-0.5)
    head_index = tp_rank // (tp_count // MEMORY_HEADS)
    offset = head_index * KEY_DIM
    query_head = lax.dynamic_slice_in_dim(queries, offset, KEY_DIM, 1).reshape(
        blocks, BLOCK, KEY_DIM
    )
    key_head = lax.dynamic_slice_in_dim(key_vectors, offset, KEY_DIM, 1).reshape(
        blocks, BLOCK, KEY_DIM
    )
    value_blocks = values.reshape(blocks, BLOCK, channels)
    select = jnp.arange(MEMORY_HEADS, dtype=jnp.int32)[None, :] == head_index
    input_head = jnp.sum(jnp.where(select, input_gate, 0.0), axis=1).reshape(blocks, BLOCK)
    forget_head = jax.nn.log_sigmoid(jnp.sum(jnp.where(select, forget_gate, 0.0), axis=1)).reshape(
        blocks, BLOCK
    )
    cumulative = jnp.cumsum(forget_head, axis=1)
    block_total = cumulative[:, -1]
    log_retention = block_total[:, None] - cumulative + input_head
    block_running = jnp.max(log_retention, axis=1)
    weighted_keys = (
        key_head.astype(jnp.float32) * jnp.exp(log_retention - block_running[:, None])[:, :, None]
    )
    block_memory = jnp.einsum(
        "bsd,bsv->bdv",
        weighted_keys,
        value_blocks.astype(jnp.float32),
        precision=lax.Precision.HIGHEST,
    )
    block_normalizer = jnp.sum(weighted_keys, axis=1)
    segments = (block_total, block_memory, block_normalizer, block_running)
    neutral = (
        jnp.zeros((), jnp.float32),
        jnp.zeros((KEY_DIM, channels), jnp.float32),
        jnp.zeros((KEY_DIM,), jnp.float32),
        jnp.full((), lowest, jnp.float32),
    )

    def fold_block(carry_in, segment):
        return (combine_segments(carry_in, segment), None)

    summary, _ = lax.scan(fold_block, neutral, segments)
    prefix = entering_2(summary, EP, combine_segments, neutral)
    start_state = (
        jnp.zeros((), jnp.float32),
        jnp.zeros((KEY_DIM, channels), jnp.float32),
        jnp.zeros((KEY_DIM,), jnp.float32),
        jnp.zeros((), jnp.float32),
    )
    entering = combine_segments(start_state, prefix)
    causal = jnp.tril(jnp.ones((BLOCK, BLOCK), dtype=bool))

    def block_pass(carry_in, inputs):
        query_block, key_block, value_block, input_block, cumulative_block, segment = inputs
        _, memory, normalizer, running = carry_in
        carried = cumulative_block + running
        log_weight = cumulative_block[:, None] - cumulative_block[None, :] + input_block[None, :]
        log_weight = jnp.where(causal, log_weight, -jnp.inf)
        stabilizer = jnp.maximum(carried, jnp.max(log_weight, axis=1))
        within = jnp.exp(log_weight - stabilizer[:, None])
        across = jnp.exp(carried - stabilizer)
        scores = (
            jnp.einsum("td,sd->ts", query_block, key_block, preferred_element_type=jnp.float32)
            * factor
        )
        weights = scores * within
        scaled = query_block.astype(jnp.float32) * factor
        numerator = across[:, None] * jnp.dot(scaled, memory, precision=lax.Precision.HIGHEST)
        numerator = numerator + jnp.dot(
            weights.astype(jnp.bfloat16), value_block, preferred_element_type=jnp.float32
        )
        denominator = across * jnp.dot(scaled, normalizer, precision=lax.Precision.HIGHEST)
        denominator = denominator + jnp.sum(weights, axis=1)
        hidden = numerator / jnp.maximum(jnp.abs(denominator), den_floor)[:, None]
        return (combine_segments(carry_in, segment), hidden)

    _, hidden = lax.scan(
        block_pass, entering, (query_head, key_head, value_blocks, input_head, cumulative, segments)
    )
    gated_rows = (
        hidden.reshape(length, channels) * jax.nn.sigmoid(out_gate.astype(jnp.float32))
    ).astype(jnp.bfloat16)
    return jnp.dot(gated_rows, mix_weight, preferred_element_type=jnp.float32)


def expert_half(
    expert_input,
    norm_gain,
    route_ids,
    route_weights,
    expert_gate,
    expert_up,
    expert_down,
    shared_gate,
    shared_up,
    shared_down,
):
    ep_count = lax.axis_size(EP)
    tp_count = lax.axis_size("tp")
    tp_rank = lax.axis_index("tp")
    tokens = expert_input.shape[0]
    top_count = route_ids.shape[1]
    slice_units = expert_gate.shape[2]
    group_size = FF // slice_units
    per_ep = tp_count // group_size
    team_index = tp_rank // group_size
    expert_count = ep_count * per_ep
    capacity = 2 * tokens * top_count // expert_count
    rows_wide = expert_input.astype(jnp.float32)
    normed = (
        rows_wide
        * lax.rsqrt(jnp.mean(rows_wide * rows_wide, axis=-1, keepdims=True) + epsilon)
        * norm_gain
    ).astype(jnp.bfloat16)
    chosen = route_ids.reshape(-1)
    onehot = (chosen[:, None] == jnp.arange(expert_count, dtype=jnp.int32)[None, :]).astype(
        jnp.int32
    )
    slot_rank = jnp.sum((jnp.cumsum(onehot, axis=0) - onehot) * onehot, axis=1)
    in_team = chosen % per_ep == team_index
    target = jnp.where(in_team, chosen // per_ep * capacity + slot_rank, ep_count * capacity)
    token_of = jnp.arange(chosen.shape[0], dtype=jnp.int32) // top_count
    slot_token = jnp.zeros((ep_count * capacity,), jnp.int32).at[target].set(token_of, mode="drop")
    slot_live = jnp.zeros((ep_count * capacity,), jnp.int32).at[target].set(1, mode="drop")
    outgoing = jnp.where(slot_live[:, None] > 0, normed[slot_token], jnp.zeros((), jnp.bfloat16))
    outgoing = outgoing.reshape(ep_count, capacity, D)
    gate_slice = expert_gate[0]
    up_slice = expert_up[0]
    down_slice = expert_down[0]
    arrived = lax.all_to_all(outgoing, EP, split_axis=0, concat_axis=0, tiled=True)
    gate_val = jnp.einsum("sid,df->sif", arrived, gate_slice, preferred_element_type=jnp.float32)
    up_val = jnp.einsum("sid,df->sif", arrived, up_slice, preferred_element_type=jnp.float32)
    hidden = (jax.nn.silu(gate_val) * up_val).astype(jnp.bfloat16)
    partial_value = jnp.einsum(
        "sif,fd->sid", hidden, down_slice, preferred_element_type=jnp.float32
    )
    partial_value = partial_value.astype(jnp.bfloat16)
    returned = lax.all_to_all(partial_value, EP, split_axis=0, concat_axis=0, tiled=True)
    flat_back = returned.reshape(ep_count * capacity, returned.shape[2])
    gather_at = jnp.where(in_team, target, 0).reshape(tokens, top_count)
    weight_at = jnp.where(in_team, route_weights.reshape(-1), 0.0).reshape(tokens, top_count)
    combined = jnp.zeros((tokens, returned.shape[2]), jnp.float32)
    for pick_index in range(top_count):
        combined = (
            combined
            + flat_back[gather_at[:, pick_index]].astype(jnp.float32)
            * weight_at[:, pick_index][:, None]
        )
    shared_gate_val = jnp.dot(normed, shared_gate, preferred_element_type=jnp.float32)
    shared_up_val = jnp.dot(normed, shared_up, preferred_element_type=jnp.float32)
    shared_act = (jax.nn.silu(shared_gate_val) * shared_up_val).astype(jnp.bfloat16)
    return combined + jnp.dot(shared_act, shared_down, preferred_element_type=jnp.float32)


def shards(
    queries,
    key_vectors,
    values,
    out_gate,
    input_gate,
    forget_gate,
    mix_weight,
    expert_input,
    norm_gain,
    route_ids,
    route_weights,
    expert_gate,
    expert_up,
    expert_down,
    shared_gate,
    shared_up,
    shared_down,
):
    mixer_partial = mixer_half(
        queries, key_vectors, values, out_gate, input_gate, forget_gate, mix_weight
    )
    expert_partial = expert_half(
        expert_input,
        norm_gain,
        route_ids,
        route_weights,
        expert_gate,
        expert_up,
        expert_down,
        shared_gate,
        shared_up,
        shared_down,
    )
    mixer_piece = summed_on_arrival(mixer_partial.astype(jnp.bfloat16), "tp", 0).astype(
        jnp.bfloat16
    )
    mixer_out = lax.all_gather(mixer_piece, "tp", axis=0, tiled=True)
    expert_piece = lax.psum_scatter(expert_partial, "tp", scatter_dimension=0, tiled=True).astype(
        jnp.bfloat16
    )
    expert_out = collect(expert_piece, "tp", 0)
    return (mixer_out, expert_out)


def solution(mesh):
    finer = Mesh(mesh.devices.reshape(8, 4, mesh.shape["tp"]), ("ep_0", "ep_1", "tp"))
    placed = (
        P(EP, None),
        P(EP, None),
        P(EP, "tp"),
        P(EP, "tp"),
        P(EP, None),
        P(EP, None),
        P("tp", None),
        P(EP, None),
        P(),
        P(EP, None),
        P(EP, None),
        P(EP_TP, None, None),
        P(EP_TP, None, None),
        P(EP_TP, None, None),
        P(None, "tp"),
        P(None, "tp"),
        P("tp", None),
    )
    return jax.shard_map(
        shards, mesh=finer, in_specs=placed, out_specs=(P(EP, None), P(EP, None)), check_vma=False
    )
```

profile of v0, /device:TPU:1, one launch (start us, length us, event | category | flops | bytes accessed | tf_op | source)
XLA Modules:
  0.0 426.6 jit_solution(15270256443497055373)
XLA Ops:
  7.2 0.9 copy.108
  8.6 18.0 %reduce-window.6 = s32[64,8,128]{2,1,0:T(8,128)S(1)} reduce-window(s32[64,8,128]{2,1,0:T(8,128)S(1)} %fusion.29, s32[]{:T(128)} %constant.140.clone.1), window={size=1x1x128 pad=0_0x0_0x127_0}, to_apply=%region_8.9 | reduce-window | flops 8323072 | bytes 524292 | tf_op jit(solution)/shard_map/reduce-window
  27.3 4.3 %scatter_custom_fusion.1 = s32[1024]{0:T(1024)S(1)} fusion(s32[1024]{0:T(1024)S(1)} %bitcast.173, s32[1024]{0:T(1024)S(1)} %add_select_fusion.3, s32[]{:T(128)} %constant.140.clone.1), kind=kCustom, calls=%fused_computation.234 | custom fusion | bytes 4100 | tf_op jit(solution)/shard_map/scatter | solution.py:227
  31.6 0.3 fusion.1
  31.9 4.3 %scatter_custom_fusion = s32[1024]{0:T(1024)S(1)} fusion(s32[1024]{0:T(1024)S(1)} %bitcast.174, s32[1024]{0:T(1024)S(1)} %broadcast.491, s32[]{:T(128)} %constant.140.clone.1), kind=kCustom, calls=%fused_computation.237 | custom fusion | bytes 4100 | tf_op jit(solution)/shard_map/scatter | solution.py:228
  36.3 0.3 fusion.3
  36.6 6.0 %gather_fusion = bf16[1024,2048]{1,0:T(8,128)(2,1)} fusion(bf16[256,2048]{1,0:T(8,128)(2,1)S(1)} %fusion.3, s32[1024]{0:T(1024)S(1)} %fusion.157), kind=kCustom, calls=%fused_computation | custom fusion | bytes 8392704 | tf_op jit(solution)/shard_map/gather | solution.py:229
  42.7 2.5 broadcast_select_fusion
  45.2 107.2 %all_to_all.20 = bf16[32,32,2048]{2,1,0:T(8,128)(2,1)S(1)} all-to-all(bf16[32,32,2048]{2,1,0:T(8,128)(2,1)S(1)} %broadcast_select_fusion), channel_id=1, replica_groups=mesh['ep_0'=8,'ep_1'=4,'tp'=16] {'ep_0','ep_1'}, dimensions={0} | all-to-all | bytes 8388608 | tf_op jit(solution)/shard_map/all_to_all | solution.py:234
  152.5 1.9 copy-done.1
  154.4 1.2 fusion.18
  155.7 8.5 %convolution_convert_fusion = bf16[32,32,2048]{2,1,0:T(8,128)(2,1)} fusion(bf16[32,32,2048]{2,1,0:T(8,128)(2,1)} %copy-done.1, bf16[1,128,2048]{2,1,0:T(8,128)(2,1)S(1)} %copy-done, bf16[1,2048,128]{2,1,0:T(8,128)(2,1)S(1)} %copy-done.4, f32[32,32,128]{2,1,0:T(8,128)S(1)} %fusion.18), kind=kOutput, calls=%fused_computation.8 | convolution fusion | flops 1076625408 | bytes 9961472 | tf_op jit(solution)/shard_map/sif,fd->sid/dot_general | solution.py:238
  164.2 6.7 %all-to-all-start.2 = ((bf16[32,32,2048]{2,1,0:T(8,128)(2,1)}), bf16[32,32,2048]{2,1,0:T(8,128)(2,1)}, u32[]{:S(2)}, u32[]{:S(2)}) async-start(bf16[32,32,2048]{2,1,0:T(8,128)(2,1)} %convolution_convert_fusion), calls=%async_computation.2 | async-start | bytes 8388608 | tf_op jit(solution)/shard_map/all_to_all | solution.py:242
  171.2 0.3 reduce_window_sum.26
  171.5 0.6 slice.281
  172.7 1.2 fusion.178
  175.4 1.3 subtract_exponential_fusion.1
  177.1 0.6 pad_bitcast_fusion.3
  178.2 20.0 %all-gather.2 = f32[4,262,64]{1,2,0:T(8,128)S(1)} all-gather(f32[1,262,64]{1,2,0:T(8,128)S(1)} %maximum_bitcast_fusion), channel_id=2, replica_groups=mesh['ep_0'=8,'ep_1'=4,'tp'=16] {'ep_1'}, dimensions={0}, use_global_device_ids=true | all-gather | bytes 335360 | tf_op jit(solution)/shard_map/all_gather | solution.py:35
  198.5 0.6 fusion.185
  208.8 0.3 copy-done.13
  209.4 0.6 copy-done.19
  211.3 0.7 copy.96
  212.1 0.3 fusion.33
  212.5 0.6 pad_clamp_fusion.2
  213.1 0.6 pad_clamp_fusion
  213.8 0.9 slice_reduce_fusion.3
  214.7 0.4 fusion.188
  215.1 48.3 %all-to-all-done.2 = bf16[32,32,2048]{2,1,0:T(8,128)(2,1)} async-done(((bf16[32,32,2048]{2,1,0:T(8,128)(2,1)}), bf16[32,32,2048]{2,1,0:T(8,128)(2,1)}, u32[]{:S(2)}, u32[]{:S(2)}) %all-to-all-start.2) | async-done | bytes 4194336 | tf_op jit(solution)/shard_map/all_to_all | solution.py:242
  263.5 5.2 %gather_fusion.1 = bf16[256,2048]{1,0:T(8,128)(2,1)S(1)} fusion(bf16[1024,2048]{1,0:T(8,128)(2,1)} %bitcast.58, s32[1024]{0:T(1024)} %get-tuple-element.135), kind=kCustom, calls=%fused_computation.1 | custom fusion | bytes 2098176 | tf_op jit(solution)/shard_map/gather | solution.py:250
  268.7 6.2 %gather_fusion.2 = bf16[256,2048]{1,0:T(8,128)(2,1)} fusion(bf16[1024,2048]{1,0:T(8,128)(2,1)} %bitcast.58, s32[1024]{0:T(1024)} %get-tuple-element.134), kind=kCustom, calls=%fused_computation.2 | custom fusion | bytes 2098176 | tf_op jit(solution)/shard_map/gather | solution.py:250
  274.9 6.2 %gather_fusion.3 = bf16[256,2048]{1,0:T(8,128)(2,1)} fusion(bf16[1024,2048]{1,0:T(8,128)(2,1)} %bitcast.58, s32[1024]{0:T(1024)} %get-tuple-element.133), kind=kCustom, calls=%fused_computation.3 | custom fusion | bytes 2098176 | tf_op jit(solution)/shard_map/gather | solution.py:250
  281.2 6.2 %gather_fusion.4 = bf16[256,2048]{1,0:T(8,128)(2,1)} fusion(bf16[1024,2048]{1,0:T(8,128)(2,1)} %bitcast.58, s32[1024]{0:T(1024)} %get-tuple-element.132), kind=kCustom, calls=%fused_computation.4 | custom fusion | bytes 2098176 | tf_op jit(solution)/shard_map/gather | solution.py:250
  287.4 5.0 %convolution_add_fusion = f32[256,2048]{1,0:T(8,128)} fusion(bf16[32,2048]{1,0:T(8,128)(2,1)S(1)} %copy-done.6, bf16[256,2048]{1,0:T(8,128)(2,1)} %gather_fusion.4, bf16[256,2048]{1,0:T(8,128)(2,1)} %gather_fusion.3, bf16[256,2048]{1,0:T(8,128)(2,1)} %gather_fusion.2, bf16[256,2048]{1,0:T(8,128)(2,1)S(1)} %gather_fusion.1, bf16[256,2048]{1,0:T(8,128)(2,1)S(1)} %fusion.3, ...), kind=kOutput, calls=%fused_computation.9 | convolution fusion | flops 73449472 | bytes 7639040 | tf_op jit(solution)/shard_map/dot_general | solution.py:256
  292.6 0.6 copy-done.10
  293.3 21.1 %all-gather.3 = f32[8,262,64]{1,2,0:T(8,128)S(1)} all-gather(f32[1,262,64]{1,2,0:T(8,128)S(1)} %maximum_bitcast_fusion.1), channel_id=3, replica_groups=mesh['ep_0'=8,'ep_1'=4,'tp'=16] {'ep_0'}, dimensions={0}, use_global_device_ids=true | all-gather | bytes 603648 | tf_op jit(solution)/shard_map/all_gather | solution.py:35
  314.7 0.6 fusion.184
  316.1 0.6 fusion.183
  340.4 0.4 convolution_multiply_fusion.4
  340.8 1.3 fusion
  342.1 16.0 %all-to-all-start = ((bf16[16,8,2048]{2,1,0:T(8,128)(2,1)}), bf16[16,8,2048]{2,1,0:T(8,128)(2,1)S(1)}, u32[]{:S(2)}, u32[]{:S(2)}) async-start(bf16[16,8,2048]{2,1,0:T(8,128)(2,1)} %fusion), calls=%async_computation | async-start | bytes 1048576 | tf_op jit(solution)/shard_map/all_to_all | solution.py:66
  358.1 0.9 convert_element_type.83
  359.0 16.3 %all-to-all-done = bf16[16,8,2048]{2,1,0:T(8,128)(2,1)S(1)} async-done(((bf16[16,8,2048]{2,1,0:T(8,128)(2,1)}), bf16[16,8,2048]{2,1,0:T(8,128)(2,1)S(1)}, u32[]{:S(2)}, u32[]{:S(2)}) %all-to-all-start) | async-done | bytes 524320 | tf_op jit(solution)/shard_map/all_to_all | solution.py:66
  375.3 1.1 broadcast_in_dim.93
  376.4 3.6 all-to-all-start.3
  380.0 37.9 %all_gather.19 = bf16[128,2048]{1,0:T(8,128)(2,1)S(1)} all-gather(bf16[8,2048]{1,0:T(8,128)(2,1)S(1)} %reduce_sum.75), channel_id=1, replica_groups=mesh['ep_0'=8,'ep_1'=4,'tp'=16] {'tp'}, dimensions={0}, use_global_device_ids=true | all-gather | bytes 557056 | tf_op jit(solution)/shard_map/all_gather | solution.py:296
  418.0 0.8 copy.149
  418.8 1.0 copy.150
  (135 shorter events, 6.0 us)
Async XLA Ops:
  7.2 148.5 %copy-start = (bf16[1,128,2048]{2,1,0:T(8,128)(2,1)S(1)}, bf16[1,128,2048]{2,1,0:T(8,128)(2,1)}, u32[]{:S(2)}) copy-start(bf16[1,128,2048]{2,1,0:T(8,128)(2,1)} %param.30) | copy-start | bytes 1572868
  7.2 24.4 %copy-start.2 = (bf16[256,2048]{1,0:T(8,128)(2,1)S(1)}, bf16[256,2048]{1,0:T(8,128)(2,1)}, u32[]{:S(2)}) copy-start(bf16[256,2048]{1,0:T(8,128)(2,1)} %param.24) | copy-start | bytes 3145732
  7.2 29.1 %copy-start.25 = (f32[2048]{0:T(1024)S(1)}, f32[2048]{0:T(1024)}, u32[]{:S(2)}) copy-start(f32[2048]{0:T(1024)} %param.25) | copy-start | bytes 24580
  45.2 109.2 %copy-start.3 = (bf16[1,2048,128]{2,1,0:T(8,128)(2,1)S(1)}, bf16[1,2048,128]{2,1,0:T(8,128)(2,1)}, u32[]{:S(2)}) copy-start(bf16[1,2048,128]{2,1,0:T(8,128)(2,1)} %param.28) | copy-start | bytes 1572868
  152.5 1.9 copy-start.1
  154.4 1.3 copy-start.4
  164.2 6.9 %copy-start.29 = (f32[128,2]{0,1:T(2,128)S(1)}, f32[128,2]{0,1:T(2,128)}, u32[]{:S(2)}) copy-start(f32[128,2]{0,1:T(2,128)} %param.21) | copy-start | bytes 3076
  164.2 6.9 %copy-start.30 = (f32[128,2]{0,1:T(2,128)S(1)}, f32[128,2]{0,1:T(2,128)}, u32[]{:S(2)}) copy-start(f32[128,2]{0,1:T(2,128)} %param.22) | copy-start | bytes 3076
  164.2 12.5 %copy-start.9 = (bf16[128,512]{1,0:T(8,128)(2,1)S(1)}, bf16[128,512]{1,0:T(8,128)(2,1)}, u32[]{:S(2)}) copy-start(bf16[128,512]{1,0:T(8,128)(2,1)} %param.18) | copy-start | bytes 393220
  164.2 13.7 %copy-start.11 = (bf16[128,64]{0,1:T(8,128)(2,1)S(1)}, bf16[128,64]{0,1:T(8,128)(2,1)}, u32[]{:S(2)}) copy-start(bf16[128,64]{0,1:T(8,128)(2,1)} %param.19) | copy-start | bytes 49156
  164.2 43.6 %copy-start.22 = (s32[256,4]{0,1:T(4,128)S(1)}, s32[256,4]{0,1:T(4,128)}, u32[]{:S(2)}) copy-start(s32[256,4]{0,1:T(4,128)} %param.26) | copy-start | bytes 12292
  164.2 43.8 %copy-start.28 = (f32[256,4]{0,1:T(4,128)S(1)}, f32[256,4]{0,1:T(4,128)}, u32[]{:S(2)}) copy-start(f32[256,4]{0,1:T(4,128)} %param.27) | copy-start | bytes 12292
  164.2 99.3 %all-to-all-start.2 = ((bf16[32,32,2048]{2,1,0:T(8,128)(2,1)}), bf16[32,32,2048]{2,1,0:T(8,128)(2,1)}, u32[]{:S(2)}, u32[]{:S(2)}) async-start(bf16[32,32,2048]{2,1,0:T(8,128)(2,1)} %convolution_convert_fusion), calls=%async_computation.2 | async-start | bytes 8388608 | tf_op jit(solution)/shard_map/all_to_all | solution.py:242
  170.9 187.2 %reduce-scatter.2.cloned.1.call-start = ((), (), s32[]{:S(2)}) async-start(), calls=%async_computation.5 | async-start | bytes 2228224 | tf_op jit(solution)/shard_map/reduce_scatter | solution.py:297
  171.2 5.6 %copy-start.26 = (f32[128]{0:T(128)}, f32[128]{0:T(128)S(1)}, u32[]{:S(2)}) copy-start(f32[128]{0:T(128)S(1)} %get-tuple-element.69) | copy-start | bytes 1540
  171.5 37.0 %copy-start.23 = (f32[1,128]{1,0:T(1,128)}, f32[1,128]{1,0:T(1,128)S(1)}, u32[]{:S(2)}) copy-start(f32[1,128]{1,0:T(1,128)S(1)} %reduce_window_sum.26) | copy-start | bytes 1540
  177.9 36.9 %copy-start.8 = (bf16[2048,32]{0,1:T(8,128)(2,1)S(1)}, bf16[2048,32]{0,1:T(8,128)(2,1)}, u32[]{:S(2)}) copy-start(bf16[2048,32]{0,1:T(8,128)(2,1)} %param.31) | copy-start | bytes 393220
  208.6 0.6 copy-start.13
  208.7 0.6 copy-start.15
  208.8 0.6 copy-start.17
  209.4 0.6 copy-start.19
  281.2 6.2 %copy-start.6 = (bf16[32,2048]{1,0:T(8,128)(2,1)S(1)}, bf16[32,2048]{1,0:T(8,128)(2,1)}, u32[]{:S(2)}) copy-start(bf16[32,2048]{1,0:T(8,128)(2,1)} %param.33) | copy-start | bytes 393220
  281.2 6.2 %copy-start.7 = (bf16[2048,32]{0,1:T(8,128)(2,1)S(1)}, bf16[2048,32]{0,1:T(8,128)(2,1)}, u32[]{:S(2)}) copy-start(bf16[2048,32]{0,1:T(8,128)(2,1)} %param.32) | copy-start | bytes 393220
  292.4 0.8 copy-start.10
  292.5 47.1 %copy-start.14 = (f32[1,4,64]{2,1,0:T(4,128)S(1)}, f32[1,4,64]{2,1,0:T(4,128)}, u32[]{:S(2)}) copy-start(f32[1,4,64]{2,1,0:T(4,128)} %copy-done.13) | copy-start | bytes 3076
  292.5 47.1 %copy-start.16 = (f32[1,4,64]{2,1,0:T(4,128)S(1)}, f32[1,4,64]{2,1,0:T(4,128)}, u32[]{:S(2)}) copy-start(f32[1,4,64]{2,1,0:T(4,128)} %copy-done.15) | copy-start | bytes 3076
  292.5 47.1 %copy-start.18 = (f32[1,4,64]{2,1,0:T(4,128)S(1)}, f32[1,4,64]{2,1,0:T(4,128)}, u32[]{:S(2)}) copy-start(f32[1,4,64]{2,1,0:T(4,128)} %copy-done.17) | copy-start | bytes 3076
  292.5 47.1 %copy-start.20 = (f32[1,4,64]{2,1,0:T(4,128)S(1)}, f32[1,4,64]{2,1,0:T(4,128)}, u32[]{:S(2)}) copy-start(f32[1,4,64]{2,1,0:T(4,128)} %copy-done.19) | copy-start | bytes 3076
  292.5 47.3 %copy-start.24 = (f32[1,128]{1,0:T(1,128)S(1)}, f32[1,128]{1,0:T(1,128)}, u32[]{:S(2)}) copy-start(f32[1,128]{1,0:T(1,128)} %copy-done.23) | copy-start | bytes 1540
  292.5 47.3 %copy-start.27 = (f32[128]{0:T(128)S(1)}, f32[128]{0:T(128)}, u32[]{:S(2)}) copy-start(f32[128]{0:T(128)} %copy-done.26) | copy-start | bytes 1540
  292.5 47.5 %copy-start.12 = (bf16[128,512]{1,0:T(8,128)(2,1)S(1)}, bf16[128,512]{1,0:T(8,128)(2,1)}, u32[]{:S(2)}) copy-start(bf16[128,512]{1,0:T(8,128)(2,1)} %param.17) | copy-start | bytes 393220
  314.3 26.5 %copy-start.5 = (bf16[64,2048]{1,0:T(8,128)(2,1)S(1)}, bf16[64,2048]{1,0:T(8,128)(2,1)}, u32[]{:S(2)}) copy-start(bf16[64,2048]{1,0:T(8,128)(2,1)} %param.23) | copy-start | bytes 786436
  314.4 26.5 %copy-start.21 = (bf16[128,64]{0,1:T(8,128)(2,1)S(1)}, bf16[128,64]{0,1:T(8,128)(2,1)}, u32[]{:S(2)}) copy-start(bf16[128,64]{0,1:T(8,128)(2,1)} %param.20) | copy-start | bytes 49156
  342.1 33.2 %all-to-all-start = ((bf16[16,8,2048]{2,1,0:T(8,128)(2,1)}), bf16[16,8,2048]{2,1,0:T(8,128)(2,1)S(1)}, u32[]{:S(2)}, u32[]{:S(2)}) async-start(bf16[16,8,2048]{2,1,0:T(8,128)(2,1)} %fusion), calls=%async_computation | async-start | bytes 1048576 | tf_op jit(solution)/shard_map/all_to_all | solution.py:66
  376.4 41.6 %all-to-all-start.3 = ((bf16[16,16,2048]{2,1,0:T(8,128)(2,1)}), bf16[16,16,2048]{2,1,0:T(8,128)(2,1)S(1)}, u32[]{:S(2)}, u32[]{:S(2)}) async-start(bf16[16,16,2048]{2,1,0:T(8,128)(2,1)} %broadcast_in_dim.93), calls=%async_computation.4 | async-start | bytes 2097152 | tf_op jit(solution)/shard_map/all_to_all | solution.py:72
Sparse Core Ops, SparseCore 0:
  292.6 61.3 reduce-scatter.1
where the time goes:
time: 428 us; the launch traced here: 427 us
  blocking collectives  186 us (43%)
  waiting for transfers between devices  64.6 us (15%)
  local copies, waits for them, and re-layouts  54.5 us (13%)
  between operations  49.7 us (12%)
  other arithmetic  27.8 us (6%)
  starting transfers between devices  26.2 us (6%)
  matrix products  17.5 us (4%)
    all_to_all x1, blocking collectives, expert_half(): lax.all_to_all(outgoing, EP, split_axis=0, concat_axis=0, tiled=True)  107 us
    all_to_all x1, waiting for transfers between devices, expert_half(): lax.all_to_all(partial_value, EP, split_axis=0, concat_axis=0, tiled=True)  48.3 us
    all_gather x2, blocking collectives, all_in_one(): both, at, found = (lax.all_gather(jnp.concatenate(lines), axis), 0, {})  41.1 us
    all_gather x1, blocking collectives, shards(): mixer_out = lax.all_gather(mixer_piece, 'tp', axis=0, tiled=True)  37.9 us
    gather x4, local copies, waits for them, and re-layouts, expert_half(): flat_back[gather_at[:, pick_index]].astype(jnp.float32)  23.9 us
    another operation x3, other arithmetic  18.2 us
    all_to_all x1, waiting for transfers between devices, summed_on_arrival(): lax.all_to_all(blocks, axis, split_axis=0, concat_axis=0, tiled=True)  16.3 us
    all_to_all x1, starting transfers between devices, summed_on_arrival(): lax.all_to_all(blocks, axis, split_axis=0, concat_axis=0, tiled=True)  16 us
  transfers between devices with their start and end apart: 4, of which 2 were waited for; matrix products, arithmetic and copies ran while one was open for 4% of the time, Pallas kernels for 0%

commit v1 on v0

v1 whole, which is shorter than its diff:
```python
import functools

import jax
import jax.numpy as jnp
from jax import lax
from jax.experimental import pallas as pl
from jax.experimental.pallas import tpu as pltpu
from jax.sharding import Mesh
from jax.sharding import PartitionSpec as P

D = 2048
KEY_DIM = 256
BLOCK = 128
N_EP = 32
SLOTS = 8
TOKENS = 256
EP = ("z", "x")
EP_TP = ("z", "x", "y", "c")
TP = ("y", "c")
bf16 = jnp.bfloat16
f32 = jnp.float32
epsilon = 1e-06
lowest = -1e30
den_floor = 4.0
HIGHEST = lax.Precision.HIGHEST

VMEM = pl.BlockSpec(memory_space=pltpu.VMEM)
SMEM = pl.BlockSpec(memory_space=pltpu.SMEM)
NT = (((1,), (1,)), ((), ()))
TN = (((0,), (0,)), ((), ()))


def call(body, place, arrays, outs, flops):
    return pl.pallas_call(
        body,
        out_shape=outs,
        in_specs=[SMEM] + [VMEM] * len(arrays),
        out_specs=[VMEM] * len(outs),
        compiler_params=pltpu.CompilerParams(vmem_limit_bytes=48 << 20),
        cost_estimate=pl.CostEstimate(flops=flops, bytes_accessed=1 << 20, transcendentals=0),
    )(place, *arrays)


def shape(dims, dtype):
    return jax.ShapeDtypeStruct(dims, dtype)


def iota(dims, dim):
    return lax.broadcasted_iota(jnp.int32, dims, dim)


def route_kernel(place, x, gain, ids, weights, send, normed, w_high, w_low):
    team, part = place[0], place[1]
    rows = x[...].astype(f32)
    scale = lax.rsqrt(jnp.mean(rows * rows, axis=-1, keepdims=True) + epsilon)
    normal = (rows * scale * gain[...]).astype(bf16)
    normed[...] = normal
    expert = iota((N_EP, TOKENS), 0) * 2 + team
    named = jnp.zeros((N_EP, TOKENS), f32)
    weight = jnp.zeros((N_EP, TOKENS), f32)
    for k in range(4):
        hit = ids[k : k + 1, :] == expert
        named = named + jnp.where(hit, 1.0, 0.0)
        weight = weight + jnp.where(hit, weights[k : k + 1, :], 0.0)
    before = jnp.where(iota((TOKENS, TOKENS), 0) < iota((TOKENS, TOKENS), 1), 1.0, 0.0).astype(bf16)
    rank = jnp.dot(named.astype(bf16), before, preferred_element_type=f32)
    rank = jnp.where(named > 0.0, rank, -1.0)
    slots = N_EP * SLOTS
    spread = jnp.where(iota((slots, N_EP), 0) // SLOTS == iota((slots, N_EP), 1), 1.0, 0.0)
    rank = jnp.dot(spread.astype(bf16), rank.astype(bf16), preferred_element_type=f32)
    weight = jnp.dot(spread, weight, preferred_element_type=f32, precision=HIGHEST)
    slot = (iota((slots, TOKENS), 0) % SLOTS + part * SLOTS).astype(f32)
    chosen = rank == slot
    pick = jnp.where(chosen, 1.0, 0.0).astype(bf16)
    send[...] = jnp.dot(pick, normal, preferred_element_type=f32).astype(bf16)
    weight = jnp.where(chosen, weight, 0.0)
    high = weight.astype(bf16)
    w_high[...] = high
    w_low[...] = (weight - high.astype(f32)).astype(bf16)


def pack_kernel(place, gate, up, down, packed):
    packed[0:D, :] = gate[...]
    packed[D : 2 * D, :] = up[...]
    for k in range(16):
        packed[2 * D + 128 * k : 2 * D + 128 * (k + 1), :] = down[:, 128 * k : 128 * (k + 1)]


def expert_kernel(place, x, own, core, near, far, out):
    rows = x[...]
    acts = []
    packs = (own, core, near, far)
    for pack in packs:
        gate = jnp.dot(rows, pack[0:D, :], preferred_element_type=f32)
        up = jnp.dot(rows, pack[D : 2 * D, :], preferred_element_type=f32)
        acts.append((gate / (1.0 + jnp.exp(-gate)) * up).astype(bf16))
    for k in range(16):
        part = slice(2 * D + 128 * k, 2 * D + 128 * (k + 1))
        total = jnp.zeros((TOKENS, 128), f32)
        for act, pack in zip(acts, packs):
            total = total + jnp.dot(act, pack[part, :], preferred_element_type=f32)
        out[:, 128 * k : 128 * (k + 1)] = total.astype(bf16)


def shared_kernel(place, x, gate, up, act):
    rows = x[...]
    gated = lax.dot_general(rows, gate[...], NT, preferred_element_type=f32)
    lifted = lax.dot_general(rows, up[...], NT, preferred_element_type=f32)
    act[...] = (gated / (1.0 + jnp.exp(-gated)) * lifted).astype(bf16)


def combine_kernel(place, back, w_high, w_low, act, down, keep, give, total):
    core = place[2]
    rows = back[...]
    total[...] = (
        lax.dot_general(w_high[...], rows, TN, preferred_element_type=f32)
        + lax.dot_general(w_low[...], rows, TN, preferred_element_type=f32)
        + jnp.dot(act[...], down[...], preferred_element_type=f32)
    )
    half = TOKENS // 2
    keep[...] = total[pl.ds(pl.multiple_of(core * half, half), half), :]
    give[...] = total[pl.ds(pl.multiple_of((1 - core) * half, half), half), :].astype(bf16)


def gates(place, input_gate, forget_gate):
    first = place[0] == 0
    given = jnp.where(first, input_gate[0:1, :], input_gate[1:2, :])
    forget = jnp.where(first, forget_gate[0:1, :], forget_gate[1:2, :])
    small = jnp.exp(-jnp.abs(forget))
    tail = jnp.where(small < 1e-4, small - 0.5 * small * small, jnp.log(1.0 + small))
    log_forget = jnp.minimum(forget, 0.0) - tail
    upto = jnp.where(iota((BLOCK, BLOCK), 0) <= iota((BLOCK, BLOCK), 1), 1.0, 0.0)
    cumulative = jnp.dot(
        jnp.broadcast_to(log_forget, (8, BLOCK)), upto, preferred_element_type=f32, precision=HIGHEST
    )[0:1, :]
    return given, cumulative


def state_kernel(place, keys, values, input_gate, forget_gate, out):
    given, cumulative = gates(place, input_gate, forget_gate)
    block_total = cumulative[:, BLOCK - 1 : BLOCK]
    log_keep = block_total - cumulative + given
    running = jnp.max(log_keep, axis=1, keepdims=True)
    kept = jnp.exp(log_keep - running)
    key = keys[:, pl.ds(pl.multiple_of(place[0] * KEY_DIM, KEY_DIM), KEY_DIM)].astype(f32)
    memory = jnp.dot(
        values[...].astype(f32) * kept, key, preferred_element_type=f32, precision=HIGHEST
    )
    normalizer = jnp.dot(
        jnp.broadcast_to(kept, (8, BLOCK)), key, preferred_element_type=f32, precision=HIGHEST
    )
    out[:, 0, :] = memory[0:32, 0:128]
    out[:, 1, :] = memory[0:32, 128:256]
    out[:, 2, :] = memory[32:64, 0:128]
    out[:, 3, :] = memory[32:64, 128:256]
    out[:, 4, :] = jnp.broadcast_to(normalizer[0:1, 0:128], (N_EP, 128))
    out[:, 5, :] = jnp.broadcast_to(normalizer[0:1, 128:256], (N_EP, 128))
    out[:, 6, :] = jnp.broadcast_to(block_total, (N_EP, 128))
    out[:, 7, :] = jnp.broadcast_to(running, (N_EP, 128))


def prefix_kernel(place, states, out):
    totals = jnp.broadcast_to(states[:, 6, :][None], (4, N_EP, 128)).reshape(128, 128).T[0:N_EP, 0:N_EP]
    peaks = jnp.broadcast_to(states[:, 7, :][None], (4, N_EP, 128)).reshape(128, 128).T[0:N_EP, 0:N_EP]
    row, column = iota((N_EP, N_EP), 0), iota((N_EP, N_EP), 1)
    earlier = column < row
    passed = jnp.where(earlier, totals, 0.0)
    later = jnp.where(row > column, 1.0, 0.0)
    between = jnp.dot(passed, later, preferred_element_type=f32, precision=HIGHEST)
    reach = jnp.where(earlier, peaks + between, lowest)
    running = jnp.maximum(
        jnp.sum(passed, axis=1, keepdims=True), jnp.max(reach, axis=1, keepdims=True)
    )
    share = jnp.where(earlier, jnp.exp(reach - running), 0.0)
    for k in range(6):
        out[:, k, :] = jnp.dot(share, states[:, k, :], preferred_element_type=f32, precision=HIGHEST)
    out[:, 6, :] = jnp.broadcast_to(running, (N_EP, 128))
    out[:, 7, :] = jnp.zeros((N_EP, 128), f32)


def memory_kernel(
    place, states, queries, keys, values, out_gate, input_gate, forget_gate, mix, keep, give, total
):
    core = place[2]
    given, cumulative = gates(place, input_gate, forget_gate)
    at = pl.ds(pl.multiple_of(place[0] * KEY_DIM, KEY_DIM), KEY_DIM)
    query, key = queries[:, at], keys[:, at]
    factor = KEY_DIM ** (-0.5)
    carried = cumulative + states[0, 6:7, :]
    source = jnp.broadcast_to(given - cumulative, (BLOCK, BLOCK)).T
    allowed = iota((BLOCK, BLOCK), 0) <= iota((BLOCK, BLOCK), 1)
    log_weight = jnp.where(allowed, cumulative + source, lowest)
    stabilizer = jnp.maximum(carried, jnp.max(log_weight, axis=0, keepdims=True))
    within = jnp.exp(log_weight - stabilizer)
    across = jnp.exp(carried - stabilizer)
    scores = lax.dot_general(key, query, NT, preferred_element_type=f32) * factor
    weights = scores * within
    scaled = query.astype(f32) * factor

    def read(first, second):
        return lax.dot_general(
            first, scaled[:, 0:128], NT, preferred_element_type=f32, precision=HIGHEST
        ) + lax.dot_general(
            second, scaled[:, 128:256], NT, preferred_element_type=f32, precision=HIGHEST
        )

    numerator = jnp.concatenate(
        [read(states[:, 0, :], states[:, 1, :]), read(states[:, 2, :], states[:, 3, :])], axis=0
    )
    numerator = across * numerator + jnp.dot(
        values[...], weights.astype(bf16), preferred_element_type=f32
    )
    normalizer = read(
        jnp.broadcast_to(states[0, 4:5, :], (8, 128)), jnp.broadcast_to(states[0, 5:6, :], (8, 128))
    )
    denominator = across * normalizer[0:1, :] + jnp.sum(weights, axis=0, keepdims=True)
    hidden = numerator / jnp.maximum(jnp.abs(denominator), den_floor)
    gated = (hidden / (1.0 + jnp.exp(-out_gate[...].astype(f32)))).astype(bf16)
    total[...] = lax.dot_general(gated, mix[...], TN, preferred_element_type=f32)
    half = BLOCK // 2
    keep[...] = total[pl.ds(pl.multiple_of(core * half, half), half), :]
    give[...] = total[pl.ds(pl.multiple_of((1 - core) * half, half), half), :].astype(bf16)


def exchange(array, axis):
    return lax.all_to_all(array, axis, split_axis=0, concat_axis=0, tiled=True)


def swap(array):
    return lax.ppermute(array, "c", [(0, 1), (1, 0)])


def reach_over(array):
    return lax.ppermute(array, "y", [(k, k ^ 1) for k in range(8)])


def with_scratch(body, place, arrays, outs, flops, rows):
    return pl.pallas_call(
        body,
        out_shape=outs,
        in_specs=[SMEM] + [VMEM] * len(arrays),
        out_specs=[VMEM] * len(outs),
        scratch_shapes=[pltpu.VMEM((rows, D), f32)],
        compiler_params=pltpu.CompilerParams(vmem_limit_bytes=48 << 20),
        cost_estimate=pl.CostEstimate(flops=flops, bytes_accessed=1 << 20, transcendentals=0),
    )(place, *arrays)


def finish(keep, give, core):
    rows = keep.shape[0] // 8
    half = (keep + swap(give).astype(f32)).astype(bf16).reshape(8, rows, D)
    piece = exchange(half, "y").astype(f32).sum(axis=0).astype(bf16)
    mine = exchange(jnp.broadcast_to(piece[None], (8, rows, D)), "y").reshape(8 * rows, D)
    other = swap(mine)
    first = core == 0
    return jnp.concatenate([jnp.where(first, mine, other), jnp.where(first, other, mine)], axis=0)


def shards(
    queries,
    key_vectors,
    values,
    out_gate,
    input_gate,
    forget_gate,
    mix_weight,
    expert_input,
    norm_gain,
    route_ids,
    route_weights,
    expert_gate,
    expert_up,
    expert_down,
    shared_gate,
    shared_up,
    shared_down,
):
    y, core = lax.axis_index("y"), lax.axis_index("c")
    place = jnp.stack([y // 4, (y % 2) * 2 + core, core]).astype(jnp.int32)
    (own,) = call(
        pack_kernel,
        place,
        (expert_gate[0], expert_up[0], expert_down[0]),
        [shape((3 * D, 128), bf16)],
        1 << 20,
    )
    near = reach_over(own)
    beside = swap(own)
    far = swap(near)
    values_t, out_gate_t = values.T, out_gate.T
    input_t, forget_t = input_gate.T, forget_gate.T
    (states,) = call(
        state_kernel,
        place,
        (key_vectors, values_t, input_t, forget_t),
        [shape((N_EP, 8, 128), f32)],
        1 << 20,
    )
    states = exchange(states, EP)
    slots = N_EP * SLOTS
    send, normed, w_high, w_low = call(
        route_kernel,
        place,
        (expert_input, norm_gain[None, :], route_ids.T, route_weights.T),
        [
            shape((slots, D), bf16),
            shape((TOKENS, D), bf16),
            shape((slots, TOKENS), bf16),
            shape((slots, TOKENS), bf16),
        ],
        1 << 28,
    )
    arrived = exchange(send.reshape(N_EP, SLOTS, D), EP).reshape(slots, D)
    (states,) = call(prefix_kernel, place, (states,), [shape((N_EP, 8, 128), f32)], 1 << 20)
    states = exchange(states, EP)
    (act,) = call(
        shared_kernel, place, (normed, shared_gate.T, shared_up.T), [shape((TOKENS, 32), bf16)], 1 << 26
    )
    (results,) = call(
        expert_kernel, place, (arrived, own, beside, near, far), [shape((slots, D), bf16)], 1 << 31
    )
    back = exchange(results.reshape(N_EP, SLOTS, D), EP).reshape(slots, D)
    mixer_keep, mixer_give = with_scratch(
        memory_kernel,
        place,
        (
            states,
            queries,
            key_vectors,
            values_t,
            out_gate_t,
            input_t,
            forget_t,
            mix_weight,
        ),
        [shape((BLOCK // 2, D), f32), shape((BLOCK // 2, D), bf16)],
        1 << 26,
        BLOCK,
    )
    mixer_out = finish(mixer_keep, mixer_give, core)
    keep, give = with_scratch(
        combine_kernel,
        place,
        (back, w_high, w_low, act, shared_down),
        [shape((TOKENS // 2, D), f32), shape((TOKENS // 2, D), bf16)],
        1 << 28,
        TOKENS,
    )
    expert_out = finish(keep, give, core)
    return (mixer_out, expert_out)


def solution(mesh):
    finer = Mesh(mesh.devices.reshape(8, 4, 8, 2), EP_TP)
    placed = (
        P(EP, None),
        P(EP, None),
        P(EP, TP),
        P(EP, TP),
        P(EP, None),
        P(EP, None),
        P(TP, None),
        P(EP, None),
        P(),
        P(EP, None),
        P(EP, None),
        P(EP_TP, None, None),
        P(EP_TP, None, None),
        P(EP_TP, None, None),
        P(None, TP),
        P(None, TP),
        P(TP, None),
    )
    return jax.shard_map(
        shards, mesh=finer, in_specs=placed, out_specs=(P(EP, None), P(EP, None)), check_vma=False
    )
```

time: 428 us -> 208 us (0.49)
  blocking collectives: 186 us -> 0 us
  starting transfers between devices: 26.2 us -> 75.4 us
  between operations: 49.7 us -> 1.08 us
  local copies, waits for them, and re-layouts: 54.5 us -> 15.1 us
  waiting for transfers between devices: 64.6 us -> 93.4 us
  other arithmetic: 27.8 us -> 4.86 us
  matrix products: 17.5 us -> 0 us
  Pallas kernels: 0 us -> 17.2 us
    all_to_all x1 -> x0, blocking collectives: 107 us -> none  [expert_half(): lax.all_to_all(outgoing, EP, split_axis=0, concat_axis=0, tiled=True)]
    all_gather x3 -> x0, blocking collectives: 79 us -> none  [the longest x2 41.1 us: all_in_one(): both, at, found = (lax.all_gather(jnp.concatenate(lines), axis), 0, {})]
    gather x5 -> x0, local copies, waits for them, and re-layouts: 29.9 us -> none  [the longest x4 23.9 us: expert_half(): flat_back[gather_at[:, pick_index]].astype(jnp.float32)]
    all_to_all x3 -> x8, waiting for transfers between devices: 64.6 us -> 92.7 us  [exchange(): return lax.all_to_all(array, axis, split_axis=0, concat_axis=0, tiled=True)]
    ppermute x0 -> x7, starting transfers between devices: none -> 28.1 us  [the longest x6 24.1 us: swap(): return lax.ppermute(array, 'c', [(0, 1), (1, 0)])]
    all_to_all x3 -> x8, starting transfers between devices: 26.2 us -> 47.3 us  [exchange(): return lax.all_to_all(array, axis, split_axis=0, concat_axis=0, tiled=True)]
    another operation x4 -> x1, other arithmetic: 18.5 us -> 0.08 us  [shards(): place = jnp.stack([y // 4, y % 2 * 2 + core, core]).astype(jnp.int32)]
    dot_general x9 -> x0, matrix products: 17.5 us -> none  [the longest x1 8.5 us: expert_half(): jnp.einsum('sif,fd->sid', hidden, down_slice, preferred_element_type=jnp....]
  transfers between devices with their start and end apart: 4 -> 15, of which waited for: 2 -> 9; matrix products, arithmetic and copies ran while one was open for 4% -> 2% of each run, Pallas kernels for 0% -> 8%
where the time goes in v1:
time: 208 us; the launch traced here: 207 us
  waiting for transfers between devices  93.4 us (45%)
  starting transfers between devices  75.4 us (36%)
  Pallas kernels  17.2 us (8%)
  local copies, waits for them, and re-layouts  15.1 us (7%)
  other arithmetic  4.86 us (2%)
    all_to_all x8, waiting for transfers between devices, exchange(): return lax.all_to_all(array, axis, split_axis=0, concat_axis=0, tiled=True)  92.7 us
    all_to_all x8, starting transfers between devices, exchange(): return lax.all_to_all(array, axis, split_axis=0, concat_axis=0, tiled=True)  47.3 us
    ppermute x6, starting transfers between devices, swap(): return lax.ppermute(array, 'c', [(0, 1), (1, 0)])  24.1 us
    unnamed x60, local copies, waits for them, and re-layouts  13.5 us
    pallas_call x6, Pallas kernels, call(): pl.pallas_call(body, out_shape=outs, in_specs=[SMEM] + [VMEM] * len(array...  12.9 us
    pallas_call x2, Pallas kernels, with_scratch(): pl.pallas_call(body, out_shape=outs, in_specs=[SMEM] + [VMEM] * len(array...  4.37 us
  transfers between devices with their start and end apart: 15, of which 9 were waited for; matrix products, arithmetic and copies ran while one was open for 2% of the time, Pallas kernels for 8%

profile of v1, /device:TPU:1, one launch (start us, length us, event | category | flops | bytes accessed | tf_op | source)
XLA Modules:
  0.0 207.0 jit_solution(5206619075831875561)
XLA Ops:
  0.7 1.0 copy-done.6
  1.8 1.0 copy-done.7
  2.8 1.0 copy-done.8
  3.9 0.7 shard_map.180.own
  4.6 4.0 %collective-permute-start.3 = (bf16[6144,128]{1,0:T(8,128)(2,1)S(1)}, bf16[6144,128]{1,0:T(8,128)(2,1)}, u32[]{:S(2)}, u32[]{:S(2)}) collective-permute-start(bf16[6144,128]{1,0:T(8,128)(2,1)S(1)} %shard_map.180.own), channel_id=1, source_target_pairs={{0,2},{2,0},{4,6},{6,4},{8,10},{10,8},{12,14},{14,12},{1,3},{3,1},... | collective-permute-start | bytes 4718600 | tf_op jit(solution)/shard_map/ppermute | solution.py:234
  8.7 1.8 shard_map.176
  10.5 12.9 %all-to-all-start = ((f32[32,8,128]{2,1,0:T(8,128)}), f32[32,8,128]{2,1,0:T(8,128)S(1)}, u32[]{:S(2)}, u32[]{:S(2)}) async-start(f32[32,8,128]{2,1,0:T(8,128)} %shard_map.176), calls=%async_computation | async-start | bytes 262144 | tf_op jit(solution)/shard_map/all_to_all | solution.py:226
  23.4 1.6 shard_map.179
  25.1 1.0 copy-done.1
  26.1 1.0 copy-done.4
  28.3 4.5 %all-to-all-done.states = f32[32,8,128]{2,1,0:T(8,128)S(1)} async-done(((f32[32,8,128]{2,1,0:T(8,128)}), f32[32,8,128]{2,1,0:T(8,128)S(1)}, u32[]{:S(2)}, u32[]{:S(2)}) %all-to-all-start) | async-done | bytes 131104 | tf_op jit(solution)/shard_map/all_to_all | solution.py:226
  32.8 4.7 %all-to-all-start.4 = ((bf16[32,8,2048]{2,1,0:T(8,128)(2,1)}), bf16[32,8,2048]{2,1,0:T(8,128)(2,1)S(1)}, u32[]{:S(2)}, u32[]{:S(2)}) async-start(bf16[32,8,2048]{2,1,0:T(8,128)(2,1)} %bitcast.31), calls=%async_computation.4 | async-start | bytes 2097152 | tf_op jit(solution)/shard_map/all_to_all | solution.py:226
  37.6 3.7 %collective-permute-start.2 = (bf16[6144,128]{1,0:T(8,128)(2,1)S(1)}, bf16[6144,128]{1,0:T(8,128)(2,1)}, u32[]{:S(2)}, u32[]{:S(2)}) collective-permute-start(bf16[6144,128]{1,0:T(8,128)(2,1)S(1)} %shard_map.180.own), channel_id=1, source_target_pairs={{0,1},{1,0},{2,3},{3,2},{4,5},{5,4},{6,7},{7,6},{8,9},{9,8},{10,11... | collective-permute-start | bytes 4718600 | tf_op jit(solution)/shard_map/ppermute | solution.py:230
  41.3 4.7 %collective-permute-start.4 = (bf16[6144,128]{1,0:T(8,128)(2,1)}, bf16[6144,128]{1,0:T(8,128)(2,1)}, u32[]{:S(2)}, u32[]{:S(2)}) collective-permute-start(bf16[6144,128]{1,0:T(8,128)(2,1)} %collective-permute-done.3.near), channel_id=1, source_target_pairs={{0,1},{1,0},{2,3},{3,2},{4,5},{5,4},{6,7},{7,6},{8,9},{9,8},{10,11... | collective-permute-start | bytes 4718600 | tf_op jit(solution)/shard_map/ppermute | solution.py:230
  46.0 1.8 shard_map.177
  47.8 15.5 %all-to-all-done.4 = bf16[32,8,2048]{2,1,0:T(8,128)(2,1)S(1)} async-done(((bf16[32,8,2048]{2,1,0:T(8,128)(2,1)}), bf16[32,8,2048]{2,1,0:T(8,128)(2,1)S(1)}, u32[]{:S(2)}, u32[]{:S(2)}) %all-to-all-start.4) | async-done | bytes 1048608 | tf_op jit(solution)/shard_map/all_to_all | solution.py:226
  63.3 6.6 %all-to-all-start.1 = ((f32[32,8,128]{2,1,0:T(8,128)}), f32[32,8,128]{2,1,0:T(8,128)S(1)}, u32[]{:S(2)}, u32[]{:S(2)}) async-start(f32[32,8,128]{2,1,0:T(8,128)} %shard_map.177), calls=%async_computation.1 | async-start | bytes 262144 | tf_op jit(solution)/shard_map/all_to_all | solution.py:226
  69.9 5.8 %shard_map.181 = bf16[256,2048]{1,0:T(8,128)(2,1)S(1)} custom-call(s32[3]{0:T(128)S(1)} %pad_add_fusion.place, bf16[256,2048]{1,0:T(8,128)(2,1)S(1)} %bitcast.28, bf16[6144,128]{1,0:T(8,128)(2,1)S(1)} %shard_map.180.own, bf16[6144,128]{1,0:T(8,128)(2,1)} %collective-permute-done.2.core, bf16[6144,128]{1,0:T(8,128)(2,1)} %collective-permute-done.3.near, ...), custom_call_target="tpu_custom_call" | custom-call | flops 2147483648 | bytes 1048576 | tf_op jit(solution)/shard_map/pallas_call | solution.py:34
  75.8 1.0 copy-done
  76.7 2.6 %all-to-all-done.1.states = f32[32,8,128]{2,1,0:T(8,128)S(1)} async-done(((f32[32,8,128]{2,1,0:T(8,128)}), f32[32,8,128]{2,1,0:T(8,128)S(1)}, u32[]{:S(2)}, u32[]{:S(2)}) %all-to-all-start.1) | async-done | bytes 131104 | tf_op jit(solution)/shard_map/all_to_all | solution.py:226
  79.4 6.7 %all-to-all-start.5 = ((bf16[32,8,2048]{2,1,0:T(8,128)(2,1)}), bf16[32,8,2048]{2,1,0:T(8,128)(2,1)S(1)}, u32[]{:S(2)}, u32[]{:S(2)}) async-start(bf16[32,8,2048]{2,1,0:T(8,128)(2,1)} %bitcast.29), calls=%async_computation.5 | async-start | bytes 2097152 | tf_op jit(solution)/shard_map/all_to_all | solution.py:226
  86.8 0.7 copy-done.22
  87.5 0.7 copy-done.27
  88.9 2.7 %shard_map.178 = (f32[64,2048]{1,0:T(8,128)S(1)}, bf16[64,2048]{1,0:T(8,128)(2,1)}) custom-call(s32[3]{0:T(128)S(1)} %copy-done.20, f32[32,8,128]{2,1,0:T(8,128)S(1)} %all-to-all-done.1.states, bf16[128,512]{1,0:T(8,128)(2,1)S(1)} %copy-done.12, bf16[128,512]{1,0:T(8,128)(2,1)S(1)} %copy-done.5, bf16[64,128]{1,0:T(8,128)(2,1)S(1)} %bitcast.38, ...), custom_call_target="tpu_custom_call" | custom-call | flops 67108864 | bytes 1048576 | tf_op jit(solution)/shard_map/pallas_call | solution.py:238
  91.6 4.7 %collective-permute-start = (bf16[64,2048]{1,0:T(8,128)(2,1)}, bf16[64,2048]{1,0:T(8,128)(2,1)}, u32[]{:S(2)}, u32[]{:S(2)}) collective-permute-start(bf16[64,2048]{1,0:T(8,128)(2,1)} %get-tuple-element.11), channel_id=1, source_target_pairs={{0,1},{1,0},{2,3},{3,2},{4,5},{5,4},{6,7},{7,6},{8,9},{9,8},{10,11... | collective-permute-start | bytes 786440 | tf_op jit(solution)/shard_map/ppermute | solution.py:230
  96.3 1.2 shard_map.182.act
  97.6 13.4 %all-to-all-done.5 = bf16[32,8,2048]{2,1,0:T(8,128)(2,1)S(1)} async-done(((bf16[32,8,2048]{2,1,0:T(8,128)(2,1)}), bf16[32,8,2048]{2,1,0:T(8,128)(2,1)S(1)}, u32[]{:S(2)}, u32[]{:S(2)}) %all-to-all-start.5) | async-done | bytes 1048608 | tf_op jit(solution)/shard_map/all_to_all | solution.py:226
  111.0 0.9 copy-done.13
  111.9 0.9 copy-done.15
  112.8 0.9 copy-done.17
  114.4 1.7 shard_map.183
  116.0 6.0 %collective-permute-start.5 = (bf16[128,2048]{1,0:T(8,128)(2,1)S(1)}, bf16[128,2048]{1,0:T(8,128)(2,1)S(1)}, u32[]{:S(2)}, u32[]{:S(2)}) collective-permute-start(bf16[128,2048]{1,0:T(8,128)(2,1)S(1)} %get-tuple-element.17), channel_id=1, source_target_pairs={{0,1},{1,0},{2,3},{3,2},{4,5},{5,4},{6,7},{7,6},{8,9},{9,8},{10,11... | collective-permute-start | bytes 1572872 | tf_op jit(solution)/shard_map/ppermute | solution.py:230
  122.1 1.7 fusion
  123.8 5.9 %all-to-all-start.2 = ((bf16[8,8,2048]{2,1,0:T(8,128)(2,1)}), bf16[8,8,2048]{2,1,0:T(8,128)(2,1)S(1)}, u32[]{:S(2)}, u32[]{:S(2)}) async-start(bf16[8,8,2048]{2,1,0:T(8,128)(2,1)} %fusion), calls=%async_computation.2 | async-start | bytes 524288 | tf_op jit(solution)/shard_map/all_to_all | solution.py:226
  129.7 0.9 add_convert_fusion
  130.6 11.5 %all-to-all-done.2 = bf16[8,8,2048]{2,1,0:T(8,128)(2,1)S(1)} async-done(((bf16[8,8,2048]{2,1,0:T(8,128)(2,1)}), bf16[8,8,2048]{2,1,0:T(8,128)(2,1)S(1)}, u32[]{:S(2)}, u32[]{:S(2)}) %all-to-all-start.2) | async-done | bytes 262176 | tf_op jit(solution)/shard_map/all_to_all | solution.py:226
  142.1 3.5 %all-to-all-start.6 = ((bf16[8,16,2048]{2,1,0:T(8,128)(2,1)}), bf16[8,16,2048]{2,1,0:T(8,128)(2,1)S(1)}, u32[]{:S(2)}, u32[]{:S(2)}) async-start(bf16[8,16,2048]{2,1,0:T(8,128)(2,1)} %bitcast.21), calls=%async_computation.6 | async-start | bytes 1048576 | tf_op jit(solution)/shard_map/all_to_all | solution.py:226
  145.6 17.8 %all-to-all-done.6 = bf16[8,16,2048]{2,1,0:T(8,128)(2,1)S(1)} async-done(((bf16[8,16,2048]{2,1,0:T(8,128)(2,1)}), bf16[8,16,2048]{2,1,0:T(8,128)(2,1)S(1)}, u32[]{:S(2)}, u32[]{:S(2)}) %all-to-all-start.6) | async-done | bytes 524320 | tf_op jit(solution)/shard_map/all_to_all | solution.py:226
  163.4 0.7 broadcast_in_dim.6
  164.2 3.4 %all-to-all-start.3 = ((bf16[8,8,2048]{2,1,0:T(8,128)(2,1)}), bf16[8,8,2048]{2,1,0:T(8,128)(2,1)S(1)}, u32[]{:S(2)}, u32[]{:S(2)}) async-start(bf16[8,8,2048]{2,1,0:T(8,128)(2,1)} %broadcast_in_dim.6), calls=%async_computation.3 | async-start | bytes 524288 | tf_op jit(solution)/shard_map/all_to_all | solution.py:226
  167.7 12.0 %all-to-all-done.3 = bf16[8,8,2048]{2,1,0:T(8,128)(2,1)S(1)} async-done(((bf16[8,8,2048]{2,1,0:T(8,128)(2,1)}), bf16[8,8,2048]{2,1,0:T(8,128)(2,1)S(1)}, u32[]{:S(2)}, u32[]{:S(2)}) %all-to-all-start.3) | async-done | bytes 262176 | tf_op jit(solution)/shard_map/all_to_all | solution.py:226
  179.7 0.8 broadcast_in_dim.8
  180.6 3.5 %all-to-all-start.7 = ((bf16[8,16,2048]{2,1,0:T(8,128)(2,1)}), bf16[8,16,2048]{2,1,0:T(8,128)(2,1)S(1)}, u32[]{:S(2)}, u32[]{:S(2)}) async-start(bf16[8,16,2048]{2,1,0:T(8,128)(2,1)} %broadcast_in_dim.8), calls=%async_computation.7 | async-start | bytes 1048576 | tf_op jit(solution)/shard_map/all_to_all | solution.py:226
  184.1 2.5 %collective-permute-start.1 = (bf16[64,2048]{1,0:T(8,128)(2,1)S(1)}, bf16[64,2048]{1,0:T(8,128)(2,1)S(1)}, u32[]{:S(2)}, u32[]{:S(2)}) collective-permute-start(bf16[64,2048]{1,0:T(8,128)(2,1)S(1)} %bitcast.48), channel_id=1, source_target_pairs={{0,1},{1,0},{2,3},{3,2},{4,5},{5,4},{6,7},{7,6},{8,9},{9,8},{10,11... | collective-permute-start | bytes 786440 | tf_op jit(solution)/shard_map/ppermute | solution.py:230
  186.6 15.3 %all-to-all-done.7 = bf16[8,16,2048]{2,1,0:T(8,128)(2,1)S(1)} async-done(((bf16[8,16,2048]{2,1,0:T(8,128)(2,1)}), bf16[8,16,2048]{2,1,0:T(8,128)(2,1)S(1)}, u32[]{:S(2)}, u32[]{:S(2)}) %all-to-all-start.7) | async-done | bytes 524320 | tf_op jit(solution)/shard_map/all_to_all | solution.py:226
  201.9 2.4 %collective-permute-start.6 = (bf16[128,2048]{1,0:T(8,128)(2,1)S(1)}, bf16[128,2048]{1,0:T(8,128)(2,1)S(1)}, u32[]{:S(2)}, u32[]{:S(2)}) collective-permute-start(bf16[128,2048]{1,0:T(8,128)(2,1)S(1)} %bitcast.47), channel_id=1, source_target_pairs={{0,1},{1,0},{2,3},{3,2},{4,5},{5,4},{6,7},{7,6},{8,9},{9,8},{10,11... | collective-permute-start | bytes 1572872 | tf_op jit(solution)/shard_map/ppermute | solution.py:230
  204.4 0.8 pad_maximum_fusion.1
  205.9 1.1 pad_maximum_fusion
  (61 shorter events, 4.4 us)
Async XLA Ops:
  0.7 69.2 %copy-start.19 = (s32[3]{0:T(128)}, s32[3]{0:T(128)S(1)}, u32[]{:S(2)}) copy-start(s32[3]{0:T(128)S(1)} %pad_add_fusion.place) | copy-start | bytes 40
  0.7 1.0 copy-start.6
  1.8 1.0 copy-start.7
  2.8 1.0 copy-start.8
  3.9 4.8 %copy-start.5 = (bf16[128,512]{1,0:T(8,128)(2,1)S(1)}, bf16[128,512]{1,0:T(8,128)(2,1)}, u32[]{:S(2)}) copy-start(bf16[128,512]{1,0:T(8,128)(2,1)} %keys.3) | copy-start | bytes 393220
  3.9 4.8 %copy-start.18 = (bf16[128,64]{0,1:T(8,128)(2,1)S(1)}, bf16[128,64]{0,1:T(8,128)(2,1)}, u32[]{:S(2)}) copy-start(bf16[128,64]{0,1:T(8,128)(2,1)} %param.19) | copy-start | bytes 49156
  3.9 4.8 %copy-start.26 = (f32[128,2]{0,1:T(2,128)S(1)}, f32[128,2]{0,1:T(2,128)}, u32[]{:S(2)}) copy-start(f32[128,2]{0,1:T(2,128)} %param.21) | copy-start | bytes 3076
  3.9 4.8 %copy-start.28 = (f32[128,2]{0,1:T(2,128)S(1)}, f32[128,2]{0,1:T(2,128)}, u32[]{:S(2)}) copy-start(f32[128,2]{0,1:T(2,128)} %param.22) | copy-start | bytes 3076
  3.9 19.5 %copy-start.3 = (bf16[256,2048]{1,0:T(8,128)(2,1)S(1)}, bf16[256,2048]{1,0:T(8,128)(2,1)}, u32[]{:S(2)}) copy-start(bf16[256,2048]{1,0:T(8,128)(2,1)} %x.1) | copy-start | bytes 3145732
  3.9 19.5 %copy-start.23 = (f32[2048]{0:T(1024)S(1)}, f32[2048]{0:T(1024)}, u32[]{:S(2)}) copy-start(f32[2048]{0:T(1024)} %param.25) | copy-start | bytes 24580
  3.9 19.5 %copy-start.24 = (s32[256,4]{0,1:T(4,128)S(1)}, s32[256,4]{0,1:T(4,128)}, u32[]{:S(2)}) copy-start(s32[256,4]{0,1:T(4,128)} %param.26) | copy-start | bytes 12292
  3.9 19.5 %copy-start.25 = (f32[256,4]{0,1:T(4,128)S(1)}, f32[256,4]{0,1:T(4,128)}, u32[]{:S(2)}) copy-start(f32[256,4]{0,1:T(4,128)} %param.27) | copy-start | bytes 12292
  4.6 36.6 %collective-permute-start.3 = (bf16[6144,128]{1,0:T(8,128)(2,1)S(1)}, bf16[6144,128]{1,0:T(8,128)(2,1)}, u32[]{:S(2)}, u32[]{:S(2)}) collective-permute-start(bf16[6144,128]{1,0:T(8,128)(2,1)S(1)} %shard_map.180.own), channel_id=1, source_target_pairs={{0,2},{2,0},{4,6},{6,4},{8,10},{10,8},{12,14},{14,12},{1,3},{3,1},... | collective-permute-start | bytes 4718600 | tf_op jit(solution)/shard_map/ppermute | solution.py:234
  10.5 22.3 %all-to-all-start = ((f32[32,8,128]{2,1,0:T(8,128)}), f32[32,8,128]{2,1,0:T(8,128)S(1)}, u32[]{:S(2)}, u32[]{:S(2)}) async-start(f32[32,8,128]{2,1,0:T(8,128)} %shard_map.176), calls=%async_computation | async-start | bytes 262144 | tf_op jit(solution)/shard_map/all_to_all | solution.py:226
  25.0 1.0 copy-start.1
  26.0 1.0 copy-start.4
  27.0 0.7 copy-start.14
  27.7 0.7 copy-start.16
  32.8 30.5 %all-to-all-start.4 = ((bf16[32,8,2048]{2,1,0:T(8,128)(2,1)}), bf16[32,8,2048]{2,1,0:T(8,128)(2,1)S(1)}, u32[]{:S(2)}, u32[]{:S(2)}) async-start(bf16[32,8,2048]{2,1,0:T(8,128)(2,1)} %bitcast.31), calls=%async_computation.4 | async-start | bytes 2097152 | tf_op jit(solution)/shard_map/all_to_all | solution.py:226
  37.6 32.4 %collective-permute-start.2 = (bf16[6144,128]{1,0:T(8,128)(2,1)S(1)}, bf16[6144,128]{1,0:T(8,128)(2,1)}, u32[]{:S(2)}, u32[]{:S(2)}) collective-permute-start(bf16[6144,128]{1,0:T(8,128)(2,1)S(1)} %shard_map.180.own), channel_id=1, source_target_pairs={{0,1},{1,0},{2,3},{3,2},{4,5},{5,4},{6,7},{7,6},{8,9},{9,8},{10,11... | collective-permute-start | bytes 4718600 | tf_op jit(solution)/shard_map/ppermute | solution.py:230
  41.3 28.6 %collective-permute-start.4 = (bf16[6144,128]{1,0:T(8,128)(2,1)}, bf16[6144,128]{1,0:T(8,128)(2,1)}, u32[]{:S(2)}, u32[]{:S(2)}) collective-permute-start(bf16[6144,128]{1,0:T(8,128)(2,1)} %collective-permute-done.3.near), channel_id=1, source_target_pairs={{0,1},{1,0},{2,3},{3,2},{4,5},{5,4},{6,7},{7,6},{8,9},{9,8},{10,11... | collective-permute-start | bytes 4718600 | tf_op jit(solution)/shard_map/ppermute | solution.py:230
  63.3 16.1 %all-to-all-start.1 = ((f32[32,8,128]{2,1,0:T(8,128)}), f32[32,8,128]{2,1,0:T(8,128)S(1)}, u32[]{:S(2)}, u32[]{:S(2)}) async-start(f32[32,8,128]{2,1,0:T(8,128)} %shard_map.177), calls=%async_computation.1 | async-start | bytes 262144 | tf_op jit(solution)/shard_map/all_to_all | solution.py:226
  75.7 1.0 copy-start
  76.7 9.4 %copy-start.9 = (bf16[64,2048]{1,0:T(8,128)(2,1)S(1)}, bf16[64,2048]{1,0:T(8,128)(2,1)}, u32[]{:S(2)}) copy-start(bf16[64,2048]{1,0:T(8,128)(2,1)} %mix.1) | copy-start | bytes 786436
  76.7 9.4 %copy-start.12 = (bf16[128,512]{1,0:T(8,128)(2,1)S(1)}, bf16[128,512]{1,0:T(8,128)(2,1)}, u32[]{:S(2)}) copy-start(bf16[128,512]{1,0:T(8,128)(2,1)} %queries.1) | copy-start | bytes 393220
  76.7 19.6 %copy-start.2 = (bf16[256,2048]{1,0:T(8,128)(2,1)S(1)}, bf16[256,2048]{1,0:T(8,128)(2,1)}, u32[]{:S(2)}) copy-start(bf16[256,2048]{1,0:T(8,128)(2,1)} %copy-done.1) | copy-start | bytes 3145732
  76.7 19.6 %copy-start.10 = (bf16[2048,32]{0,1:T(8,128)(2,1)S(1)}, bf16[2048,32]{0,1:T(8,128)(2,1)}, u32[]{:S(2)}) copy-start(bf16[2048,32]{0,1:T(8,128)(2,1)} %param.31) | copy-start | bytes 393220
  76.7 19.6 %copy-start.11 = (bf16[2048,32]{0,1:T(8,128)(2,1)S(1)}, bf16[2048,32]{0,1:T(8,128)(2,1)}, u32[]{:S(2)}) copy-start(bf16[2048,32]{0,1:T(8,128)(2,1)} %param.32) | copy-start | bytes 393220
  79.4 31.6 %all-to-all-start.5 = ((bf16[32,8,2048]{2,1,0:T(8,128)(2,1)}), bf16[32,8,2048]{2,1,0:T(8,128)(2,1)S(1)}, u32[]{:S(2)}, u32[]{:S(2)}) async-start(bf16[32,8,2048]{2,1,0:T(8,128)(2,1)} %bitcast.29), calls=%async_computation.5 | async-start | bytes 2097152 | tf_op jit(solution)/shard_map/all_to_all | solution.py:226
  86.1 0.7 copy-start.20
  86.8 0.7 copy-start.22
  87.5 0.7 copy-start.27
  88.2 0.7 copy-start.29
  91.6 30.5 %collective-permute-start = (bf16[64,2048]{1,0:T(8,128)(2,1)}, bf16[64,2048]{1,0:T(8,128)(2,1)}, u32[]{:S(2)}, u32[]{:S(2)}) collective-permute-start(bf16[64,2048]{1,0:T(8,128)(2,1)} %get-tuple-element.11), channel_id=1, source_target_pairs={{0,1},{1,0},{2,3},{3,2},{4,5},{5,4},{6,7},{7,6},{8,9},{9,8},{10,11... | collective-permute-start | bytes 786440 | tf_op jit(solution)/shard_map/ppermute | solution.py:230
  111.0 0.9 copy-start.13
  111.9 0.9 copy-start.15
  112.8 0.9 copy-start.17
  113.7 0.7 copy-start.21
  116.0 13.7 %collective-permute-start.5 = (bf16[128,2048]{1,0:T(8,128)(2,1)S(1)}, bf16[128,2048]{1,0:T(8,128)(2,1)S(1)}, u32[]{:S(2)}, u32[]{:S(2)}) collective-permute-start(bf16[128,2048]{1,0:T(8,128)(2,1)S(1)} %get-tuple-element.17), channel_id=1, source_target_pairs={{0,1},{1,0},{2,3},{3,2},{4,5},{5,4},{6,7},{7,6},{8,9},{9,8},{10,11... | collective-permute-start | bytes 1572872 | tf_op jit(solution)/shard_map/ppermute | solution.py:230
  123.8 18.3 %all-to-all-start.2 = ((bf16[8,8,2048]{2,1,0:T(8,128)(2,1)}), bf16[8,8,2048]{2,1,0:T(8,128)(2,1)S(1)}, u32[]{:S(2)}, u32[]{:S(2)}) async-start(bf16[8,8,2048]{2,1,0:T(8,128)(2,1)} %fusion), calls=%async_computation.2 | async-start | bytes 524288 | tf_op jit(solution)/shard_map/all_to_all | solution.py:226
  142.1 21.4 %all-to-all-start.6 = ((bf16[8,16,2048]{2,1,0:T(8,128)(2,1)}), bf16[8,16,2048]{2,1,0:T(8,128)(2,1)S(1)}, u32[]{:S(2)}, u32[]{:S(2)}) async-start(bf16[8,16,2048]{2,1,0:T(8,128)(2,1)} %bitcast.21), calls=%async_computation.6 | async-start | bytes 1048576 | tf_op jit(solution)/shard_map/all_to_all | solution.py:226
  164.2 15.5 %all-to-all-start.3 = ((bf16[8,8,2048]{2,1,0:T(8,128)(2,1)}), bf16[8,8,2048]{2,1,0:T(8,128)(2,1)S(1)}, u32[]{:S(2)}, u32[]{:S(2)}) async-start(bf16[8,8,2048]{2,1,0:T(8,128)(2,1)} %broadcast_in_dim.6), calls=%async_computation.3 | async-start | bytes 524288 | tf_op jit(solution)/shard_map/all_to_all | solution.py:226
  180.6 21.4 %all-to-all-start.7 = ((bf16[8,16,2048]{2,1,0:T(8,128)(2,1)}), bf16[8,16,2048]{2,1,0:T(8,128)(2,1)S(1)}, u32[]{:S(2)}, u32[]{:S(2)}) async-start(bf16[8,16,2048]{2,1,0:T(8,128)(2,1)} %broadcast_in_dim.8), calls=%async_computation.7 | async-start | bytes 1048576 | tf_op jit(solution)/shard_map/all_to_all | solution.py:226
  184.1 20.3 %collective-permute-start.1 = (bf16[64,2048]{1,0:T(8,128)(2,1)S(1)}, bf16[64,2048]{1,0:T(8,128)(2,1)S(1)}, u32[]{:S(2)}, u32[]{:S(2)}) collective-permute-start(bf16[64,2048]{1,0:T(8,128)(2,1)S(1)} %bitcast.48), channel_id=1, source_target_pairs={{0,1},{1,0},{2,3},{3,2},{4,5},{5,4},{6,7},{7,6},{8,9},{9,8},{10,11... | collective-permute-start | bytes 786440 | tf_op jit(solution)/shard_map/ppermute | solution.py:230
  201.9 3.9 %collective-permute-start.6 = (bf16[128,2048]{1,0:T(8,128)(2,1)S(1)}, bf16[128,2048]{1,0:T(8,128)(2,1)S(1)}, u32[]{:S(2)}, u32[]{:S(2)}) collective-permute-start(bf16[128,2048]{1,0:T(8,128)(2,1)S(1)} %bitcast.47), channel_id=1, source_target_pairs={{0,1},{1,0},{2,3},{3,2},{4,5},{5,4},{6,7},{7,6},{8,9},{9,8},{10,11... | collective-permute-start | bytes 1572872 | tf_op jit(solution)/shard_map/ppermute | solution.py:230

commit v2 on v1

v2 whole, which is shorter than its diff:
```python
import jax
import jax.numpy as jnp
from jax import lax
from jax.experimental import pallas as pl
from jax.experimental.pallas import tpu as pltpu
from jax.sharding import Mesh
from jax.sharding import PartitionSpec as P

D = 2048
WIDE = D + 128
KEY_DIM = 256
BLOCK = 128
N_EP = 32
N_Y = 8
SLOTS = 8
TOKENS = 256
ROWS = N_EP * SLOTS
E_ROWS = TOKENS // 16
M_ROWS = BLOCK // 16
PIECE = E_ROWS + M_ROWS
EP = ("z", "x")
EP_TP = ("z", "x", "y", "c")
TP = ("y", "c")
bf16 = jnp.bfloat16
f32 = jnp.float32
epsilon = 1e-06
lowest = -1e30
den_floor = 4.0
HIGHEST = lax.Precision.HIGHEST

VMEM = pl.BlockSpec(memory_space=pltpu.VMEM)
HBM = pl.BlockSpec(memory_space=pltpu.HBM)
NT = (((1,), (1,)), ((), ()))
TN = (((0,), (0,)), ((), ()))


def call(body, arrays, ins, outs, spaces, scratch, flops, limit=16):
    return pl.pallas_call(
        body,
        out_shape=outs,
        in_specs=ins,
        out_specs=spaces,
        scratch_shapes=scratch,
        compiler_params=pltpu.CompilerParams(vmem_limit_bytes=limit << 20),
        cost_estimate=pl.CostEstimate(flops=flops, bytes_accessed=1 << 20, transcendentals=0),
    )(*arrays)


def shape(dims, dtype):
    return jax.ShapeDtypeStruct(dims, dtype)


def iota(dims, dim):
    return lax.broadcasted_iota(jnp.int32, dims, dim)


def split_scalar(value):
    high = value.astype(bf16).astype(f32)
    middle = (value - high).astype(bf16).astype(f32)
    lane = iota((N_EP, 128), 1)
    return jnp.where(
        lane == 0,
        high,
        jnp.where(lane == 1, middle, jnp.where(lane == 2, value - high - middle, 0.0)),
    )


def gates(team, input_gate, forget_gate):
    first = team == 0
    given = jnp.where(first, input_gate[0:1, :], input_gate[1:2, :])
    forget = jnp.where(first, forget_gate[0:1, :], forget_gate[1:2, :])
    small = jnp.exp(-jnp.abs(forget))
    tail = jnp.where(small < 1e-4, small - 0.5 * small * small, jnp.log(1.0 + small))
    log_forget = jnp.minimum(forget, 0.0) - tail
    upto = jnp.where(iota((BLOCK, BLOCK), 0) <= iota((BLOCK, BLOCK), 1), 1.0, 0.0)
    cumulative = jnp.dot(
        jnp.broadcast_to(log_forget, (8, BLOCK)), upto, preferred_element_type=f32, precision=HIGHEST
    )[0:1, :]
    return given, cumulative


def pack_kernel(gate, up, down, packed, sem):
    copies = [
        pltpu.make_async_copy(gate, packed.at[0:D, :], sem.at[0]),
        pltpu.make_async_copy(up, packed.at[D : 2 * D, :], sem.at[1]),
    ]
    for k in range(16):
        copies.append(
            pltpu.make_async_copy(
                down.at[:, 128 * k : 128 * (k + 1)],
                packed.at[2 * D + 128 * k : 2 * D + 128 * (k + 1), :],
                sem.at[2 + k],
            )
        )
    for copy in copies:
        copy.start()
    for copy in copies:
        copy.wait()


def normalize(x, gain):
    rows = x[...].astype(f32)
    scale = lax.rsqrt(jnp.mean(rows * rows, axis=-1, keepdims=True) + epsilon)
    return (rows * scale * gain[...]).astype(bf16)


def route_kernel(
    x, gain, ids, weights, keys, values, input_gate, forget_gate,
    send, w_high, w_low, staged, states, sem,
):
    y, core = lax.axis_index("y"), lax.axis_index("c")
    team, part = y // 4, lax.rem(y, 2) * 2 + core
    normal = normalize(x, gain)
    expert = iota((N_EP, TOKENS), 0) * 2 + team
    named = jnp.zeros((N_EP, TOKENS), f32)
    weight = jnp.zeros((N_EP, TOKENS), f32)
    for k in range(4):
        hit = ids[k : k + 1, :] == expert
        named = named + jnp.where(hit, 1.0, 0.0)
        weight = weight + jnp.where(hit, weights[k : k + 1, :], 0.0)
    before = jnp.where(iota((TOKENS, TOKENS), 0) < iota((TOKENS, TOKENS), 1), 1.0, 0.0).astype(bf16)
    rank = jnp.dot(named.astype(bf16), before, preferred_element_type=f32)
    rank = jnp.where(named > 0.0, rank, -1.0)
    spread = jnp.where(iota((ROWS, N_EP), 0) // SLOTS == iota((ROWS, N_EP), 1), 1.0, 0.0)
    rank = jnp.dot(spread.astype(bf16), rank.astype(bf16), preferred_element_type=f32)
    weight = jnp.dot(spread, weight, preferred_element_type=f32, precision=HIGHEST)
    slot = (lax.rem(iota((ROWS, TOKENS), 0), SLOTS) + part * SLOTS).astype(f32)
    chosen = rank == slot
    pick = jnp.where(chosen, 1.0, 0.0).astype(bf16)
    copies = []
    for k in range(4):
        at = slice(512 * k, 512 * (k + 1))
        staged[:, at] = jnp.dot(pick, normal[:, at], preferred_element_type=f32).astype(bf16)
        copies.append(pltpu.make_async_copy(staged.at[:, at], send.at[:, at], sem.at[k]))
        copies[-1].start()
    weight = jnp.where(chosen, weight, 0.0)
    high = weight.astype(bf16)
    w_high[...] = high
    w_low[...] = (weight - high.astype(f32)).astype(bf16)

    given, cumulative = gates(team, input_gate, forget_gate)
    block_total = cumulative[:, BLOCK - 1 : BLOCK]
    log_keep = block_total - cumulative + given
    running = jnp.max(log_keep, axis=1, keepdims=True)
    kept = jnp.exp(log_keep - running)
    key = keys[:, pl.ds(pl.multiple_of(team * KEY_DIM, KEY_DIM), KEY_DIM)].astype(f32)
    memory = jnp.dot(
        values[...].astype(f32) * kept, key, preferred_element_type=f32, precision=HIGHEST
    )
    normalizer = jnp.dot(
        jnp.broadcast_to(kept, (8, BLOCK)), key, preferred_element_type=f32, precision=HIGHEST
    )
    states[:, 0, :] = memory[0:32, 0:128]
    states[:, 1, :] = memory[0:32, 128:256]
    states[:, 2, :] = memory[32:64, 0:128]
    states[:, 3, :] = memory[32:64, 128:256]
    states[:, 4, :] = jnp.broadcast_to(normalizer[0:1, 0:128], (N_EP, 128))
    states[:, 5, :] = jnp.broadcast_to(normalizer[0:1, 128:256], (N_EP, 128))
    states[:, 6, :] = split_scalar(block_total)
    states[:, 7, :] = split_scalar(running)
    staged[:, D:WIDE] = states[...].reshape(ROWS, 128).astype(bf16)
    copies.append(pltpu.make_async_copy(staged.at[:, D:WIDE], send.at[:, D:WIDE], sem.at[4]))
    copies[-1].start()
    for copy in copies:
        copy.wait()


def as_row(column):
    return jnp.broadcast_to(
        jnp.broadcast_to(column, (N_EP, 128))[None], (4, N_EP, 128)
    ).reshape(128, 128).T[0:N_EP, 0:N_EP]


def prefix(states):
    totals = as_row(jnp.sum(states[:, 6, :], axis=1, keepdims=True))
    peaks = as_row(jnp.sum(states[:, 7, :], axis=1, keepdims=True))
    row, column = iota((N_EP, N_EP), 0), iota((N_EP, N_EP), 1)
    earlier = column < row
    passed = jnp.where(earlier, totals, 0.0)
    later = jnp.where(row > column, 1.0, 0.0)
    between = jnp.dot(passed, later, preferred_element_type=f32, precision=HIGHEST)
    reach = jnp.where(earlier, peaks + between, lowest)
    running = jnp.maximum(
        jnp.sum(passed, axis=1, keepdims=True), jnp.max(reach, axis=1, keepdims=True)
    )
    share = jnp.where(earlier, jnp.exp(reach - running), 0.0)
    for k in range(6):
        states[:, k, :] = jnp.dot(
            share, states[:, k, :], preferred_element_type=f32, precision=HIGHEST
        )
    states[:, 6, :] = split_scalar(running)
    states[:, 7, :] = jnp.zeros((N_EP, 128), f32)


def expert_kernel(x, own, beside, near, far, out, staged, states, taken, sem, fetch):
    fetches = [
        pltpu.make_async_copy(pack, taken.at[k], fetch.at[k])
        for k, pack in enumerate((beside, near, far))
    ]
    for copy in fetches:
        copy.start()
    states[...] = x[:, D:WIDE].astype(f32).reshape(N_EP, 8, 128)
    prefix(states)
    staged[:, D:WIDE] = states[...].reshape(ROWS, 128).astype(bf16)
    copies = [pltpu.make_async_copy(staged.at[:, D:WIDE], out.at[:, D:WIDE], sem.at[0])]
    copies[0].start()
    rows = x[:, 0:D]
    packs = (own, taken.at[0], taken.at[1], taken.at[2])
    acts = []
    for k, pack in enumerate(packs):
        if k > 0:
            fetches[k - 1].wait()
        both = jnp.dot(
            rows,
            jnp.concatenate([pack[0:D, :], pack[D : 2 * D, :]], axis=1),
            preferred_element_type=f32,
        )
        gate, up = both[:, 0:128], both[:, 128:256]
        acts.append((gate / (1.0 + jnp.exp(-gate)) * up).astype(bf16))
    act = jnp.concatenate(acts, axis=1)
    for k in range(8):
        low = 2 * D + 256 * k
        down = jnp.concatenate(
            [
                jnp.concatenate(
                    [pack[low : low + 128, :], pack[low + 128 : low + 256, :]], axis=1
                )
                for pack in packs
            ],
            axis=0,
        )
        at = slice(256 * k, 256 * (k + 1))
        staged[:, at] = jnp.dot(act, down, preferred_element_type=f32).astype(bf16)
        copies.append(pltpu.make_async_copy(staged.at[:, at], out.at[:, at], sem.at[k + 1]))
        copies[-1].start()
    for copy in copies:
        copy.wait()


def shared_kernel(x, gain, gate, up, act):
    rows = normalize(x, gain)
    gated = lax.dot_general(rows, gate[...], NT, preferred_element_type=f32)
    lifted = lax.dot_general(rows, up[...], NT, preferred_element_type=f32)
    act[...] = (gated / (1.0 + jnp.exp(-gated)) * lifted).astype(bf16)


def combine_kernel(
    back, w_high, w_low, act, down, queries, keys, values, out_gate, input_gate, forget_gate, mix,
    keep, give, states, mixed, total,
):
    core = lax.axis_index("c")
    team = lax.axis_index("y") // 4
    states[...] = back[:, D:WIDE].astype(f32).reshape(N_EP, 8, 128)
    given, cumulative = gates(team, input_gate, forget_gate)
    at = pl.ds(pl.multiple_of(team * KEY_DIM, KEY_DIM), KEY_DIM)
    query, key = queries[:, at], keys[:, at]
    factor = KEY_DIM ** (-0.5)
    carried = cumulative + jnp.sum(states[0, 6:7, :], axis=1, keepdims=True)
    source = jnp.broadcast_to(given - cumulative, (BLOCK, BLOCK)).T
    allowed = iota((BLOCK, BLOCK), 0) <= iota((BLOCK, BLOCK), 1)
    log_weight = jnp.where(allowed, cumulative + source, lowest)
    stabilizer = jnp.maximum(carried, jnp.max(log_weight, axis=0, keepdims=True))
    within = jnp.exp(log_weight - stabilizer)
    across = jnp.exp(carried - stabilizer)
    scores = lax.dot_general(key, query, NT, preferred_element_type=f32) * factor
    weights = scores * within
    scaled = (query.astype(f32) * factor).astype(bf16)

    def read(first, second):
        return lax.dot_general(
            first.astype(bf16), scaled[:, 0:128], NT, preferred_element_type=f32
        ) + lax.dot_general(second.astype(bf16), scaled[:, 128:256], NT, preferred_element_type=f32)

    numerator = jnp.concatenate(
        [read(states[:, 0, :], states[:, 1, :]), read(states[:, 2, :], states[:, 3, :])], axis=0
    )
    numerator = across * numerator + jnp.dot(
        values[...], weights.astype(bf16), preferred_element_type=f32
    )
    normalizer = read(
        jnp.broadcast_to(states[0, 4:5, :], (16, 128)),
        jnp.broadcast_to(states[0, 5:6, :], (16, 128)),
    )
    denominator = across * normalizer[0:1, :] + jnp.sum(weights, axis=0, keepdims=True)
    hidden = numerator / jnp.maximum(jnp.abs(denominator), den_floor)
    gated = (hidden / (1.0 + jnp.exp(-out_gate[...].astype(f32)))).astype(bf16)
    mixed[...] = lax.dot_general(gated, mix[...], TN, preferred_element_type=f32)
    rows = back[:, 0:D]
    total[...] = (
        lax.dot_general(w_high[...], rows, TN, preferred_element_type=f32)
        + lax.dot_general(w_low[...], rows, TN, preferred_element_type=f32)
        + jnp.dot(act[...], down[...], preferred_element_type=f32)
    )
    for target, first in ((keep, core), (give, 1 - core)):
        for k in range(N_Y):
            start = pl.multiple_of(first * (TOKENS // 2) + k * E_ROWS, E_ROWS)
            target[k, 0:E_ROWS, :] = total[pl.ds(start, E_ROWS), :].astype(target.dtype)
            start = pl.multiple_of(first * (BLOCK // 2) + k * M_ROWS, M_ROWS)
            target[k, E_ROWS:PIECE, :] = mixed[pl.ds(start, M_ROWS), :].astype(target.dtype)


def place_kernel(mine, other, mixer, expert, sem):
    core = lax.axis_index("c")
    copies = []
    for half, (source, first) in enumerate(((mine, core), (other, 1 - core))):
        for k in range(N_Y):
            start = pl.multiple_of(first * (TOKENS // 2) + k * E_ROWS, E_ROWS)
            copies.append(
                pltpu.make_async_copy(
                    source.at[k, 0:E_ROWS, :], expert.at[pl.ds(start, E_ROWS), :], sem.at[half, k, 0]
                )
            )
            start = pl.multiple_of(first * (BLOCK // 2) + k * M_ROWS, M_ROWS)
            copies.append(
                pltpu.make_async_copy(
                    source.at[k, E_ROWS:PIECE, :], mixer.at[pl.ds(start, M_ROWS), :], sem.at[half, k, 1]
                )
            )
    for copy in copies:
        copy.start()
    for copy in copies:
        copy.wait()


def exchange(array, axis):
    return lax.all_to_all(array, axis, split_axis=0, concat_axis=0, tiled=True)


def swap(array):
    return lax.ppermute(array, "c", [(0, 1), (1, 0)])


def reach_over(array):
    return lax.ppermute(array, "y", [(k, k ^ 1) for k in range(N_Y)])


def after(array, *earlier):
    return lax.optimization_barrier((array, *earlier))[0]


def shards(
    queries,
    key_vectors,
    values,
    out_gate,
    input_gate,
    forget_gate,
    mix_weight,
    expert_input,
    norm_gain,
    route_ids,
    route_weights,
    expert_gate,
    expert_up,
    expert_down,
    shared_gate,
    shared_up,
    shared_down,
):
    dma = pltpu.SemaphoreType.DMA
    (own,) = call(
        pack_kernel,
        (expert_gate[0], expert_up[0], expert_down[0]),
        [HBM] * 3,
        [shape((3 * D, 128), bf16)],
        [VMEM],
        [dma((18,))],
        1 << 20,
    )
    near = reach_over(own)
    values_t, out_gate_t = values.T, out_gate.T
    input_t, forget_t = input_gate.T, forget_gate.T
    send, w_high, w_low = call(
        route_kernel,
        (
            expert_input,
            norm_gain[None, :],
            route_ids.T,
            route_weights.T,
            key_vectors,
            values_t,
            input_t,
            forget_t,
        ),
        [VMEM] * 8,
        [
            shape((ROWS, WIDE), bf16),
            shape((ROWS, TOKENS), bf16),
            shape((ROWS, TOKENS), bf16),
        ],
        [HBM] + [VMEM] * 2,
        [pltpu.VMEM((ROWS, WIDE), bf16), pltpu.VMEM((N_EP, 8, 128), f32), dma((5,))],
        1 << 28,
    )
    arrived = exchange(send.reshape(N_EP, SLOTS, WIDE), EP).reshape(ROWS, WIDE)
    beside = swap(after(own, w_high))
    far = swap(near)
    (act,) = call(
        shared_kernel,
        (after(expert_input, w_high), norm_gain[None, :], shared_gate.T, shared_up.T),
        [VMEM] * 4,
        [shape((TOKENS, 32), bf16)],
        [VMEM],
        [],
        1 << 26,
    )
    (results,) = call(
        expert_kernel,
        (arrived, own, beside, near, far),
        [VMEM] * 2 + [HBM] * 3,
        [shape((ROWS, WIDE), bf16)],
        [HBM],
        [
            pltpu.VMEM((ROWS, WIDE), bf16),
            pltpu.VMEM((N_EP, 8, 128), f32),
            pltpu.VMEM((3, 3 * D, 128), bf16),
            dma((9,)),
            dma((3,)),
        ],
        1 << 31,
        24,
    )
    back = exchange(results.reshape(N_EP, SLOTS, WIDE), EP).reshape(ROWS, WIDE)
    keep, give = call(
        combine_kernel,
        (
            back,
            w_high,
            w_low,
            act,
            shared_down,
            queries,
            key_vectors,
            values_t,
            out_gate_t,
            input_t,
            forget_t,
            mix_weight,
        ),
        [VMEM] * 12,
        [shape((N_Y, PIECE, D), f32), shape((N_Y, PIECE, D), bf16)],
        [VMEM] * 2,
        [
            pltpu.VMEM((N_EP, 8, 128), f32),
            pltpu.VMEM((BLOCK, D), f32),
            pltpu.VMEM((TOKENS, D), f32),
        ],
        1 << 28,
    )
    half = (keep + swap(give).astype(f32)).astype(bf16)
    piece = exchange(half, "y").astype(f32).sum(axis=0).astype(bf16)
    mine = exchange(jnp.broadcast_to(piece[None], (N_Y, PIECE, D)), "y")
    other = swap(mine)
    return call(
        place_kernel,
        (mine, other),
        [VMEM] * 2,
        [shape((BLOCK, D), bf16), shape((TOKENS, D), bf16)],
        [HBM] * 2,
        [dma((2, N_Y, 2))],
        1 << 20,
    )


def solution(mesh):
    finer = Mesh(mesh.devices.reshape(8, 4, N_Y, 2), EP_TP)
    placed = (
        P(EP, None),
        P(EP, None),
        P(EP, TP),
        P(EP, TP),
        P(EP, None),
        P(EP, None),
        P(TP, None),
        P(EP, None),
        P(),
        P(EP, None),
        P(EP, None),
        P(EP_TP, None, None),
        P(EP_TP, None, None),
        P(EP_TP, None, None),
        P(None, TP),
        P(None, TP),
        P(TP, None),
    )
    return jax.shard_map(
        shards, mesh=finer, in_specs=placed, out_specs=(P(EP, None), P(EP, None)), check_vma=False
    )
```

time: 208 us -> 169 us (0.81)
  blocking collectives: 0 us -> 52.1 us
  waiting for transfers between devices: 93.4 us -> 45.7 us
  starting transfers between devices: 75.4 us -> 47.6 us
  local copies, waits for them, and re-layouts: 15.1 us -> 7.86 us
  other arithmetic: 4.86 us -> 0.29 us
  Pallas kernels: 17.2 us -> 13.5 us
    all_to_all x8 -> x2, waiting for transfers between devices: 92.7 us -> 32.4 us  [exchange(): return lax.all_to_all(array, axis, split_axis=0, concat_axis=0, tiled=True)]
    all_to_all x0 -> x2, blocking collectives: none -> 52.1 us  [exchange(): return lax.all_to_all(array, axis, split_axis=0, concat_axis=0, tiled=True)]
    all_to_all x8 -> x2, starting transfers between devices: 47.3 us -> 22.9 us  [exchange(): return lax.all_to_all(array, axis, split_axis=0, concat_axis=0, tiled=True)]
    ppermute x1, waiting for transfers between devices: 0.01 us -> 9.52 us  [reach_over(): return lax.ppermute(array, 'y', [(k, k ^ 1) for k in range(N_Y)])]
    unnamed x60 -> x44, local copies, waits for them, and re-layouts: 13.5 us -> 7.79 us
    pallas_call x8 -> x6, Pallas kernels: 17.2 us -> 13.5 us  [call(): pl.pallas_call(body, out_shape=outs, in_specs=ins, out_specs=spaces, scra...]
    ppermute x6 -> x4, starting transfers between devices: 24.1 us -> 20.6 us  [swap(): return lax.ppermute(array, 'c', [(0, 1), (1, 0)])]
    ppermute x6 -> x4, waiting for transfers between devices: 0.63 us -> 3.79 us  [swap(): return lax.ppermute(array, 'c', [(0, 1), (1, 0)])]
  transfers between devices with their start and end apart: 15 -> 7, of which waited for: 9 -> 5; matrix products, arithmetic and copies ran while one was open for 2% -> 0% of each run, Pallas kernels for 8% -> 2%
where the time goes in v2:
time: 169 us; the launch traced here: 168 us
  blocking collectives  52.1 us (31%)
  starting transfers between devices  47.6 us (28%)
  waiting for transfers between devices  45.7 us (27%)
  Pallas kernels  13.5 us (8%)
  local copies, waits for them, and re-layouts  7.86 us (5%)
    all_to_all x2, blocking collectives, exchange(): return lax.all_to_all(array, axis, split_axis=0, concat_axis=0, tiled=True)  52.1 us
    all_to_all x2, waiting for transfers between devices, exchange(): return lax.all_to_all(array, axis, split_axis=0, concat_axis=0, tiled=True)  32.4 us
    all_to_all x2, starting transfers between devices, exchange(): return lax.all_to_all(array, axis, split_axis=0, concat_axis=0, tiled=True)  22.9 us
    ppermute x4, starting transfers between devices, swap(): return lax.ppermute(array, 'c', [(0, 1), (1, 0)])  20.6 us
    pallas_call x6, Pallas kernels, call(): pl.pallas_call(body, out_shape=outs, in_specs=ins, out_specs=spaces, scra...  13.5 us
    ppermute x1, waiting for transfers between devices, reach_over(): return lax.ppermute(array, 'y', [(k, k ^ 1) for k in range(N_Y)])  9.52 us
    unnamed x44, local copies, waits for them, and re-layouts  7.79 us
    ppermute x1, starting transfers between devices, reach_over(): return lax.ppermute(array, 'y', [(k, k ^ 1) for k in range(N_Y)])  4.02 us
  transfers between devices with their start and end apart: 7, of which 5 were waited for; matrix products, arithmetic and copies ran while one was open for 0% of the time, Pallas kernels for 2%

profile of v2, /device:TPU:1, one launch (start us, length us, event | category | flops | bytes accessed | tf_op | source)
XLA Modules:
  0.0 168.0 jit_solution(1963208825400792460)
XLA Ops:
  0.6 0.0 copy-start.7
  0.6 1.0 copy-done.7
  1.7 1.0 copy-done.8
  2.7 1.0 copy-done.9
  3.8 0.0 copy-start.18
  3.8 0.0 copy-start.19
  3.8 0.0 copy-start.20
  3.8 0.4 shard_map.177.own
  4.2 4.0 %collective-permute-start.1 = (bf16[6144,128]{1,0:T(8,128)(2,1)S(1)}, bf16[6144,128]{1,0:T(8,128)(2,1)}, u32[]{:S(2)}, u32[]{:S(2)}) collective-permute-start(bf16[6144,128]{1,0:T(8,128)(2,1)S(1)} %shard_map.177.own), channel_id=1, source_target_pairs={{0,2},{2,0},{4,6},{6,4},{8,10},{10,8},{12,14},{14,12},{1,3},{3,1},... | collective-permute-start | bytes 4718600 | tf_op jit(solution)/shard_map/ppermute | solution.py:334
  8.3 0.0 copy-done.1
  8.3 0.0 copy-done.6
  8.3 0.0 copy-done.15
  8.3 0.0 copy-done.16
  8.3 0.0 copy-done.18
  8.3 0.0 copy-done.19
  8.3 0.0 copy-done.20
  8.3 0.0 copy-done.21
  8.3 2.6 %shard_map.176 = (bf16[256,2176]{1,0:T(8,128)(2,1)S(1)}, bf16[256,256]{1,0:T(8,128)(2,1)S(1)}, bf16[256,256]{1,0:T(8,128)(2,1)S(1)}) custom-call(bf16[256,2048]{1,0:T(8,128)(2,1)S(1)} %copy-done.1, f32[1,2048]{1,0:T(1,128)S(1)} %bitcast.27, s32[4,256]{1,0:T(4,128)S(1)} %bitcast.34, f32[4,256]{1,0:T(4,128)S(1)} %bitcast.35, bf16[128,512]{1,0:T(8,128)(2,1)S(1)} %copy-done.6, ...), custom_call_target="tpu_custom_call" | custom-call | flops 268435456 | bytes 1048576 | tf_op jit(solution)/shard_map/pallas_call | solution.py:38
  11.0 1.0 copy-done.5
  12.0 12.9 %all-to-all-start = ((bf16[32,8,2176]{2,1,0:T(8,128)(2,1)}), bf16[32,8,2176]{2,1,0:T(8,128)(2,1)S(1)}, u32[]{:S(2)}, u32[]{:S(2)}) async-start(bf16[32,8,2176]{2,1,0:T(8,128)(2,1)} %bitcast.19), calls=%async_computation | async-start | bytes 2228224 | tf_op jit(solution)/shard_map/all_to_all | solution.py:326
  24.9 3.1 %collective-permute-start = (bf16[6144,128]{1,0:T(8,128)(2,1)S(1)}, bf16[6144,128]{1,0:T(8,128)(2,1)S(1)}, u32[]{:S(2)}, u32[]{:S(2)}) collective-permute-start(bf16[6144,128]{1,0:T(8,128)(2,1)S(1)} %shard_map.177.own), channel_id=1, source_target_pairs={{0,1},{1,0},{2,3},{3,2},{4,5},{5,4},{6,7},{7,6},{8,9},{9,8},{10,11... | collective-permute-start | bytes 4718600 | tf_op jit(solution)/shard_map/ppermute | solution.py:330
  28.0 9.5 %collective-permute-done.1.near = bf16[6144,128]{1,0:T(8,128)(2,1)} collective-permute-done((bf16[6144,128]{1,0:T(8,128)(2,1)S(1)}, bf16[6144,128]{1,0:T(8,128)(2,1)}, u32[]{:S(2)}, u32[]{:S(2)}) %collective-permute-start.1) | collective-permute-done | bytes 1572896 | tf_op jit(solution)/shard_map/ppermute | solution.py:334
  37.5 8.1 %collective-permute-start.2 = (bf16[6144,128]{1,0:T(8,128)(2,1)}, bf16[6144,128]{1,0:T(8,128)(2,1)}, u32[]{:S(2)}, u32[]{:S(2)}) collective-permute-start(bf16[6144,128]{1,0:T(8,128)(2,1)} %collective-permute-done.1.near), channel_id=1, source_target_pairs={{0,1},{1,0},{2,3},{3,2},{4,5},{5,4},{6,7},{7,6},{8,9},{9,8},{10,11... | collective-permute-start | bytes 4718600 | tf_op jit(solution)/shard_map/ppermute | solution.py:330
  45.6 0.0 collective-permute-done.beside
  45.6 1.2 copy-done.3
  46.8 5.3 %all-to-all-done = bf16[32,8,2176]{2,1,0:T(8,128)(2,1)S(1)} async-done(((bf16[32,8,2176]{2,1,0:T(8,128)(2,1)}), bf16[32,8,2176]{2,1,0:T(8,128)(2,1)S(1)}, u32[]{:S(2)}, u32[]{:S(2)}) %all-to-all-start) | async-done | bytes 1114144 | tf_op jit(solution)/shard_map/all_to_all | solution.py:326
  52.1 0.0 collective-permute-done.2.far
  52.1 1.4 copy-done.4
  53.5 5.9 %shard_map.178 = bf16[256,2176]{1,0:T(8,128)(2,1)S(1)} custom-call(bf16[256,2176]{1,0:T(8,128)(2,1)S(1)} %bitcast.17, bf16[6144,128]{1,0:T(8,128)(2,1)S(1)} %shard_map.177.own, bf16[6144,128]{1,0:T(8,128)(2,1)S(1)} %copy-done.4, bf16[6144,128]{1,0:T(8,128)(2,1)} %collective-permute-done.1.near, bf16[6144,128]{1,0:T(8,128)(2,1)} %collective-permute-done.2.far), custom_call_target="tpu_custom_call" | custom-call | flops 2147483648 | bytes 1048576 | tf_op jit(solution)/shard_map/pallas_call | solution.py:38
  59.4 1.0 copy-done
  60.5 0.0 copy-start.11
  60.5 0.0 copy-start.12
  60.5 0.0 copy-start.17
  60.5 10.0 %all-to-all-start.1 = ((bf16[32,8,2176]{2,1,0:T(8,128)(2,1)}), bf16[32,8,2176]{2,1,0:T(8,128)(2,1)S(1)}, u32[]{:S(2)}, u32[]{:S(2)}) async-start(bf16[32,8,2176]{2,1,0:T(8,128)(2,1)} %bitcast.18), calls=%async_computation.1 | async-start | bytes 2228224 | tf_op jit(solution)/shard_map/all_to_all | solution.py:326
  70.6 0.9 shard_map.179.act
  71.5 27.1 %all-to-all-done.1 = bf16[32,8,2176]{2,1,0:T(8,128)(2,1)S(1)} async-done(((bf16[32,8,2176]{2,1,0:T(8,128)(2,1)}), bf16[32,8,2176]{2,1,0:T(8,128)(2,1)S(1)}, u32[]{:S(2)}, u32[]{:S(2)}) %all-to-all-start.1) | async-done | bytes 1114144 | tf_op jit(solution)/shard_map/all_to_all | solution.py:326
  98.7 0.0 copy-done.12
  98.7 2.2 %shard_map.180 = (f32[8,24,2048]{2,1,0:T(8,128)S(1)}, bf16[8,24,2048]{2,1,0:T(8,128)(2,1)S(1)}) custom-call(bf16[256,2176]{1,0:T(8,128)(2,1)S(1)} %bitcast.16, bf16[256,256]{1,0:T(8,128)(2,1)S(1)} %get-tuple-element.10.w_high, bf16[256,256]{1,0:T(8,128)(2,1)S(1)} %get-tuple-element.12.w_low, bf16[256,32]{1,0:T(8,128)(2,1)S(1)} %shard_map.179.act, ...), custom_call_target="tpu_custom_call" | custom-call | flops 268435456 | bytes 1048576 | tf_op jit(solution)/shard_map/pallas_call | solution.py:38
  100.9 4.2 %collective-permute-start.3 = (bf16[8,24,2048]{2,1,0:T(8,128)(2,1)S(1)}, bf16[8,24,2048]{2,1,0:T(8,128)(2,1)S(1)}, u32[]{:S(2)}, u32[]{:S(2)}) collective-permute-start(bf16[8,24,2048]{2,1,0:T(8,128)(2,1)S(1)} %get-tuple-element.15), channel_id=1, source_target_pairs={{0,1},{1,0},{2,3},{3,2},{4,5},{5,4},{6,7},{7,6},{8,9},{9,8},{10,11... | collective-permute-start | bytes 2359304 | tf_op jit(solution)/shard_map/ppermute | solution.py:330
  105.1 1.9 %collective-permute-done.3 = bf16[8,24,2048]{2,1,0:T(8,128)(2,1)S(1)} collective-permute-done((bf16[8,24,2048]{2,1,0:T(8,128)(2,1)S(1)}, bf16[8,24,2048]{2,1,0:T(8,128)(2,1)S(1)}, u32[]{:S(2)}, u32[]{:S(2)}) %collective-permute-start.3) | collective-permute-done | bytes 786464 | tf_op jit(solution)/shard_map/ppermute | solution.py:330
  107.0 0.2 add_convert_fusion
  107.1 29.0 %all_to_all.20 = bf16[8,24,2048]{2,1,0:T(8,128)(2,1)S(1)} all-to-all(bf16[8,24,2048]{2,1,0:T(8,128)(2,1)S(1)} %add_convert_fusion), channel_id=1, replica_groups=mesh['z'=8,'x'=4,'y'=8,'c'=2] {'y'}, dimensions={0} | all-to-all | bytes 1572864 | tf_op jit(solution)/shard_map/all_to_all | solution.py:326
  136.1 0.1 reduce_sum.12
  136.2 0.1 broadcast_in_dim.5
  136.3 23.1 %all_to_all.21.mine = bf16[8,24,2048]{2,1,0:T(8,128)(2,1)S(1)} all-to-all(bf16[8,24,2048]{2,1,0:T(8,128)(2,1)S(1)} %broadcast_in_dim.5), channel_id=1, replica_groups=mesh['z'=8,'x'=4,'y'=8,'c'=2] {'y'}, dimensions={0} | all-to-all | bytes 1572864 | tf_op jit(solution)/shard_map/all_to_all | solution.py:326
  159.5 5.2 %collective-permute-start.4 = (bf16[8,24,2048]{2,1,0:T(8,128)(2,1)S(1)}, bf16[8,24,2048]{2,1,0:T(8,128)(2,1)S(1)}, u32[]{:S(2)}, u32[]{:S(2)}) collective-permute-start(bf16[8,24,2048]{2,1,0:T(8,128)(2,1)S(1)} %all_to_all.21.mine), channel_id=1, source_target_pairs={{0,1},{1,0},{2,3},{3,2},{4,5},{5,4},{6,7},{7,6},{8,9},{9,8},{10,11... | collective-permute-start | bytes 2359304 | tf_op jit(solution)/shard_map/ppermute | solution.py:330
  164.7 1.9 %collective-permute-done.4.other = bf16[8,24,2048]{2,1,0:T(8,128)(2,1)S(1)} collective-permute-done((bf16[8,24,2048]{2,1,0:T(8,128)(2,1)S(1)}, bf16[8,24,2048]{2,1,0:T(8,128)(2,1)S(1)}, u32[]{:S(2)}, u32[]{:S(2)}) %collective-permute-start.4) | collective-permute-done | bytes 786464 | tf_op jit(solution)/shard_map/ppermute | solution.py:330
  166.6 1.4 shard_map.181
  (21 shorter events, 0.0 us)
Async XLA Ops:
  0.6 1.0 copy-start.7
  1.7 1.0 copy-start.8
  2.7 1.0 copy-start.9
  3.8 4.5 %copy-start.1 = (bf16[256,2048]{1,0:T(8,128)(2,1)S(1)}, bf16[256,2048]{1,0:T(8,128)(2,1)}, u32[]{:S(2)}) copy-start(bf16[256,2048]{1,0:T(8,128)(2,1)} %x.2) | copy-start | bytes 3145732
  3.8 4.5 %copy-start.6 = (bf16[128,512]{1,0:T(8,128)(2,1)S(1)}, bf16[128,512]{1,0:T(8,128)(2,1)}, u32[]{:S(2)}) copy-start(bf16[128,512]{1,0:T(8,128)(2,1)} %keys.3) | copy-start | bytes 393220
  3.8 4.5 %copy-start.15 = (bf16[128,64]{0,1:T(8,128)(2,1)S(1)}, bf16[128,64]{0,1:T(8,128)(2,1)}, u32[]{:S(2)}) copy-start(bf16[128,64]{0,1:T(8,128)(2,1)} %param.19) | copy-start | bytes 49156
  3.8 4.5 %copy-start.16 = (f32[2048]{0:T(1024)S(1)}, f32[2048]{0:T(1024)}, u32[]{:S(2)}) copy-start(f32[2048]{0:T(1024)} %param.25) | copy-start | bytes 24580
  3.8 4.5 %copy-start.18 = (f32[128,2]{0,1:T(2,128)S(1)}, f32[128,2]{0,1:T(2,128)}, u32[]{:S(2)}) copy-start(f32[128,2]{0,1:T(2,128)} %param.21) | copy-start | bytes 3076
  3.8 4.5 %copy-start.19 = (f32[128,2]{0,1:T(2,128)S(1)}, f32[128,2]{0,1:T(2,128)}, u32[]{:S(2)}) copy-start(f32[128,2]{0,1:T(2,128)} %param.22) | copy-start | bytes 3076
  3.8 4.5 %copy-start.20 = (s32[256,4]{0,1:T(4,128)S(1)}, s32[256,4]{0,1:T(4,128)}, u32[]{:S(2)}) copy-start(s32[256,4]{0,1:T(4,128)} %param.26) | copy-start | bytes 12292
  3.8 4.5 %copy-start.21 = (f32[256,4]{0,1:T(4,128)S(1)}, f32[256,4]{0,1:T(4,128)}, u32[]{:S(2)}) copy-start(f32[256,4]{0,1:T(4,128)} %param.27) | copy-start | bytes 12292
  4.2 33.3 %collective-permute-start.1 = (bf16[6144,128]{1,0:T(8,128)(2,1)S(1)}, bf16[6144,128]{1,0:T(8,128)(2,1)}, u32[]{:S(2)}, u32[]{:S(2)}) collective-permute-start(bf16[6144,128]{1,0:T(8,128)(2,1)S(1)} %shard_map.177.own), channel_id=1, source_target_pairs={{0,2},{2,0},{4,6},{6,4},{8,10},{10,8},{12,14},{14,12},{1,3},{3,1},... | collective-permute-start | bytes 4718600 | tf_op jit(solution)/shard_map/ppermute | solution.py:334
  10.9 1.0 copy-start.5
  12.0 40.1 %all-to-all-start = ((bf16[32,8,2176]{2,1,0:T(8,128)(2,1)}), bf16[32,8,2176]{2,1,0:T(8,128)(2,1)S(1)}, u32[]{:S(2)}, u32[]{:S(2)}) async-start(bf16[32,8,2176]{2,1,0:T(8,128)(2,1)} %bitcast.19), calls=%async_computation | async-start | bytes 2228224 | tf_op jit(solution)/shard_map/all_to_all | solution.py:326
  24.9 20.7 %collective-permute-start = (bf16[6144,128]{1,0:T(8,128)(2,1)S(1)}, bf16[6144,128]{1,0:T(8,128)(2,1)S(1)}, u32[]{:S(2)}, u32[]{:S(2)}) collective-permute-start(bf16[6144,128]{1,0:T(8,128)(2,1)S(1)} %shard_map.177.own), channel_id=1, source_target_pairs={{0,1},{1,0},{2,3},{3,2},{4,5},{5,4},{6,7},{7,6},{8,9},{9,8},{10,11... | collective-permute-start | bytes 4718600 | tf_op jit(solution)/shard_map/ppermute | solution.py:330
  37.5 14.6 %collective-permute-start.2 = (bf16[6144,128]{1,0:T(8,128)(2,1)}, bf16[6144,128]{1,0:T(8,128)(2,1)}, u32[]{:S(2)}, u32[]{:S(2)}) collective-permute-start(bf16[6144,128]{1,0:T(8,128)(2,1)} %collective-permute-done.1.near), channel_id=1, source_target_pairs={{0,1},{1,0},{2,3},{3,2},{4,5},{5,4},{6,7},{7,6},{8,9},{9,8},{10,11... | collective-permute-start | bytes 4718600 | tf_op jit(solution)/shard_map/ppermute | solution.py:330
  45.6 1.2 copy-start.3
  52.1 1.4 copy-start.4
  59.4 1.0 copy-start
  60.5 10.1 %copy-start.2 = (bf16[256,2048]{1,0:T(8,128)(2,1)S(1)}, bf16[256,2048]{1,0:T(8,128)(2,1)}, u32[]{:S(2)}) copy-start(bf16[256,2048]{1,0:T(8,128)(2,1)} %x.2) | copy-start | bytes 3145732
  60.5 10.1 %copy-start.13 = (bf16[2048,32]{0,1:T(8,128)(2,1)S(1)}, bf16[2048,32]{0,1:T(8,128)(2,1)}, u32[]{:S(2)}) copy-start(bf16[2048,32]{0,1:T(8,128)(2,1)} %param.31) | copy-start | bytes 393220
  60.5 10.1 %copy-start.14 = (bf16[2048,32]{0,1:T(8,128)(2,1)S(1)}, bf16[2048,32]{0,1:T(8,128)(2,1)}, u32[]{:S(2)}) copy-start(bf16[2048,32]{0,1:T(8,128)(2,1)} %param.32) | copy-start | bytes 393220
  60.5 38.2 %copy-start.10 = (bf16[64,2048]{1,0:T(8,128)(2,1)S(1)}, bf16[64,2048]{1,0:T(8,128)(2,1)}, u32[]{:S(2)}) copy-start(bf16[64,2048]{1,0:T(8,128)(2,1)} %mix.1) | copy-start | bytes 786436
  60.5 38.2 %copy-start.11 = (bf16[32,2048]{1,0:T(8,128)(2,1)S(1)}, bf16[32,2048]{1,0:T(8,128)(2,1)}, u32[]{:S(2)}) copy-start(bf16[32,2048]{1,0:T(8,128)(2,1)} %down.1) | copy-start | bytes 393220
  60.5 38.2 %copy-start.12 = (bf16[128,512]{1,0:T(8,128)(2,1)S(1)}, bf16[128,512]{1,0:T(8,128)(2,1)}, u32[]{:S(2)}) copy-start(bf16[128,512]{1,0:T(8,128)(2,1)} %queries.1) | copy-start | bytes 393220
  60.5 38.2 %copy-start.17 = (bf16[128,64]{0,1:T(8,128)(2,1)S(1)}, bf16[128,64]{0,1:T(8,128)(2,1)}, u32[]{:S(2)}) copy-start(bf16[128,64]{0,1:T(8,128)(2,1)} %param.20) | copy-start | bytes 49156
  60.5 38.1 %all-to-all-start.1 = ((bf16[32,8,2176]{2,1,0:T(8,128)(2,1)}), bf16[32,8,2176]{2,1,0:T(8,128)(2,1)S(1)}, u32[]{:S(2)}, u32[]{:S(2)}) async-start(bf16[32,8,2176]{2,1,0:T(8,128)(2,1)} %bitcast.18), calls=%async_computation.1 | async-start | bytes 2228224 | tf_op jit(solution)/shard_map/all_to_all | solution.py:326
  100.9 6.1 %collective-permute-start.3 = (bf16[8,24,2048]{2,1,0:T(8,128)(2,1)S(1)}, bf16[8,24,2048]{2,1,0:T(8,128)(2,1)S(1)}, u32[]{:S(2)}, u32[]{:S(2)}) collective-permute-start(bf16[8,24,2048]{2,1,0:T(8,128)(2,1)S(1)} %get-tuple-element.15), channel_id=1, source_target_pairs={{0,1},{1,0},{2,3},{3,2},{4,5},{5,4},{6,7},{7,6},{8,9},{9,8},{10,11... | collective-permute-start | bytes 2359304 | tf_op jit(solution)/shard_map/ppermute | solution.py:330
  159.5 7.1 %collective-permute-start.4 = (bf16[8,24,2048]{2,1,0:T(8,128)(2,1)S(1)}, bf16[8,24,2048]{2,1,0:T(8,128)(2,1)S(1)}, u32[]{:S(2)}, u32[]{:S(2)}) collective-permute-start(bf16[8,24,2048]{2,1,0:T(8,128)(2,1)S(1)} %all_to_all.21.mine), channel_id=1, source_target_pairs={{0,1},{1,0},{2,3},{3,2},{4,5},{5,4},{6,7},{7,6},{8,9},{9,8},{10,11... | collective-permute-start | bytes 2359304 | tf_op jit(solution)/shard_map/ppermute | solution.py:330

commit v3 on v2

--- a/solution.py
+++ b/solution.py
@@ -19,6 +19,7 @@
 M_ROWS = BLOCK // 16
 PIECE = E_ROWS + M_ROWS
 EP = ("z", "x")
+WHOLE = 67_000_000
 EP_TP = ("z", "x", "y", "c")
 TP = ("y", "c")
 bf16 = jnp.bfloat16
@@ -34,14 +35,14 @@
 TN = (((0,), (0,)), ((), ()))
 
 
-def call(body, arrays, ins, outs, spaces, scratch, flops, limit=16):
+def call(body, arrays, ins, outs, spaces, scratch, flops, limit=16 << 20):
     return pl.pallas_call(
         body,
         out_shape=outs,
         in_specs=ins,
         out_specs=spaces,
         scratch_shapes=scratch,
-        compiler_params=pltpu.CompilerParams(vmem_limit_bytes=limit << 20),
+        compiler_params=pltpu.CompilerParams(vmem_limit_bytes=limit),
         cost_estimate=pl.CostEstimate(flops=flops, bytes_accessed=1 << 20, transcendentals=0),
     )(*arrays)
 
@@ -77,25 +78,6 @@
         jnp.broadcast_to(log_forget, (8, BLOCK)), upto, preferred_element_type=f32, precision=HIGHEST
     )[0:1, :]
     return given, cumulative
-
-
-def pack_kernel(gate, up, down, packed, sem):
-    copies = [
-        pltpu.make_async_copy(gate, packed.at[0:D, :], sem.at[0]),
-        pltpu.make_async_copy(up, packed.at[D : 2 * D, :], sem.at[1]),
-    ]
-    for k in range(16):
-        copies.append(
-            pltpu.make_async_copy(
-                down.at[:, 128 * k : 128 * (k + 1)],
-                packed.at[2 * D + 128 * k : 2 * D + 128 * (k + 1), :],
-                sem.at[2 + k],
-            )
-        )
-    for copy in copies:
-        copy.start()
-    for copy in copies:
-        copy.wait()
 
 
 def normalize(x, gain):
@@ -192,45 +174,37 @@
     states[:, 7, :] = jnp.zeros((N_EP, 128), f32)
 
 
-def expert_kernel(x, own, beside, near, far, out, staged, states, taken, sem, fetch):
-    fetches = [
-        pltpu.make_async_copy(pack, taken.at[k], fetch.at[k])
-        for k, pack in enumerate((beside, near, far))
-    ]
-    for copy in fetches:
-        copy.start()
-    states[...] = x[:, D:WIDE].astype(f32).reshape(N_EP, 8, 128)
+def expert_kernel(*refs):
+    x, weights = refs[0], refs[1:13]
+    out, taken, wide, tall, staged, states, sem, fetch = refs[13:]
+    first = pltpu.make_async_copy(x, taken, fetch.at[12])
+    first.start()
+    fetches = []
+    for k in range(4):
+        targets = (wide.at[k, :, 0:128], wide.at[k, :, 128:256], tall.at[128 * k : 128 * (k + 1), :])
+        for j in range(3):
+            fetches.append(pltpu.make_async_copy(weights[3 * k + j], targets[j], fetch.at[3 * k + j]))
+            fetches[-1].start()
+    first.wait()
+    states[...] = taken[:, D:WIDE].astype(f32).reshape(N_EP, 8, 128)
     prefix(states)
     staged[:, D:WIDE] = states[...].reshape(ROWS, 128).astype(bf16)
     copies = [pltpu.make_async_copy(staged.at[:, D:WIDE], out.at[:, D:WIDE], sem.at[0])]
     copies[0].start()
-    rows = x[:, 0:D]
-    packs = (own, taken.at[0], taken.at[1], taken.at[2])
+    rows = taken[:, 0:D]
     acts = []
-    for k, pack in enumerate(packs):
-        if k > 0:
-            fetches[k - 1].wait()
-        both = jnp.dot(
-            rows,
-            jnp.concatenate([pack[0:D, :], pack[D : 2 * D, :]], axis=1),
-            preferred_element_type=f32,
-        )
-        gate, up = both[:, 0:128], both[:, 128:256]
-        acts.append((gate / (1.0 + jnp.exp(-gate)) * up).astype(bf16))
+    for k in range(4):
+        fetches[3 * k].wait()
+        fetches[3 * k + 1].wait()
+        both = jnp.dot(rows, wide[k], preferred_element_type=f32)
+        gated, lifted = both[:, 0:128], both[:, 128:256]
+        acts.append((gated / (1.0 + jnp.exp(-gated)) * lifted).astype(bf16))
+    for k in range(4):
+        fetches[3 * k + 2].wait()
     act = jnp.concatenate(acts, axis=1)
-    for k in range(8):
-        low = 2 * D + 256 * k
-        down = jnp.concatenate(
-            [
-                jnp.concatenate(
-                    [pack[low : low + 128, :], pack[low + 128 : low + 256, :]], axis=1
-                )
-                for pack in packs
-            ],
-            axis=0,
-        )
-        at = slice(256 * k, 256 * (k + 1))
-        staged[:, at] = jnp.dot(act, down, preferred_element_type=f32).astype(bf16)
+    for k in range(4):
+        at = slice(512 * k, 512 * (k + 1))
+        staged[:, at] = jnp.dot(act, tall[:, at], preferred_element_type=f32).astype(bf16)
         copies.append(pltpu.make_async_copy(staged.at[:, at], out.at[:, at], sem.at[k + 1]))
         copies[-1].start()
     for copy in copies:
@@ -358,16 +332,8 @@
     shared_down,
 ):
     dma = pltpu.SemaphoreType.DMA
-    (own,) = call(
-        pack_kernel,
-        (expert_gate[0], expert_up[0], expert_down[0]),
-        [HBM] * 3,
-        [shape((3 * D, 128), bf16)],
-        [VMEM],
-        [dma((18,))],
-        1 << 20,
-    )
-    near = reach_over(own)
+    own = (expert_gate[0], expert_up[0], expert_down[0])
+    near_gate = reach_over(own[0])
     values_t, out_gate_t = values.T, out_gate.T
     input_t, forget_t = input_gate.T, forget_gate.T
     send, w_high, w_low = call(
@@ -391,10 +357,14 @@
         [HBM] + [VMEM] * 2,
         [pltpu.VMEM((ROWS, WIDE), bf16), pltpu.VMEM((N_EP, 8, 128), f32), dma((5,))],
         1 << 28,
+        WHOLE,
     )
     arrived = exchange(send.reshape(N_EP, SLOTS, WIDE), EP).reshape(ROWS, WIDE)
-    beside = swap(after(own, w_high))
-    far = swap(near)
+    near_up = reach_over(own[1])
+    near_down = reach_over(after(own[2], w_high))
+    near = (near_gate, near_up, near_down)
+    beside = tuple(swap(after(array, w_high)) for array in own)
+    far = tuple(swap(array) for array in near)
     (act,) = call(
         shared_kernel,
         (after(expert_input, w_high), norm_gain[None, :], shared_gate.T, shared_up.T),
@@ -406,19 +376,21 @@
     )
     (results,) = call(
         expert_kernel,
-        (arrived, own, beside, near, far),
-        [VMEM] * 2 + [HBM] * 3,
+        (arrived,) + own + beside + near + far,
+        [HBM] * 13,
         [shape((ROWS, WIDE), bf16)],
         [HBM],
         [
             pltpu.VMEM((ROWS, WIDE), bf16),
+            pltpu.VMEM((4, D, 256), bf16),
+            pltpu.VMEM((512, D), bf16),
+            pltpu.VMEM((ROWS, WIDE), bf16),
             pltpu.VMEM((N_EP, 8, 128), f32),
-            pltpu.VMEM((3, 3 * D, 128), bf16),
-            dma((9,)),
-            dma((3,)),
+            dma((5,)),
+            dma((13,)),
         ],
         1 << 31,
-        24,
+        WHOLE,
     )
     back = exchange(results.reshape(N_EP, SLOTS, WIDE), EP).reshape(ROWS, WIDE)
     keep, give = call(

time: 169 us -> 175 us (1.036)
  starting transfers between devices: 47.6 us -> 62 us
  local copies, waits for them, and re-layouts: 7.86 us -> 2.05 us
  waiting for transfers between devices: 45.7 us -> 42.1 us
    ppermute x4 -> x8, starting transfers between devices: 20.6 us -> 30.2 us  [swap(): return lax.ppermute(array, 'c', [(0, 1), (1, 0)])]
    unnamed x44 -> x50, local copies, waits for them, and re-layouts: 7.79 us -> 1.98 us
    all_to_all x2, waiting for transfers between devices: 32.4 us -> 27.6 us  [exchange(): return lax.all_to_all(array, axis, split_axis=0, concat_axis=0, tiled=True)]
    ppermute x1 -> x3, starting transfers between devices: 4.02 us -> 8.49 us  [reach_over(): return lax.ppermute(array, 'y', [(k, k ^ 1) for k in range(N_Y)])]
    pallas_call x6 -> x5, Pallas kernels: 13.5 us -> 15.1 us  [call(): pl.pallas_call(body, out_shape=outs, in_specs=ins, out_specs=spaces, scra...]
    ppermute x1 -> x3, waiting for transfers between devices: 9.52 us -> 10.7 us  [reach_over(): return lax.ppermute(array, 'y', [(k, k ^ 1) for k in range(N_Y)])]
    ppermute x4 -> x8, waiting for transfers between devices: 3.79 us -> 3.8 us  [swap(): return lax.ppermute(array, 'c', [(0, 1), (1, 0)])]
  transfers between devices with their start and end apart: 7 -> 13, of which waited for: 5 -> 6; matrix products, arithmetic and copies ran while one was open for 0% -> 0% of each run, Pallas kernels for 2% -> 1%
where the time goes in v3:
time: 175 us
  starting transfers between devices  62 us (35%)
  blocking collectives  52.1 us (30%)
  waiting for transfers between devices  42.1 us (24%)
  Pallas kernels  15.1 us (9%)
  local copies, waits for them, and re-layouts  2.05 us (1%)
    all_to_all x2, blocking collectives, exchange(): return lax.all_to_all(array, axis, split_axis=0, concat_axis=0, tiled=True)  52.1 us
    ppermute x8, starting transfers between devices, swap(): return lax.ppermute(array, 'c', [(0, 1), (1, 0)])  30.2 us
    all_to_all x2, waiting for transfers between devices, exchange(): return lax.all_to_all(array, axis, split_axis=0, concat_axis=0, tiled=True)  27.6 us
    all_to_all x2, starting transfers between devices, exchange(): return lax.all_to_all(array, axis, split_axis=0, concat_axis=0, tiled=True)  23.3 us
    pallas_call x5, Pallas kernels, call(): pl.pallas_call(body, out_shape=outs, in_specs=ins, out_specs=spaces, scra...  15.1 us
    ppermute x3, waiting for transfers between devices, reach_over(): return lax.ppermute(array, 'y', [(k, k ^ 1) for k in range(N_Y)])  10.7 us
    ppermute x3, starting transfers between devices, reach_over(): return lax.ppermute(array, 'y', [(k, k ^ 1) for k in range(N_Y)])  8.49 us
    ppermute x8, waiting for transfers between devices, swap(): return lax.ppermute(array, 'c', [(0, 1), (1, 0)])  3.8 us
  transfers between devices with their start and end apart: 13, of which 6 were waited for; matrix products, arithmetic and copies ran while one was open for 0% of the time, Pallas kernels for 1%

profile of v3, /device:TPU:1, one launch (start us, length us, event | category | flops | bytes accessed | tf_op | source)
XLA Modules:
  0.0 174.7 jit_solution(9353951241639228673)
XLA Ops:
  0.6 4.1 %shard_map.176 = (bf16[256,2176]{1,0:T(8,128)(2,1)}, bf16[256,256]{1,0:T(8,128)(2,1)}, bf16[256,256]{1,0:T(8,128)(2,1)}) custom-call(bf16[256,2048]{1,0:T(8,128)(2,1)} %x.2, f32[1,2048]{1,0:T(1,128)} %bitcast.21, s32[4,256]{1,0:T(4,128)} %bitcast.39, f32[4,256]{1,0:T(4,128)} %bitcast.40, bf16[128,512]{1,0:T(8,128)(2,1)} %keys.3, bf16[64,128]{1,0:T(8,128)(2,1)} %bitcast.19, ...), custom_call_target="tpu_custom_call" | custom-call | flops 268435456 | bytes 1048576 | tf_op jit(solution)/shard_map/pallas_call | solution.py:39
  4.7 0.0 copy-start.16
  4.7 0.0 copy-start.14
  4.7 0.0 copy-start.15
  4.8 14.0 %all-to-all-start = ((bf16[32,8,2176]{2,1,0:T(8,128)(2,1)}), bf16[32,8,2176]{2,1,0:T(8,128)(2,1)}, u32[]{:S(2)}, u32[]{:S(2)}) async-start(bf16[32,8,2176]{2,1,0:T(8,128)(2,1)} %bitcast.29), calls=%async_computation | async-start | bytes 2228224 | tf_op jit(solution)/shard_map/all_to_all | solution.py:300
  18.7 3.2 %collective-permute-start.5 = (bf16[128,2048]{1,0:T(8,128)(2,1)S(1)}, bf16[128,2048]{1,0:T(8,128)(2,1)S(1)}, u32[]{:S(2)}, u32[]{:S(2)}) collective-permute-start(bf16[128,2048]{1,0:T(8,128)(2,1)S(1)} %bitcast.37), channel_id=1, source_target_pairs={{0,2},{2,0},{4,6},{6,4},{8,10},{10,8},{12,14},{14,12},{1,3},{3,1},... | collective-permute-start | bytes 1572872 | tf_op jit(solution)/shard_map/ppermute | solution.py:308
  22.0 3.1 %collective-permute-start = (bf16[2048,128]{1,0:T(8,128)(2,1)S(1)}, bf16[2048,128]{1,0:T(8,128)(2,1)S(1)}, u32[]{:S(2)}, u32[]{:S(2)}) collective-permute-start(bf16[2048,128]{1,0:T(8,128)(2,1)S(1)} %bitcast.31), channel_id=1, source_target_pairs={{0,1},{1,0},{2,3},{3,2},{4,5},{5,4},{6,7},{7,6},{8,9},{9,8},{10,11... | collective-permute-start | bytes 1572872 | tf_op jit(solution)/shard_map/ppermute | solution.py:304
  25.1 2.1 %collective-permute-start.3 = (bf16[2048,128]{1,0:T(8,128)(2,1)S(1)}, bf16[2048,128]{1,0:T(8,128)(2,1)S(1)}, u32[]{:S(2)}, u32[]{:S(2)}) collective-permute-start(bf16[2048,128]{1,0:T(8,128)(2,1)S(1)} %bitcast.32), channel_id=1, source_target_pairs={{0,2},{2,0},{4,6},{6,4},{8,10},{10,8},{12,14},{14,12},{1,3},{3,1},... | collective-permute-start | bytes 1572872 | tf_op jit(solution)/shard_map/ppermute | solution.py:308
  27.2 3.2 %collective-permute-start.4 = (bf16[2048,128]{1,0:T(8,128)(2,1)S(1)}, bf16[2048,128]{1,0:T(8,128)(2,1)S(1)}, u32[]{:S(2)}, u32[]{:S(2)}) collective-permute-start(bf16[2048,128]{1,0:T(8,128)(2,1)S(1)} %bitcast.34), channel_id=1, source_target_pairs={{0,2},{2,0},{4,6},{6,4},{8,10},{10,8},{12,14},{14,12},{1,3},{3,1},... | collective-permute-start | bytes 1572872 | tf_op jit(solution)/shard_map/ppermute | solution.py:308
  30.4 2.5 %collective-permute-start.2 = (bf16[128,2048]{1,0:T(8,128)(2,1)S(1)}, bf16[128,2048]{1,0:T(8,128)(2,1)S(1)}, u32[]{:S(2)}, u32[]{:S(2)}) collective-permute-start(bf16[128,2048]{1,0:T(8,128)(2,1)S(1)} %bitcast.38), channel_id=1, source_target_pairs={{0,1},{1,0},{2,3},{3,2},{4,5},{5,4},{6,7},{7,6},{8,9},{9,8},{10,11... | collective-permute-start | bytes 1572872 | tf_op jit(solution)/shard_map/ppermute | solution.py:304
  32.9 0.4 collective-permute-done.5.refs_9_
  33.3 5.0 %collective-permute-start.1 = (bf16[2048,128]{1,0:T(8,128)(2,1)S(1)}, bf16[2048,128]{1,0:T(8,128)(2,1)S(1)}, u32[]{:S(2)}, u32[]{:S(2)}) collective-permute-start(bf16[2048,128]{1,0:T(8,128)(2,1)S(1)} %bitcast.35), channel_id=1, source_target_pairs={{0,1},{1,0},{2,3},{3,2},{4,5},{5,4},{6,7},{7,6},{8,9},{9,8},{10,11... | collective-permute-start | bytes 1572872 | tf_op jit(solution)/shard_map/ppermute | solution.py:304
  38.3 0.0 copy-start.18
  38.3 1.9 %collective-permute-start.8 = (bf16[128,2048]{1,0:T(8,128)(2,1)S(1)}, bf16[128,2048]{1,0:T(8,128)(2,1)S(1)}, u32[]{:S(2)}, u32[]{:S(2)}) collective-permute-start(bf16[128,2048]{1,0:T(8,128)(2,1)S(1)} %collective-permute-done.5.refs_9_), channel_id=1, source_target_pairs={{0,1},{1,0},{2,3},{3,2},{4,5},{5,4},{6,7},{7,6},{8,9},{9,8},{10,11... | collective-permute-start | bytes 1572872 | tf_op jit(solution)/shard_map/ppermute | solution.py:304
  40.2 4.3 %collective-permute-done.3.refs_7_ = bf16[2048,128]{1,0:T(8,128)(2,1)S(1)} collective-permute-done((bf16[2048,128]{1,0:T(8,128)(2,1)S(1)}, bf16[2048,128]{1,0:T(8,128)(2,1)S(1)}, u32[]{:S(2)}, u32[]{:S(2)}) %collective-permute-start.3) | collective-permute-done | bytes 524320 | tf_op jit(solution)/shard_map/ppermute | solution.py:308
  44.5 5.0 %collective-permute-start.6 = (bf16[2048,128]{1,0:T(8,128)(2,1)S(1)}, bf16[2048,128]{1,0:T(8,128)(2,1)S(1)}, u32[]{:S(2)}, u32[]{:S(2)}) collective-permute-start(bf16[2048,128]{1,0:T(8,128)(2,1)S(1)} %collective-permute-done.3.refs_7_), channel_id=1, source_target_pairs={{0,1},{1,0},{2,3},{3,2},{4,5},{5,4},{6,7},{7,6},{8,9},{9,8},{10,11... | collective-permute-start | bytes 1572872 | tf_op jit(solution)/shard_map/ppermute | solution.py:304
  49.5 6.1 %collective-permute-done.4.refs_8_ = bf16[2048,128]{1,0:T(8,128)(2,1)S(1)} collective-permute-done((bf16[2048,128]{1,0:T(8,128)(2,1)S(1)}, bf16[2048,128]{1,0:T(8,128)(2,1)S(1)}, u32[]{:S(2)}, u32[]{:S(2)}) %collective-permute-start.4) | collective-permute-done | bytes 524320 | tf_op jit(solution)/shard_map/ppermute | solution.py:308
  55.6 3.7 %collective-permute-start.7 = (bf16[2048,128]{1,0:T(8,128)(2,1)S(1)}, bf16[2048,128]{1,0:T(8,128)(2,1)}, u32[]{:S(2)}, u32[]{:S(2)}) collective-permute-start(bf16[2048,128]{1,0:T(8,128)(2,1)S(1)} %collective-permute-done.4.refs_8_), channel_id=1, source_target_pairs={{0,1},{1,0},{2,3},{3,2},{4,5},{5,4},{6,7},{7,6},{8,9},{9,8},{10,11... | collective-permute-start | bytes 1572872 | tf_op jit(solution)/shard_map/ppermute | solution.py:304
  59.4 0.0 copy-start.22
  59.5 0.7 copy-done.22
  60.2 0.2 copy-done.21
  60.4 0.2 copy-done.23
  60.5 0.8 copy-done.24
  61.3 6.5 %shard_map.177 = bf16[256,2176]{1,0:T(8,128)(2,1)} custom-call(bf16[256,2176]{1,0:T(8,128)(2,1)} %bitcast.7.refs_0_, bf16[2048,128]{1,0:T(8,128)(2,1)} %bitcast.30, bf16[2048,128]{1,0:T(8,128)(2,1)} %bitcast.33, bf16[128,2048]{1,0:T(8,128)(2,1)} %bitcast.36, bf16[2048,128]{1,0:T(8,128)(2,1)} %copy-done.18, bf16[2048,128]{1,0:T(8,128)(2,1)} %copy-done.22, ...), custom_call_target="tpu_custom_call" | custom-call | flops 2147483648 | bytes 1048576 | tf_op jit(solution)/shard_map/pallas_call | solution.py:39
  67.8 0.0 copy-start
  67.8 0.0 copy-start.7
  67.8 0.0 copy-start.8
  67.8 0.0 copy-start.10
  67.9 0.0 copy-start.1
  67.9 0.0 copy-start.2
  67.9 0.0 copy-start.3
  67.9 0.0 copy-start.4
  67.9 0.0 copy-start.9
  67.9 0.0 copy-start.11
  68.0 9.3 %all-to-all-start.1 = ((bf16[32,8,2176]{2,1,0:T(8,128)(2,1)}), bf16[32,8,2176]{2,1,0:T(8,128)(2,1)S(1)}, u32[]{:S(2)}, u32[]{:S(2)}) async-start(bf16[32,8,2176]{2,1,0:T(8,128)(2,1)} %bitcast.28), calls=%async_computation.1 | async-start | bytes 2228224 | tf_op jit(solution)/shard_map/all_to_all | solution.py:300
  77.3 0.9 shard_map.178.act
  78.3 27.6 %all-to-all-done.1 = bf16[32,8,2176]{2,1,0:T(8,128)(2,1)S(1)} async-done(((bf16[32,8,2176]{2,1,0:T(8,128)(2,1)}), bf16[32,8,2176]{2,1,0:T(8,128)(2,1)S(1)}, u32[]{:S(2)}, u32[]{:S(2)}) %all-to-all-start.1) | async-done | bytes 1114144 | tf_op jit(solution)/shard_map/all_to_all | solution.py:300
  105.9 2.2 %shard_map.179 = (f32[8,24,2048]{2,1,0:T(8,128)S(1)}, bf16[8,24,2048]{2,1,0:T(8,128)(2,1)S(1)}) custom-call(bf16[256,2176]{1,0:T(8,128)(2,1)S(1)} %bitcast.16, bf16[256,256]{1,0:T(8,128)(2,1)S(1)} %copy-done.5, bf16[256,256]{1,0:T(8,128)(2,1)S(1)} %copy-done.6, bf16[256,32]{1,0:T(8,128)(2,1)S(1)} %shard_map.178.act, bf16[32,2048]{1,0:T(8,128)(2,1)S(1)} %copy-done.3, ...), custom_call_target="tpu_custom_call" | custom-call | flops 268435456 | bytes 1048576 | tf_op jit(solution)/shard_map/pallas_call | solution.py:39
  108.1 3.7 %collective-permute-start.9 = (bf16[8,24,2048]{2,1,0:T(8,128)(2,1)S(1)}, bf16[8,24,2048]{2,1,0:T(8,128)(2,1)S(1)}, u32[]{:S(2)}, u32[]{:S(2)}) collective-permute-start(bf16[8,24,2048]{2,1,0:T(8,128)(2,1)S(1)} %get-tuple-element.19), channel_id=1, source_target_pairs={{0,1},{1,0},{2,3},{3,2},{4,5},{5,4},{6,7},{7,6},{8,9},{9,8},{10,11... | collective-permute-start | bytes 2359304 | tf_op jit(solution)/shard_map/ppermute | solution.py:304
  111.9 1.9 %collective-permute-done.9 = bf16[8,24,2048]{2,1,0:T(8,128)(2,1)S(1)} collective-permute-done((bf16[8,24,2048]{2,1,0:T(8,128)(2,1)S(1)}, bf16[8,24,2048]{2,1,0:T(8,128)(2,1)S(1)}, u32[]{:S(2)}, u32[]{:S(2)}) %collective-permute-start.9) | collective-permute-done | bytes 786464 | tf_op jit(solution)/shard_map/ppermute | solution.py:304
  113.7 0.2 add_convert_fusion
  113.9 28.9 %all_to_all.20 = bf16[8,24,2048]{2,1,0:T(8,128)(2,1)S(1)} all-to-all(bf16[8,24,2048]{2,1,0:T(8,128)(2,1)S(1)} %add_convert_fusion), channel_id=1, replica_groups=mesh['z'=8,'x'=4,'y'=8,'c'=2] {'y'}, dimensions={0} | all-to-all | bytes 1572864 | tf_op jit(solution)/shard_map/all_to_all | solution.py:300
  142.9 0.1 reduce_sum.12
  143.0 0.1 broadcast_in_dim.5
  143.1 23.1 %all_to_all.21.mine = bf16[8,24,2048]{2,1,0:T(8,128)(2,1)S(1)} all-to-all(bf16[8,24,2048]{2,1,0:T(8,128)(2,1)S(1)} %broadcast_in_dim.5), channel_id=1, replica_groups=mesh['z'=8,'x'=4,'y'=8,'c'=2] {'y'}, dimensions={0} | all-to-all | bytes 1572864 | tf_op jit(solution)/shard_map/all_to_all | solution.py:300
  166.2 5.2 %collective-permute-start.10 = (bf16[8,24,2048]{2,1,0:T(8,128)(2,1)S(1)}, bf16[8,24,2048]{2,1,0:T(8,128)(2,1)S(1)}, u32[]{:S(2)}, u32[]{:S(2)}) collective-permute-start(bf16[8,24,2048]{2,1,0:T(8,128)(2,1)S(1)} %all_to_all.21.mine), channel_id=1, source_target_pairs={{0,1},{1,0},{2,3},{3,2},{4,5},{5,4},{6,7},{7,6},{8,9},{9,8},{10,11... | collective-permute-start | bytes 2359304 | tf_op jit(solution)/shard_map/ppermute | solution.py:304
  171.5 1.9 %collective-permute-done.10.other = bf16[8,24,2048]{2,1,0:T(8,128)(2,1)S(1)} collective-permute-done((bf16[8,24,2048]{2,1,0:T(8,128)(2,1)S(1)}, bf16[8,24,2048]{2,1,0:T(8,128)(2,1)S(1)}, u32[]{:S(2)}, u32[]{:S(2)}) %collective-permute-start.10) | collective-permute-done | bytes 786464 | tf_op jit(solution)/shard_map/ppermute | solution.py:304
  173.4 1.4 shard_map.180
  (38 shorter events, 0.1 us)
Async XLA Ops:
  4.7 14.0 %copy-start.16 = (bf16[1,128,2048]{2,1,0:T(8,128)(2,1)S(1)}, bf16[1,128,2048]{2,1,0:T(8,128)(2,1)}, u32[]{:S(2)}) copy-start(bf16[1,128,2048]{2,1,0:T(8,128)(2,1)} %param.30) | copy-start | bytes 1572868
  4.7 17.2 %copy-start.14 = (bf16[1,2048,128]{2,1,0:T(8,128)(2,1)S(1)}, bf16[1,2048,128]{2,1,0:T(8,128)(2,1)}, u32[]{:S(2)}) copy-start(bf16[1,2048,128]{2,1,0:T(8,128)(2,1)} %param.28) | copy-start | bytes 1572868
  4.7 22.5 %copy-start.15 = (bf16[1,2048,128]{2,1,0:T(8,128)(2,1)S(1)}, bf16[1,2048,128]{2,1,0:T(8,128)(2,1)}, u32[]{:S(2)}) copy-start(bf16[1,2048,128]{2,1,0:T(8,128)(2,1)} %param.29) | copy-start | bytes 1572868
  4.8 56.6 %all-to-all-start = ((bf16[32,8,2176]{2,1,0:T(8,128)(2,1)}), bf16[32,8,2176]{2,1,0:T(8,128)(2,1)}, u32[]{:S(2)}, u32[]{:S(2)}) async-start(bf16[32,8,2176]{2,1,0:T(8,128)(2,1)} %bitcast.29), calls=%async_computation | async-start | bytes 2228224 | tf_op jit(solution)/shard_map/all_to_all | solution.py:300
  18.7 14.5 %collective-permute-start.5 = (bf16[128,2048]{1,0:T(8,128)(2,1)S(1)}, bf16[128,2048]{1,0:T(8,128)(2,1)S(1)}, u32[]{:S(2)}, u32[]{:S(2)}) collective-permute-start(bf16[128,2048]{1,0:T(8,128)(2,1)S(1)} %bitcast.37), channel_id=1, source_target_pairs={{0,2},{2,0},{4,6},{6,4},{8,10},{10,8},{12,14},{14,12},{1,3},{3,1},... | collective-permute-start | bytes 1572872 | tf_op jit(solution)/shard_map/ppermute | solution.py:308
  22.0 16.3 %collective-permute-start = (bf16[2048,128]{1,0:T(8,128)(2,1)S(1)}, bf16[2048,128]{1,0:T(8,128)(2,1)S(1)}, u32[]{:S(2)}, u32[]{:S(2)}) collective-permute-start(bf16[2048,128]{1,0:T(8,128)(2,1)S(1)} %bitcast.31), channel_id=1, source_target_pairs={{0,1},{1,0},{2,3},{3,2},{4,5},{5,4},{6,7},{7,6},{8,9},{9,8},{10,11... | collective-permute-start | bytes 1572872 | tf_op jit(solution)/shard_map/ppermute | solution.py:304
  25.1 19.4 %collective-permute-start.3 = (bf16[2048,128]{1,0:T(8,128)(2,1)S(1)}, bf16[2048,128]{1,0:T(8,128)(2,1)S(1)}, u32[]{:S(2)}, u32[]{:S(2)}) collective-permute-start(bf16[2048,128]{1,0:T(8,128)(2,1)S(1)} %bitcast.32), channel_id=1, source_target_pairs={{0,2},{2,0},{4,6},{6,4},{8,10},{10,8},{12,14},{14,12},{1,3},{3,1},... | collective-permute-start | bytes 1572872 | tf_op jit(solution)/shard_map/ppermute | solution.py:308
  27.2 28.4 %collective-permute-start.4 = (bf16[2048,128]{1,0:T(8,128)(2,1)S(1)}, bf16[2048,128]{1,0:T(8,128)(2,1)S(1)}, u32[]{:S(2)}, u32[]{:S(2)}) collective-permute-start(bf16[2048,128]{1,0:T(8,128)(2,1)S(1)} %bitcast.34), channel_id=1, source_target_pairs={{0,2},{2,0},{4,6},{6,4},{8,10},{10,8},{12,14},{14,12},{1,3},{3,1},... | collective-permute-start | bytes 1572872 | tf_op jit(solution)/shard_map/ppermute | solution.py:308
  30.4 29.0 %collective-permute-start.2 = (bf16[128,2048]{1,0:T(8,128)(2,1)S(1)}, bf16[128,2048]{1,0:T(8,128)(2,1)S(1)}, u32[]{:S(2)}, u32[]{:S(2)}) collective-permute-start(bf16[128,2048]{1,0:T(8,128)(2,1)S(1)} %bitcast.38), channel_id=1, source_target_pairs={{0,1},{1,0},{2,3},{3,2},{4,5},{5,4},{6,7},{7,6},{8,9},{9,8},{10,11... | collective-permute-start | bytes 1572872 | tf_op jit(solution)/shard_map/ppermute | solution.py:304
  33.3 26.1 %copy-start.17 = (bf16[128,2048]{1,0:T(8,128)(2,1)}, bf16[128,2048]{1,0:T(8,128)(2,1)S(1)}, u32[]{:S(2)}) copy-start(bf16[128,2048]{1,0:T(8,128)(2,1)S(1)} %collective-permute-done.5.refs_9_) | copy-start | bytes 1572868
  33.3 26.1 %collective-permute-start.1 = (bf16[2048,128]{1,0:T(8,128)(2,1)S(1)}, bf16[2048,128]{1,0:T(8,128)(2,1)S(1)}, u32[]{:S(2)}, u32[]{:S(2)}) collective-permute-start(bf16[2048,128]{1,0:T(8,128)(2,1)S(1)} %bitcast.35), channel_id=1, source_target_pairs={{0,1},{1,0},{2,3},{3,2},{4,5},{5,4},{6,7},{7,6},{8,9},{9,8},{10,11... | collective-permute-start | bytes 1572872 | tf_op jit(solution)/shard_map/ppermute | solution.py:304
  38.3 21.1 %copy-start.18 = (bf16[2048,128]{1,0:T(8,128)(2,1)}, bf16[2048,128]{1,0:T(8,128)(2,1)S(1)}, u32[]{:S(2)}) copy-start(bf16[2048,128]{1,0:T(8,128)(2,1)S(1)} %collective-permute-done.refs_4_) | copy-start | bytes 1572868
  38.3 21.1 %collective-permute-start.8 = (bf16[128,2048]{1,0:T(8,128)(2,1)S(1)}, bf16[128,2048]{1,0:T(8,128)(2,1)S(1)}, u32[]{:S(2)}, u32[]{:S(2)}) collective-permute-start(bf16[128,2048]{1,0:T(8,128)(2,1)S(1)} %collective-permute-done.5.refs_9_), channel_id=1, source_target_pairs={{0,1},{1,0},{2,3},{3,2},{4,5},{5,4},{6,7},{7,6},{8,9},{9,8},{10,11... | collective-permute-start | bytes 1572872 | tf_op jit(solution)/shard_map/ppermute | solution.py:304
  44.5 14.9 %copy-start.19 = (bf16[2048,128]{1,0:T(8,128)(2,1)}, bf16[2048,128]{1,0:T(8,128)(2,1)S(1)}, u32[]{:S(2)}) copy-start(bf16[2048,128]{1,0:T(8,128)(2,1)S(1)} %collective-permute-done.3.refs_7_) | copy-start | bytes 1572868
  44.5 14.9 %collective-permute-start.6 = (bf16[2048,128]{1,0:T(8,128)(2,1)S(1)}, bf16[2048,128]{1,0:T(8,128)(2,1)S(1)}, u32[]{:S(2)}, u32[]{:S(2)}) collective-permute-start(bf16[2048,128]{1,0:T(8,128)(2,1)S(1)} %collective-permute-done.3.refs_7_), channel_id=1, source_target_pairs={{0,1},{1,0},{2,3},{3,2},{4,5},{5,4},{6,7},{7,6},{8,9},{9,8},{10,11... | collective-permute-start | bytes 1572872 | tf_op jit(solution)/shard_map/ppermute | solution.py:304
  55.6 3.8 %copy-start.20 = (bf16[2048,128]{1,0:T(8,128)(2,1)}, bf16[2048,128]{1,0:T(8,128)(2,1)S(1)}, u32[]{:S(2)}) copy-start(bf16[2048,128]{1,0:T(8,128)(2,1)S(1)} %collective-permute-done.4.refs_8_) | copy-start | bytes 1572868
  55.6 5.7 %collective-permute-start.7 = (bf16[2048,128]{1,0:T(8,128)(2,1)S(1)}, bf16[2048,128]{1,0:T(8,128)(2,1)}, u32[]{:S(2)}, u32[]{:S(2)}) collective-permute-start(bf16[2048,128]{1,0:T(8,128)(2,1)S(1)} %collective-permute-done.4.refs_8_), channel_id=1, source_target_pairs={{0,1},{1,0},{2,3},{3,2},{4,5},{5,4},{6,7},{7,6},{8,9},{9,8},{10,11... | collective-permute-start | bytes 1572872 | tf_op jit(solution)/shard_map/ppermute | solution.py:304
  59.4 0.8 copy-start.22
  59.4 1.0 copy-start.21
  59.4 1.1 copy-start.23
  60.5 0.8 copy-start.24
  67.8 9.5 %copy-start = (bf16[256,2048]{1,0:T(8,128)(2,1)S(1)}, bf16[256,2048]{1,0:T(8,128)(2,1)}, u32[]{:S(2)}) copy-start(bf16[256,2048]{1,0:T(8,128)(2,1)} %x.2) | copy-start | bytes 3145732
  67.8 9.5 %copy-start.7 = (bf16[2048,32]{0,1:T(8,128)(2,1)S(1)}, bf16[2048,32]{0,1:T(8,128)(2,1)}, u32[]{:S(2)}) copy-start(bf16[2048,32]{0,1:T(8,128)(2,1)} %param.31) | copy-start | bytes 393220
  67.8 9.5 %copy-start.8 = (bf16[2048,32]{0,1:T(8,128)(2,1)S(1)}, bf16[2048,32]{0,1:T(8,128)(2,1)}, u32[]{:S(2)}) copy-start(bf16[2048,32]{0,1:T(8,128)(2,1)} %param.32) | copy-start | bytes 393220
  67.8 9.5 %copy-start.10 = (f32[2048]{0:T(1024)S(1)}, f32[2048]{0:T(1024)}, u32[]{:S(2)}) copy-start(f32[2048]{0:T(1024)} %param.25) | copy-start | bytes 24580
  67.9 38.0 %copy-start.1 = (bf16[128,512]{1,0:T(8,128)(2,1)S(1)}, bf16[128,512]{1,0:T(8,128)(2,1)}, u32[]{:S(2)}) copy-start(bf16[128,512]{1,0:T(8,128)(2,1)} %keys.3) | copy-start | bytes 393220
  67.9 38.0 %copy-start.2 = (bf16[64,2048]{1,0:T(8,128)(2,1)S(1)}, bf16[64,2048]{1,0:T(8,128)(2,1)}, u32[]{:S(2)}) copy-start(bf16[64,2048]{1,0:T(8,128)(2,1)} %mix.1) | copy-start | bytes 786436
  67.9 38.0 %copy-start.3 = (bf16[32,2048]{1,0:T(8,128)(2,1)S(1)}, bf16[32,2048]{1,0:T(8,128)(2,1)}, u32[]{:S(2)}) copy-start(bf16[32,2048]{1,0:T(8,128)(2,1)} %down.1) | copy-start | bytes 393220
  67.9 38.0 %copy-start.4 = (bf16[128,512]{1,0:T(8,128)(2,1)S(1)}, bf16[128,512]{1,0:T(8,128)(2,1)}, u32[]{:S(2)}) copy-start(bf16[128,512]{1,0:T(8,128)(2,1)} %queries.1) | copy-start | bytes 393220
  67.9 38.0 %copy-start.5 = (bf16[256,256]{1,0:T(8,128)(2,1)S(1)}, bf16[256,256]{1,0:T(8,128)(2,1)}, u32[]{:S(2)}) copy-start(bf16[256,256]{1,0:T(8,128)(2,1)} %get-tuple-element.12.w_high) | copy-start | bytes 393220
  67.9 38.0 %copy-start.6 = (bf16[256,256]{1,0:T(8,128)(2,1)S(1)}, bf16[256,256]{1,0:T(8,128)(2,1)}, u32[]{:S(2)}) copy-start(bf16[256,256]{1,0:T(8,128)(2,1)} %get-tuple-element.16.w_low) | copy-start | bytes 393220
  67.9 38.0 %copy-start.9 = (bf16[128,64]{0,1:T(8,128)(2,1)S(1)}, bf16[128,64]{0,1:T(8,128)(2,1)}, u32[]{:S(2)}) copy-start(bf16[128,64]{0,1:T(8,128)(2,1)} %param.19) | copy-start | bytes 49156
  67.9 38.0 %copy-start.11 = (bf16[128,64]{0,1:T(8,128)(2,1)S(1)}, bf16[128,64]{0,1:T(8,128)(2,1)}, u32[]{:S(2)}) copy-start(bf16[128,64]{0,1:T(8,128)(2,1)} %param.20) | copy-start | bytes 49156
  67.9 38.0 %copy-start.12 = (f32[128,2]{0,1:T(2,128)S(1)}, f32[128,2]{0,1:T(2,128)}, u32[]{:S(2)}) copy-start(f32[128,2]{0,1:T(2,128)} %param.21) | copy-start | bytes 3076
  68.0 38.0 %copy-start.13 = (f32[128,2]{0,1:T(2,128)S(1)}, f32[128,2]{0,1:T(2,128)}, u32[]{:S(2)}) copy-start(f32[128,2]{0,1:T(2,128)} %param.22) | copy-start | bytes 3076
  68.0 37.9 %all-to-all-start.1 = ((bf16[32,8,2176]{2,1,0:T(8,128)(2,1)}), bf16[32,8,2176]{2,1,0:T(8,128)(2,1)S(1)}, u32[]{:S(2)}, u32[]{:S(2)}) async-start(bf16[32,8,2176]{2,1,0:T(8,128)(2,1)} %bitcast.28), calls=%async_computation.1 | async-start | bytes 2228224 | tf_op jit(solution)/shard_map/all_to_all | solution.py:300
  108.1 5.6 %collective-permute-start.9 = (bf16[8,24,2048]{2,1,0:T(8,128)(2,1)S(1)}, bf16[8,24,2048]{2,1,0:T(8,128)(2,1)S(1)}, u32[]{:S(2)}, u32[]{:S(2)}) collective-permute-start(bf16[8,24,2048]{2,1,0:T(8,128)(2,1)S(1)} %get-tuple-element.19), channel_id=1, source_target_pairs={{0,1},{1,0},{2,3},{3,2},{4,5},{5,4},{6,7},{7,6},{8,9},{9,8},{10,11... | collective-permute-start | bytes 2359304 | tf_op jit(solution)/shard_map/ppermute | solution.py:304
  166.2 7.1 %collective-permute-start.10 = (bf16[8,24,2048]{2,1,0:T(8,128)(2,1)S(1)}, bf16[8,24,2048]{2,1,0:T(8,128)(2,1)S(1)}, u32[]{:S(2)}, u32[]{:S(2)}) collective-permute-start(bf16[8,24,2048]{2,1,0:T(8,128)(2,1)S(1)} %all_to_all.21.mine), channel_id=1, source_target_pairs={{0,1},{1,0},{2,3},{3,2},{4,5},{5,4},{6,7},{7,6},{8,9},{9,8},{10,11... | collective-permute-start | bytes 2359304 | tf_op jit(solution)/shard_map/ppermute | solution.py:304

commit v4 on v3

--- a/solution.py
+++ b/solution.py
@@ -35,13 +35,14 @@
 TN = (((0,), (0,)), ((), ()))
 
 
-def call(body, arrays, ins, outs, spaces, scratch, flops, limit=16 << 20):
+def call(body, arrays, ins, outs, spaces, scratch, flops, limit=16 << 20, aliases=None):
     return pl.pallas_call(
         body,
         out_shape=outs,
         in_specs=ins,
         out_specs=spaces,
         scratch_shapes=scratch,
+        input_output_aliases=aliases or {},
         compiler_params=pltpu.CompilerParams(vmem_limit_bytes=limit),
         cost_estimate=pl.CostEstimate(flops=flops, bytes_accessed=1 << 20, transcendentals=0),
     )(*arrays)
@@ -182,25 +183,34 @@
     fetches = []
     for k in range(4):
         targets = (wide.at[k, :, 0:128], wide.at[k, :, 128:256], tall.at[128 * k : 128 * (k + 1), :])
-        for j in range(3):
-            fetches.append(pltpu.make_async_copy(weights[3 * k + j], targets[j], fetch.at[3 * k + j]))
-            fetches[-1].start()
+        fetches.append(
+            [
+                pltpu.make_async_copy(weights[3 * k + j], targets[j], fetch.at[3 * k + j])
+                for j in range(3)
+            ]
+        )
+    for copy in fetches[0][0:2] + fetches[1][0:2]:
+        copy.start()
     first.wait()
+    for copy in fetches[2][0:2] + fetches[3][0:2]:
+        copy.start()
     states[...] = taken[:, D:WIDE].astype(f32).reshape(N_EP, 8, 128)
     prefix(states)
     staged[:, D:WIDE] = states[...].reshape(ROWS, 128).astype(bf16)
     copies = [pltpu.make_async_copy(staged.at[:, D:WIDE], out.at[:, D:WIDE], sem.at[0])]
     copies[0].start()
+    for k in range(4):
+        fetches[k][2].start()
     rows = taken[:, 0:D]
     acts = []
     for k in range(4):
-        fetches[3 * k].wait()
-        fetches[3 * k + 1].wait()
+        fetches[k][0].wait()
+        fetches[k][1].wait()
         both = jnp.dot(rows, wide[k], preferred_element_type=f32)
         gated, lifted = both[:, 0:128], both[:, 128:256]
         acts.append((gated / (1.0 + jnp.exp(-gated)) * lifted).astype(bf16))
     for k in range(4):
-        fetches[3 * k + 2].wait()
+        fetches[k][2].wait()
     act = jnp.concatenate(acts, axis=1)
     for k in range(4):
         at = slice(512 * k, 512 * (k + 1))
@@ -218,9 +228,19 @@
     act[...] = (gated / (1.0 + jnp.exp(-gated)) * lifted).astype(bf16)
 
 
-def combine_kernel(
+def routed(back, w_high, w_low, act, down, half):
+    at = pl.ds(pl.multiple_of(half * (TOKENS // 2), TOKENS // 2), TOKENS // 2)
+    rows = back[:, 0:D]
+    return (
+        lax.dot_general(w_high[:, at], rows, TN, preferred_element_type=f32)
+        + lax.dot_general(w_low[:, at], rows, TN, preferred_element_type=f32)
+        + jnp.dot(act[at, :], down[...], preferred_element_type=f32)
+    )
+
+
+def give_kernel(
     back, w_high, w_low, act, down, queries, keys, values, out_gate, input_gate, forget_gate, mix,
-    keep, give, states, mixed, total,
+    give, kept, states, mixed, total,
 ):
     core = lax.axis_index("c")
     team = lax.axis_index("y") // 4
@@ -259,41 +279,48 @@
     hidden = numerator / jnp.maximum(jnp.abs(denominator), den_floor)
     gated = (hidden / (1.0 + jnp.exp(-out_gate[...].astype(f32)))).astype(bf16)
     mixed[...] = lax.dot_general(gated, mix[...], TN, preferred_element_type=f32)
-    rows = back[:, 0:D]
-    total[...] = (
-        lax.dot_general(w_high[...], rows, TN, preferred_element_type=f32)
-        + lax.dot_general(w_low[...], rows, TN, preferred_element_type=f32)
-        + jnp.dot(act[...], down[...], preferred_element_type=f32)
-    )
-    for target, first in ((keep, core), (give, 1 - core)):
-        for k in range(N_Y):
-            start = pl.multiple_of(first * (TOKENS // 2) + k * E_ROWS, E_ROWS)
-            target[k, 0:E_ROWS, :] = total[pl.ds(start, E_ROWS), :].astype(target.dtype)
-            start = pl.multiple_of(first * (BLOCK // 2) + k * M_ROWS, M_ROWS)
-            target[k, E_ROWS:PIECE, :] = mixed[pl.ds(start, M_ROWS), :].astype(target.dtype)
-
-
-def place_kernel(mine, other, mixer, expert, sem):
-    core = lax.axis_index("c")
+    total[...] = routed(back, w_high, w_low, act, down, 1 - core)
+    for k in range(N_Y):
+        give[k, 0:E_ROWS, :] = total[E_ROWS * k : E_ROWS * (k + 1), :].astype(bf16)
+        start = pl.multiple_of((1 - core) * (BLOCK // 2) + k * M_ROWS, M_ROWS)
+        give[k, E_ROWS:PIECE, :] = mixed[pl.ds(start, M_ROWS), :].astype(bf16)
+    kept[...] = mixed[pl.ds(pl.multiple_of(core * (BLOCK // 2), BLOCK // 2), BLOCK // 2), :]
+
+
+def keep_kernel(back, w_high, w_low, act, down, kept, keep, total):
+    total[...] = routed(back, w_high, w_low, act, down, lax.axis_index("c"))
+    for k in range(N_Y):
+        keep[k, 0:E_ROWS, :] = total[E_ROWS * k : E_ROWS * (k + 1), :]
+        keep[k, E_ROWS:PIECE, :] = kept[M_ROWS * k : M_ROWS * (k + 1), :]
+
+
+def put(source, half, mixer, expert, sem):
     copies = []
-    for half, (source, first) in enumerate(((mine, core), (other, 1 - core))):
-        for k in range(N_Y):
-            start = pl.multiple_of(first * (TOKENS // 2) + k * E_ROWS, E_ROWS)
-            copies.append(
-                pltpu.make_async_copy(
-                    source.at[k, 0:E_ROWS, :], expert.at[pl.ds(start, E_ROWS), :], sem.at[half, k, 0]
-                )
+    for k in range(N_Y):
+        start = pl.multiple_of(half * (TOKENS // 2) + k * E_ROWS, E_ROWS)
+        copies.append(
+            pltpu.make_async_copy(
+                source.at[k, 0:E_ROWS, :], expert.at[pl.ds(start, E_ROWS), :], sem.at[k, 0]
             )
-            start = pl.multiple_of(first * (BLOCK // 2) + k * M_ROWS, M_ROWS)
-            copies.append(
-                pltpu.make_async_copy(
-                    source.at[k, E_ROWS:PIECE, :], mixer.at[pl.ds(start, M_ROWS), :], sem.at[half, k, 1]
-                )
+        )
+        start = pl.multiple_of(half * (BLOCK // 2) + k * M_ROWS, M_ROWS)
+        copies.append(
+            pltpu.make_async_copy(
+                source.at[k, E_ROWS:PIECE, :], mixer.at[pl.ds(start, M_ROWS), :], sem.at[k, 1]
             )
+        )
     for copy in copies:
         copy.start()
     for copy in copies:
         copy.wait()
+
+
+def place_kernel(mine, mixer, expert, sem):
+    put(mine, lax.axis_index("c"), mixer, expert, sem)
+
+
+def fill_kernel(other, mixer_in, expert_in, mixer, expert, sem):
+    put(other, 1 - lax.axis_index("c"), mixer, expert, sem)
 
 
 def exchange(array, axis):
@@ -360,7 +387,7 @@
         WHOLE,
     )
     arrived = exchange(send.reshape(N_EP, SLOTS, WIDE), EP).reshape(ROWS, WIDE)
-    near_up = reach_over(own[1])
+    near_up = reach_over(after(own[1], w_high))
     near_down = reach_over(after(own[2], w_high))
     near = (near_gate, near_up, near_down)
     beside = tuple(swap(after(array, w_high)) for array in own)
@@ -393,8 +420,8 @@
         WHOLE,
     )
     back = exchange(results.reshape(N_EP, SLOTS, WIDE), EP).reshape(ROWS, WIDE)
-    keep, give = call(
-        combine_kernel,
+    give, kept = call(
+        give_kernel,
         (
             back,
             w_high,
@@ -410,27 +437,41 @@
             mix_weight,
         ),
         [VMEM] * 12,
-        [shape((N_Y, PIECE, D), f32), shape((N_Y, PIECE, D), bf16)],
+        [shape((N_Y, PIECE, D), bf16), shape((BLOCK // 2, D), f32)],
         [VMEM] * 2,
         [
             pltpu.VMEM((N_EP, 8, 128), f32),
             pltpu.VMEM((BLOCK, D), f32),
-            pltpu.VMEM((TOKENS, D), f32),
+            pltpu.VMEM((TOKENS // 2, D), f32),
         ],
+        1 << 28,
+    )
+    (keep,) = call(
+        keep_kernel,
+        (back, w_high, w_low, act, shared_down, kept),
+        [VMEM] * 6,
+        [shape((N_Y, PIECE, D), f32)],
+        [VMEM],
+        [pltpu.VMEM((TOKENS // 2, D), f32)],
         1 << 28,
     )
     half = (keep + swap(give).astype(f32)).astype(bf16)
     piece = exchange(half, "y").astype(f32).sum(axis=0).astype(bf16)
     mine = exchange(jnp.broadcast_to(piece[None], (N_Y, PIECE, D)), "y")
     other = swap(mine)
+    outs = [shape((BLOCK, D), bf16), shape((TOKENS, D), bf16)]
+    mixer, expert = call(
+        place_kernel, (mine,), [VMEM], outs, [HBM] * 2, [dma((N_Y, 2))], 1 << 24
+    )
     return call(
-        place_kernel,
-        (mine, other),
-        [VMEM] * 2,
-        [shape((BLOCK, D), bf16), shape((TOKENS, D), bf16)],
+        fill_kernel,
+        (other, mixer, expert),
+        [VMEM] + [HBM] * 2,
+        outs,
         [HBM] * 2,
-        [dma((2, N_Y, 2))],
-        1 << 20,
+        [dma((N_Y, 2))],
+        1 << 24,
+        aliases={1: 0, 2: 1},
     )
 
 

time: 175 us -> 175 us (level)
    pallas_call x5 -> x7, Pallas kernels: 15.1 us -> 15.7 us  [call(): pl.pallas_call(body, out_shape=outs, in_specs=ins, out_specs=spaces, scra...]
where the time goes in v4:
time: 175 us; the launch traced here: 174 us
  starting transfers between devices  61.9 us (35%)
  blocking collectives  52.1 us (30%)
  waiting for transfers between devices  40.5 us (23%)
  Pallas kernels  15.7 us (9%)
  local copies, waits for them, and re-layouts  2.09 us (1%)
    all_to_all x2, blocking collectives, exchange(): return lax.all_to_all(array, axis, split_axis=0, concat_axis=0, tiled=True)  52.1 us
    ppermute x8, starting transfers between devices, swap(): return lax.ppermute(array, 'c', [(0, 1), (1, 0)])  30.2 us
    all_to_all x2, waiting for transfers between devices, exchange(): return lax.all_to_all(array, axis, split_axis=0, concat_axis=0, tiled=True)  27.6 us
    all_to_all x2, starting transfers between devices, exchange(): return lax.all_to_all(array, axis, split_axis=0, concat_axis=0, tiled=True)  23.3 us
    pallas_call x7, Pallas kernels, call(): pl.pallas_call(body, out_shape=outs, in_specs=ins, out_specs=spaces, scra...  15.7 us
    ppermute x3, waiting for transfers between devices, reach_over(): return lax.ppermute(array, 'y', [(k, k ^ 1) for k in range(N_Y)])  10.7 us
    ppermute x3, starting transfers between devices, reach_over(): return lax.ppermute(array, 'y', [(k, k ^ 1) for k in range(N_Y)])  8.49 us
  transfers between devices with their start and end apart: 13, of which 6 were waited for; matrix products, arithmetic and copies ran while one was open for 0% of the time, Pallas kernels for 1%

profile of v4, /device:TPU:1, one launch (start us, length us, event | category | flops | bytes accessed | tf_op | source)
XLA Modules:
  0.0 173.8 jit_solution(3683077669591965242)
XLA Ops:
  0.6 4.1 %shard_map.176 = (bf16[256,2176]{1,0:T(8,128)(2,1)}, bf16[256,256]{1,0:T(8,128)(2,1)}, bf16[256,256]{1,0:T(8,128)(2,1)}) custom-call(bf16[256,2048]{1,0:T(8,128)(2,1)} %x.2, f32[1,2048]{1,0:T(1,128)} %bitcast.22, s32[4,256]{1,0:T(4,128)} %bitcast.40, f32[4,256]{1,0:T(4,128)} %bitcast.41, bf16[128,512]{1,0:T(8,128)(2,1)} %keys.3, bf16[64,128]{1,0:T(8,128)(2,1)} %bitcast.20, ...), custom_call_target="tpu_custom_call" | custom-call | flops 268435456 | bytes 1048576 | tf_op jit(solution)/shard_map/pallas_call | solution.py:39
  4.7 0.0 copy-start.15
  4.7 0.0 copy-start.16
  4.7 0.0 copy-start.14
  4.8 14.0 %all-to-all-start = ((bf16[32,8,2176]{2,1,0:T(8,128)(2,1)}), bf16[32,8,2176]{2,1,0:T(8,128)(2,1)}, u32[]{:S(2)}, u32[]{:S(2)}) async-start(bf16[32,8,2176]{2,1,0:T(8,128)(2,1)} %bitcast.30), calls=%async_computation | async-start | bytes 2228224 | tf_op jit(solution)/shard_map/all_to_all | solution.py:327
  18.7 3.2 %collective-permute-start.4 = (bf16[2048,128]{1,0:T(8,128)(2,1)S(1)}, bf16[2048,128]{1,0:T(8,128)(2,1)S(1)}, u32[]{:S(2)}, u32[]{:S(2)}) collective-permute-start(bf16[2048,128]{1,0:T(8,128)(2,1)S(1)} %bitcast.35), channel_id=1, source_target_pairs={{0,2},{2,0},{4,6},{6,4},{8,10},{10,8},{12,14},{14,12},{1,3},{3,1},... | collective-permute-start | bytes 1572872 | tf_op jit(solution)/shard_map/ppermute | solution.py:335
  22.0 2.1 %collective-permute-start.5 = (bf16[128,2048]{1,0:T(8,128)(2,1)S(1)}, bf16[128,2048]{1,0:T(8,128)(2,1)S(1)}, u32[]{:S(2)}, u32[]{:S(2)}) collective-permute-start(bf16[128,2048]{1,0:T(8,128)(2,1)S(1)} %bitcast.38), channel_id=1, source_target_pairs={{0,2},{2,0},{4,6},{6,4},{8,10},{10,8},{12,14},{14,12},{1,3},{3,1},... | collective-permute-start | bytes 1572872 | tf_op jit(solution)/shard_map/ppermute | solution.py:335
  24.1 3.4 %collective-permute-start = (bf16[2048,128]{1,0:T(8,128)(2,1)S(1)}, bf16[2048,128]{1,0:T(8,128)(2,1)S(1)}, u32[]{:S(2)}, u32[]{:S(2)}) collective-permute-start(bf16[2048,128]{1,0:T(8,128)(2,1)S(1)} %bitcast.32), channel_id=1, source_target_pairs={{0,1},{1,0},{2,3},{3,2},{4,5},{5,4},{6,7},{7,6},{8,9},{9,8},{10,11... | collective-permute-start | bytes 1572872 | tf_op jit(solution)/shard_map/ppermute | solution.py:331
  27.5 3.2 %collective-permute-start.3 = (bf16[2048,128]{1,0:T(8,128)(2,1)S(1)}, bf16[2048,128]{1,0:T(8,128)(2,1)S(1)}, u32[]{:S(2)}, u32[]{:S(2)}) collective-permute-start(bf16[2048,128]{1,0:T(8,128)(2,1)S(1)} %bitcast.33), channel_id=1, source_target_pairs={{0,2},{2,0},{4,6},{6,4},{8,10},{10,8},{12,14},{14,12},{1,3},{3,1},... | collective-permute-start | bytes 1572872 | tf_op jit(solution)/shard_map/ppermute | solution.py:335
  30.7 2.2 %collective-permute-start.1 = (bf16[2048,128]{1,0:T(8,128)(2,1)S(1)}, bf16[2048,128]{1,0:T(8,128)(2,1)S(1)}, u32[]{:S(2)}, u32[]{:S(2)}) collective-permute-start(bf16[2048,128]{1,0:T(8,128)(2,1)S(1)} %bitcast.36), channel_id=1, source_target_pairs={{0,1},{1,0},{2,3},{3,2},{4,5},{5,4},{6,7},{7,6},{8,9},{9,8},{10,11... | collective-permute-start | bytes 1572872 | tf_op jit(solution)/shard_map/ppermute | solution.py:331
  32.9 0.4 collective-permute-done.4.refs_8_
  33.3 5.0 %collective-permute-start.2 = (bf16[128,2048]{1,0:T(8,128)(2,1)S(1)}, bf16[128,2048]{1,0:T(8,128)(2,1)S(1)}, u32[]{:S(2)}, u32[]{:S(2)}) collective-permute-start(bf16[128,2048]{1,0:T(8,128)(2,1)S(1)} %bitcast.39), channel_id=1, source_target_pairs={{0,1},{1,0},{2,3},{3,2},{4,5},{5,4},{6,7},{7,6},{8,9},{9,8},{10,11... | collective-permute-start | bytes 1572872 | tf_op jit(solution)/shard_map/ppermute | solution.py:331
  38.3 6.2 %collective-permute-done.5.refs_9_ = bf16[128,2048]{1,0:T(8,128)(2,1)S(1)} collective-permute-done((bf16[128,2048]{1,0:T(8,128)(2,1)S(1)}, bf16[128,2048]{1,0:T(8,128)(2,1)S(1)}, u32[]{:S(2)}, u32[]{:S(2)}) %collective-permute-start.5) | collective-permute-done | bytes 524320 | tf_op jit(solution)/shard_map/ppermute | solution.py:335
  44.5 5.0 %collective-permute-start.7 = (bf16[2048,128]{1,0:T(8,128)(2,1)S(1)}, bf16[2048,128]{1,0:T(8,128)(2,1)S(1)}, u32[]{:S(2)}, u32[]{:S(2)}) collective-permute-start(bf16[2048,128]{1,0:T(8,128)(2,1)S(1)} %collective-permute-done.4.refs_8_), channel_id=1, source_target_pairs={{0,1},{1,0},{2,3},{3,2},{4,5},{5,4},{6,7},{7,6},{8,9},{9,8},{10,11... | collective-permute-start | bytes 1572872 | tf_op jit(solution)/shard_map/ppermute | solution.py:331
  49.5 0.0 copy-start.19
  49.5 1.9 %collective-permute-start.8 = (bf16[128,2048]{1,0:T(8,128)(2,1)S(1)}, bf16[128,2048]{1,0:T(8,128)(2,1)S(1)}, u32[]{:S(2)}, u32[]{:S(2)}) collective-permute-start(bf16[128,2048]{1,0:T(8,128)(2,1)S(1)} %collective-permute-done.5.refs_9_), channel_id=1, source_target_pairs={{0,1},{1,0},{2,3},{3,2},{4,5},{5,4},{6,7},{7,6},{8,9},{9,8},{10,11... | collective-permute-start | bytes 1572872 | tf_op jit(solution)/shard_map/ppermute | solution.py:331
  51.5 4.2 %collective-permute-done.3.refs_7_ = bf16[2048,128]{1,0:T(8,128)(2,1)S(1)} collective-permute-done((bf16[2048,128]{1,0:T(8,128)(2,1)S(1)}, bf16[2048,128]{1,0:T(8,128)(2,1)S(1)}, u32[]{:S(2)}, u32[]{:S(2)}) %collective-permute-start.3) | collective-permute-done | bytes 524320 | tf_op jit(solution)/shard_map/ppermute | solution.py:335
  55.6 3.7 %collective-permute-start.6 = (bf16[2048,128]{1,0:T(8,128)(2,1)S(1)}, bf16[2048,128]{1,0:T(8,128)(2,1)}, u32[]{:S(2)}, u32[]{:S(2)}) collective-permute-start(bf16[2048,128]{1,0:T(8,128)(2,1)S(1)} %collective-permute-done.3.refs_7_), channel_id=1, source_target_pairs={{0,1},{1,0},{2,3},{3,2},{4,5},{5,4},{6,7},{7,6},{8,9},{9,8},{10,11... | collective-permute-start | bytes 1572872 | tf_op jit(solution)/shard_map/ppermute | solution.py:331
  59.4 0.0 copy-start.21
  59.5 0.7 copy-done.21
  60.2 0.2 copy-done.22
  60.3 0.2 copy-done.23
  60.5 0.8 copy-done.24
  61.4 6.5 %shard_map.177 = bf16[256,2176]{1,0:T(8,128)(2,1)} custom-call(bf16[256,2176]{1,0:T(8,128)(2,1)} %bitcast.7.refs_0_, bf16[2048,128]{1,0:T(8,128)(2,1)} %bitcast.31, bf16[2048,128]{1,0:T(8,128)(2,1)} %bitcast.34, bf16[128,2048]{1,0:T(8,128)(2,1)} %bitcast.37, bf16[2048,128]{1,0:T(8,128)(2,1)} %copy-done.19, bf16[2048,128]{1,0:T(8,128)(2,1)} %copy-done.21, ...), custom_call_target="tpu_custom_call" | custom-call | flops 2147483648 | bytes 1048576 | tf_op jit(solution)/shard_map/pallas_call | solution.py:39
  67.9 0.0 copy-start
  67.9 0.0 copy-start.7
  67.9 0.0 copy-start.8
  67.9 0.0 copy-start.1
  67.9 0.0 copy-start.2
  68.0 0.0 copy-start.6
  68.0 0.0 copy-start.9
  68.0 0.0 copy-start.13
  68.0 9.3 %all-to-all-start.1 = ((bf16[32,8,2176]{2,1,0:T(8,128)(2,1)}), bf16[32,8,2176]{2,1,0:T(8,128)(2,1)S(1)}, u32[]{:S(2)}, u32[]{:S(2)}) async-start(bf16[32,8,2176]{2,1,0:T(8,128)(2,1)} %bitcast.29), calls=%async_computation.1 | async-start | bytes 2228224 | tf_op jit(solution)/shard_map/all_to_all | solution.py:327
  77.4 0.9 shard_map.178.act
  78.3 27.6 %all-to-all-done.1 = bf16[32,8,2176]{2,1,0:T(8,128)(2,1)S(1)} async-done(((bf16[32,8,2176]{2,1,0:T(8,128)(2,1)}), bf16[32,8,2176]{2,1,0:T(8,128)(2,1)S(1)}, u32[]{:S(2)}, u32[]{:S(2)}) %all-to-all-start.1) | async-done | bytes 1114144 | tf_op jit(solution)/shard_map/all_to_all | solution.py:327
  106.0 1.6 shard_map.179
  107.6 3.7 %collective-permute-start.9 = (bf16[8,24,2048]{2,1,0:T(8,128)(2,1)S(1)}, bf16[8,24,2048]{2,1,0:T(8,128)(2,1)S(1)}, u32[]{:S(2)}, u32[]{:S(2)}) collective-permute-start(bf16[8,24,2048]{2,1,0:T(8,128)(2,1)S(1)} %get-tuple-element.21), channel_id=1, source_target_pairs={{0,1},{1,0},{2,3},{3,2},{4,5},{5,4},{6,7},{7,6},{8,9},{9,8},{10,11... | collective-permute-start | bytes 2359304 | tf_op jit(solution)/shard_map/ppermute | solution.py:331
  111.3 0.6 shard_map.180
  111.9 1.3 collective-permute-done.9
  113.2 0.2 add_convert_fusion
  113.4 29.0 %all_to_all.20 = bf16[8,24,2048]{2,1,0:T(8,128)(2,1)S(1)} all-to-all(bf16[8,24,2048]{2,1,0:T(8,128)(2,1)S(1)} %add_convert_fusion), channel_id=1, replica_groups=mesh['z'=8,'x'=4,'y'=8,'c'=2] {'y'}, dimensions={0} | all-to-all | bytes 1572864 | tf_op jit(solution)/shard_map/all_to_all | solution.py:327
  142.3 0.1 reduce_sum.12
  142.5 0.1 broadcast_in_dim.5
  142.5 23.1 %all_to_all.21.mine = bf16[8,24,2048]{2,1,0:T(8,128)(2,1)S(1)} all-to-all(bf16[8,24,2048]{2,1,0:T(8,128)(2,1)S(1)} %broadcast_in_dim.5), channel_id=1, replica_groups=mesh['z'=8,'x'=4,'y'=8,'c'=2] {'y'}, dimensions={0} | all-to-all | bytes 1572864 | tf_op jit(solution)/shard_map/all_to_all | solution.py:327
  165.7 5.2 %collective-permute-start.10 = (bf16[8,24,2048]{2,1,0:T(8,128)(2,1)S(1)}, bf16[8,24,2048]{2,1,0:T(8,128)(2,1)S(1)}, u32[]{:S(2)}, u32[]{:S(2)}) collective-permute-start(bf16[8,24,2048]{2,1,0:T(8,128)(2,1)S(1)} %all_to_all.21.mine), channel_id=1, source_target_pairs={{0,1},{1,0},{2,3},{3,2},{4,5},{5,4},{6,7},{7,6},{8,9},{9,8},{10,11... | collective-permute-start | bytes 2359304 | tf_op jit(solution)/shard_map/ppermute | solution.py:331
  170.9 1.0 shard_map.181
  171.9 0.9 collective-permute-done.10.other
  172.8 1.0 shard_map.182
  (40 shorter events, 0.1 us)
Async XLA Ops:
  4.7 14.0 %copy-start.15 = (bf16[1,2048,128]{2,1,0:T(8,128)(2,1)S(1)}, bf16[1,2048,128]{2,1,0:T(8,128)(2,1)}, u32[]{:S(2)}) copy-start(bf16[1,2048,128]{2,1,0:T(8,128)(2,1)} %param.29) | copy-start | bytes 1572868
  4.7 17.2 %copy-start.16 = (bf16[1,128,2048]{2,1,0:T(8,128)(2,1)S(1)}, bf16[1,128,2048]{2,1,0:T(8,128)(2,1)}, u32[]{:S(2)}) copy-start(bf16[1,128,2048]{2,1,0:T(8,128)(2,1)} %param.30) | copy-start | bytes 1572868
  4.7 19.3 %copy-start.14 = (bf16[1,2048,128]{2,1,0:T(8,128)(2,1)S(1)}, bf16[1,2048,128]{2,1,0:T(8,128)(2,1)}, u32[]{:S(2)}) copy-start(bf16[1,2048,128]{2,1,0:T(8,128)(2,1)} %param.28) | copy-start | bytes 1572868
  4.8 56.6 %all-to-all-start = ((bf16[32,8,2176]{2,1,0:T(8,128)(2,1)}), bf16[32,8,2176]{2,1,0:T(8,128)(2,1)}, u32[]{:S(2)}, u32[]{:S(2)}) async-start(bf16[32,8,2176]{2,1,0:T(8,128)(2,1)} %bitcast.30), calls=%async_computation | async-start | bytes 2228224 | tf_op jit(solution)/shard_map/all_to_all | solution.py:327
  18.7 14.5 %collective-permute-start.4 = (bf16[2048,128]{1,0:T(8,128)(2,1)S(1)}, bf16[2048,128]{1,0:T(8,128)(2,1)S(1)}, u32[]{:S(2)}, u32[]{:S(2)}) collective-permute-start(bf16[2048,128]{1,0:T(8,128)(2,1)S(1)} %bitcast.35), channel_id=1, source_target_pairs={{0,2},{2,0},{4,6},{6,4},{8,10},{10,8},{12,14},{14,12},{1,3},{3,1},... | collective-permute-start | bytes 1572872 | tf_op jit(solution)/shard_map/ppermute | solution.py:335
  22.0 22.5 %collective-permute-start.5 = (bf16[128,2048]{1,0:T(8,128)(2,1)S(1)}, bf16[128,2048]{1,0:T(8,128)(2,1)S(1)}, u32[]{:S(2)}, u32[]{:S(2)}) collective-permute-start(bf16[128,2048]{1,0:T(8,128)(2,1)S(1)} %bitcast.38), channel_id=1, source_target_pairs={{0,2},{2,0},{4,6},{6,4},{8,10},{10,8},{12,14},{14,12},{1,3},{3,1},... | collective-permute-start | bytes 1572872 | tf_op jit(solution)/shard_map/ppermute | solution.py:335
  24.1 25.5 %collective-permute-start = (bf16[2048,128]{1,0:T(8,128)(2,1)S(1)}, bf16[2048,128]{1,0:T(8,128)(2,1)S(1)}, u32[]{:S(2)}, u32[]{:S(2)}) collective-permute-start(bf16[2048,128]{1,0:T(8,128)(2,1)S(1)} %bitcast.32), channel_id=1, source_target_pairs={{0,1},{1,0},{2,3},{3,2},{4,5},{5,4},{6,7},{7,6},{8,9},{9,8},{10,11... | collective-permute-start | bytes 1572872 | tf_op jit(solution)/shard_map/ppermute | solution.py:331
  27.5 28.1 %collective-permute-start.3 = (bf16[2048,128]{1,0:T(8,128)(2,1)S(1)}, bf16[2048,128]{1,0:T(8,128)(2,1)S(1)}, u32[]{:S(2)}, u32[]{:S(2)}) collective-permute-start(bf16[2048,128]{1,0:T(8,128)(2,1)S(1)} %bitcast.33), channel_id=1, source_target_pairs={{0,2},{2,0},{4,6},{6,4},{8,10},{10,8},{12,14},{14,12},{1,3},{3,1},... | collective-permute-start | bytes 1572872 | tf_op jit(solution)/shard_map/ppermute | solution.py:335
  30.7 28.7 %collective-permute-start.1 = (bf16[2048,128]{1,0:T(8,128)(2,1)S(1)}, bf16[2048,128]{1,0:T(8,128)(2,1)S(1)}, u32[]{:S(2)}, u32[]{:S(2)}) collective-permute-start(bf16[2048,128]{1,0:T(8,128)(2,1)S(1)} %bitcast.36), channel_id=1, source_target_pairs={{0,1},{1,0},{2,3},{3,2},{4,5},{5,4},{6,7},{7,6},{8,9},{9,8},{10,11... | collective-permute-start | bytes 1572872 | tf_op jit(solution)/shard_map/ppermute | solution.py:331
  33.3 26.1 %copy-start.17 = (bf16[2048,128]{1,0:T(8,128)(2,1)}, bf16[2048,128]{1,0:T(8,128)(2,1)S(1)}, u32[]{:S(2)}) copy-start(bf16[2048,128]{1,0:T(8,128)(2,1)S(1)} %collective-permute-done.4.refs_8_) | copy-start | bytes 1572868
  33.3 26.1 %collective-permute-start.2 = (bf16[128,2048]{1,0:T(8,128)(2,1)S(1)}, bf16[128,2048]{1,0:T(8,128)(2,1)S(1)}, u32[]{:S(2)}, u32[]{:S(2)}) collective-permute-start(bf16[128,2048]{1,0:T(8,128)(2,1)S(1)} %bitcast.39), channel_id=1, source_target_pairs={{0,1},{1,0},{2,3},{3,2},{4,5},{5,4},{6,7},{7,6},{8,9},{9,8},{10,11... | collective-permute-start | bytes 1572872 | tf_op jit(solution)/shard_map/ppermute | solution.py:331
  44.5 14.9 %copy-start.18 = (bf16[128,2048]{1,0:T(8,128)(2,1)}, bf16[128,2048]{1,0:T(8,128)(2,1)S(1)}, u32[]{:S(2)}) copy-start(bf16[128,2048]{1,0:T(8,128)(2,1)S(1)} %collective-permute-done.5.refs_9_) | copy-start | bytes 1572868
  44.5 14.9 %collective-permute-start.7 = (bf16[2048,128]{1,0:T(8,128)(2,1)S(1)}, bf16[2048,128]{1,0:T(8,128)(2,1)S(1)}, u32[]{:S(2)}, u32[]{:S(2)}) collective-permute-start(bf16[2048,128]{1,0:T(8,128)(2,1)S(1)} %collective-permute-done.4.refs_8_), channel_id=1, source_target_pairs={{0,1},{1,0},{2,3},{3,2},{4,5},{5,4},{6,7},{7,6},{8,9},{9,8},{10,11... | collective-permute-start | bytes 1572872 | tf_op jit(solution)/shard_map/ppermute | solution.py:331
  49.5 9.9 %copy-start.19 = (bf16[2048,128]{1,0:T(8,128)(2,1)}, bf16[2048,128]{1,0:T(8,128)(2,1)S(1)}, u32[]{:S(2)}) copy-start(bf16[2048,128]{1,0:T(8,128)(2,1)S(1)} %collective-permute-done.refs_4_) | copy-start | bytes 1572868
  49.5 9.9 %collective-permute-start.8 = (bf16[128,2048]{1,0:T(8,128)(2,1)S(1)}, bf16[128,2048]{1,0:T(8,128)(2,1)S(1)}, u32[]{:S(2)}, u32[]{:S(2)}) collective-permute-start(bf16[128,2048]{1,0:T(8,128)(2,1)S(1)} %collective-permute-done.5.refs_9_), channel_id=1, source_target_pairs={{0,1},{1,0},{2,3},{3,2},{4,5},{5,4},{6,7},{7,6},{8,9},{9,8},{10,11... | collective-permute-start | bytes 1572872 | tf_op jit(solution)/shard_map/ppermute | solution.py:331
  55.6 3.8 %copy-start.20 = (bf16[2048,128]{1,0:T(8,128)(2,1)}, bf16[2048,128]{1,0:T(8,128)(2,1)S(1)}, u32[]{:S(2)}) copy-start(bf16[2048,128]{1,0:T(8,128)(2,1)S(1)} %collective-permute-done.3.refs_7_) | copy-start | bytes 1572868
  55.6 5.7 %collective-permute-start.6 = (bf16[2048,128]{1,0:T(8,128)(2,1)S(1)}, bf16[2048,128]{1,0:T(8,128)(2,1)}, u32[]{:S(2)}, u32[]{:S(2)}) collective-permute-start(bf16[2048,128]{1,0:T(8,128)(2,1)S(1)} %collective-permute-done.3.refs_7_), channel_id=1, source_target_pairs={{0,1},{1,0},{2,3},{3,2},{4,5},{5,4},{6,7},{7,6},{8,9},{9,8},{10,11... | collective-permute-start | bytes 1572872 | tf_op jit(solution)/shard_map/ppermute | solution.py:331
  59.4 0.8 copy-start.21
  59.4 1.0 copy-start.22
  59.4 1.1 copy-start.23
  60.5 0.8 copy-start.24
  67.9 9.5 %copy-start = (bf16[256,2048]{1,0:T(8,128)(2,1)S(1)}, bf16[256,2048]{1,0:T(8,128)(2,1)}, u32[]{:S(2)}) copy-start(bf16[256,2048]{1,0:T(8,128)(2,1)} %x.2) | copy-start | bytes 3145732
  67.9 9.5 %copy-start.7 = (bf16[2048,32]{0,1:T(8,128)(2,1)S(1)}, bf16[2048,32]{0,1:T(8,128)(2,1)}, u32[]{:S(2)}) copy-start(bf16[2048,32]{0,1:T(8,128)(2,1)} %param.31) | copy-start | bytes 393220
  67.9 9.5 %copy-start.8 = (bf16[2048,32]{0,1:T(8,128)(2,1)S(1)}, bf16[2048,32]{0,1:T(8,128)(2,1)}, u32[]{:S(2)}) copy-start(bf16[2048,32]{0,1:T(8,128)(2,1)} %param.32) | copy-start | bytes 393220
  67.9 9.5 %copy-start.10 = (f32[2048]{0:T(1024)S(1)}, f32[2048]{0:T(1024)}, u32[]{:S(2)}) copy-start(f32[2048]{0:T(1024)} %param.25) | copy-start | bytes 24580
  67.9 38.0 %copy-start.1 = (bf16[128,512]{1,0:T(8,128)(2,1)S(1)}, bf16[128,512]{1,0:T(8,128)(2,1)}, u32[]{:S(2)}) copy-start(bf16[128,512]{1,0:T(8,128)(2,1)} %keys.3) | copy-start | bytes 393220
  67.9 38.0 %copy-start.2 = (bf16[32,2048]{1,0:T(8,128)(2,1)S(1)}, bf16[32,2048]{1,0:T(8,128)(2,1)}, u32[]{:S(2)}) copy-start(bf16[32,2048]{1,0:T(8,128)(2,1)} %down.3) | copy-start | bytes 393220
  68.0 38.0 %copy-start.3 = (bf16[256,256]{1,0:T(8,128)(2,1)S(1)}, bf16[256,256]{1,0:T(8,128)(2,1)}, u32[]{:S(2)}) copy-start(bf16[256,256]{1,0:T(8,128)(2,1)} %get-tuple-element.14.w_high) | copy-start | bytes 393220
  68.0 38.0 %copy-start.4 = (bf16[256,256]{1,0:T(8,128)(2,1)S(1)}, bf16[256,256]{1,0:T(8,128)(2,1)}, u32[]{:S(2)}) copy-start(bf16[256,256]{1,0:T(8,128)(2,1)} %get-tuple-element.18.w_low) | copy-start | bytes 393220
  68.0 38.0 %copy-start.5 = (bf16[64,2048]{1,0:T(8,128)(2,1)S(1)}, bf16[64,2048]{1,0:T(8,128)(2,1)}, u32[]{:S(2)}) copy-start(bf16[64,2048]{1,0:T(8,128)(2,1)} %mix.1) | copy-start | bytes 786436
  68.0 38.0 %copy-start.6 = (bf16[128,512]{1,0:T(8,128)(2,1)S(1)}, bf16[128,512]{1,0:T(8,128)(2,1)}, u32[]{:S(2)}) copy-start(bf16[128,512]{1,0:T(8,128)(2,1)} %queries.1) | copy-start | bytes 393220
  68.0 38.0 %copy-start.9 = (bf16[128,64]{0,1:T(8,128)(2,1)S(1)}, bf16[128,64]{0,1:T(8,128)(2,1)}, u32[]{:S(2)}) copy-start(bf16[128,64]{0,1:T(8,128)(2,1)} %param.19) | copy-start | bytes 49156
  68.0 38.0 %copy-start.11 = (bf16[128,64]{0,1:T(8,128)(2,1)S(1)}, bf16[128,64]{0,1:T(8,128)(2,1)}, u32[]{:S(2)}) copy-start(bf16[128,64]{0,1:T(8,128)(2,1)} %param.20) | copy-start | bytes 49156
  68.0 38.0 %copy-start.12 = (f32[128,2]{0,1:T(2,128)S(1)}, f32[128,2]{0,1:T(2,128)}, u32[]{:S(2)}) copy-start(f32[128,2]{0,1:T(2,128)} %param.21) | copy-start | bytes 3076
  68.0 38.0 %copy-start.13 = (f32[128,2]{0,1:T(2,128)S(1)}, f32[128,2]{0,1:T(2,128)}, u32[]{:S(2)}) copy-start(f32[128,2]{0,1:T(2,128)} %param.22) | copy-start | bytes 3076
  68.0 37.9 %all-to-all-start.1 = ((bf16[32,8,2176]{2,1,0:T(8,128)(2,1)}), bf16[32,8,2176]{2,1,0:T(8,128)(2,1)S(1)}, u32[]{:S(2)}, u32[]{:S(2)}) async-start(bf16[32,8,2176]{2,1,0:T(8,128)(2,1)} %bitcast.29), calls=%async_computation.1 | async-start | bytes 2228224 | tf_op jit(solution)/shard_map/all_to_all | solution.py:327
  107.6 5.6 %collective-permute-start.9 = (bf16[8,24,2048]{2,1,0:T(8,128)(2,1)S(1)}, bf16[8,24,2048]{2,1,0:T(8,128)(2,1)S(1)}, u32[]{:S(2)}, u32[]{:S(2)}) collective-permute-start(bf16[8,24,2048]{2,1,0:T(8,128)(2,1)S(1)} %get-tuple-element.21), channel_id=1, source_target_pairs={{0,1},{1,0},{2,3},{3,2},{4,5},{5,4},{6,7},{7,6},{8,9},{9,8},{10,11... | collective-permute-start | bytes 2359304 | tf_op jit(solution)/shard_map/ppermute | solution.py:331
  165.7 7.1 %collective-permute-start.10 = (bf16[8,24,2048]{2,1,0:T(8,128)(2,1)S(1)}, bf16[8,24,2048]{2,1,0:T(8,128)(2,1)S(1)}, u32[]{:S(2)}, u32[]{:S(2)}) collective-permute-start(bf16[8,24,2048]{2,1,0:T(8,128)(2,1)S(1)} %all_to_all.21.mine), channel_id=1, source_target_pairs={{0,1},{1,0},{2,3},{3,2},{4,5},{5,4},{6,7},{7,6},{8,9},{9,8},{10,11... | collective-permute-start | bytes 2359304 | tf_op jit(solution)/shard_map/ppermute | solution.py:331

commit v5 on v4

--- a/solution.py
+++ b/solution.py
@@ -27,7 +27,6 @@
 epsilon = 1e-06
 lowest = -1e30
 den_floor = 4.0
-HIGHEST = lax.Precision.HIGHEST
 
 VMEM = pl.BlockSpec(memory_space=pltpu.VMEM)
 HBM = pl.BlockSpec(memory_space=pltpu.HBM)
@@ -56,6 +55,16 @@
     return lax.broadcasted_iota(jnp.int32, dims, dim)
 
 
+def exact_dot(left, right, parts):
+    total, rest = None, left
+    for _ in range(parts):
+        piece = rest.astype(bf16)
+        product = jnp.dot(piece, right, preferred_element_type=f32)
+        total = product if total is None else total + product
+        rest = rest - piece.astype(f32)
+    return total
+
+
 def split_scalar(value):
     high = value.astype(bf16).astype(f32)
     middle = (value - high).astype(bf16).astype(f32)
@@ -75,9 +84,7 @@
     tail = jnp.where(small < 1e-4, small - 0.5 * small * small, jnp.log(1.0 + small))
     log_forget = jnp.minimum(forget, 0.0) - tail
     upto = jnp.where(iota((BLOCK, BLOCK), 0) <= iota((BLOCK, BLOCK), 1), 1.0, 0.0)
-    cumulative = jnp.dot(
-        jnp.broadcast_to(log_forget, (8, BLOCK)), upto, preferred_element_type=f32, precision=HIGHEST
-    )[0:1, :]
+    cumulative = exact_dot(jnp.broadcast_to(log_forget, (16, BLOCK)), upto.astype(bf16), 3)[0:1, :]
     return given, cumulative
 
 
@@ -105,8 +112,10 @@
     rank = jnp.dot(named.astype(bf16), before, preferred_element_type=f32)
     rank = jnp.where(named > 0.0, rank, -1.0)
     spread = jnp.where(iota((ROWS, N_EP), 0) // SLOTS == iota((ROWS, N_EP), 1), 1.0, 0.0)
-    rank = jnp.dot(spread.astype(bf16), rank.astype(bf16), preferred_element_type=f32)
-    weight = jnp.dot(spread, weight, preferred_element_type=f32, precision=HIGHEST)
+    spread = spread.astype(bf16)
+    rank = jnp.dot(spread, rank.astype(bf16), preferred_element_type=f32)
+    upper = weight.astype(bf16)
+    lower = (weight - upper.astype(f32)).astype(bf16)
     slot = (lax.rem(iota((ROWS, TOKENS), 0), SLOTS) + part * SLOTS).astype(f32)
     chosen = rank == slot
     pick = jnp.where(chosen, 1.0, 0.0).astype(bf16)
@@ -116,23 +125,21 @@
         staged[:, at] = jnp.dot(pick, normal[:, at], preferred_element_type=f32).astype(bf16)
         copies.append(pltpu.make_async_copy(staged.at[:, at], send.at[:, at], sem.at[k]))
         copies[-1].start()
-    weight = jnp.where(chosen, weight, 0.0)
-    high = weight.astype(bf16)
-    w_high[...] = high
-    w_low[...] = (weight - high.astype(f32)).astype(bf16)
+    for target, part_of in ((w_high, upper), (w_low, lower)):
+        placed = jnp.dot(spread, part_of, preferred_element_type=f32)
+        target[...] = jnp.where(chosen, placed, 0.0).astype(bf16)
 
     given, cumulative = gates(team, input_gate, forget_gate)
     block_total = cumulative[:, BLOCK - 1 : BLOCK]
     log_keep = block_total - cumulative + given
     running = jnp.max(log_keep, axis=1, keepdims=True)
     kept = jnp.exp(log_keep - running)
-    key = keys[:, pl.ds(pl.multiple_of(team * KEY_DIM, KEY_DIM), KEY_DIM)].astype(f32)
-    memory = jnp.dot(
-        values[...].astype(f32) * kept, key, preferred_element_type=f32, precision=HIGHEST
-    )
-    normalizer = jnp.dot(
-        jnp.broadcast_to(kept, (8, BLOCK)), key, preferred_element_type=f32, precision=HIGHEST
-    )
+    key = keys[:, pl.ds(pl.multiple_of(team * KEY_DIM, KEY_DIM), KEY_DIM)]
+    lifted = jnp.concatenate(
+        [values[...].astype(f32) * kept, jnp.broadcast_to(kept, (16, BLOCK))], axis=0
+    )
+    memory = exact_dot(lifted, key, 2)
+    normalizer = memory[64:65, :]
     states[:, 0, :] = memory[0:32, 0:128]
     states[:, 1, :] = memory[0:32, 128:256]
     states[:, 2, :] = memory[32:64, 0:128]
@@ -160,17 +167,17 @@
     row, column = iota((N_EP, N_EP), 0), iota((N_EP, N_EP), 1)
     earlier = column < row
     passed = jnp.where(earlier, totals, 0.0)
-    later = jnp.where(row > column, 1.0, 0.0)
-    between = jnp.dot(passed, later, preferred_element_type=f32, precision=HIGHEST)
+    later = jnp.where(row > column, 1.0, 0.0).astype(bf16)
+    between = exact_dot(passed, later, 3)
     reach = jnp.where(earlier, peaks + between, lowest)
     running = jnp.maximum(
         jnp.sum(passed, axis=1, keepdims=True), jnp.max(reach, axis=1, keepdims=True)
     )
     share = jnp.where(earlier, jnp.exp(reach - running), 0.0)
+    held = jnp.concatenate([states[:, k, :] for k in range(6)], axis=1).astype(bf16)
+    entering = exact_dot(share, held, 2)
     for k in range(6):
-        states[:, k, :] = jnp.dot(
-            share, states[:, k, :], preferred_element_type=f32, precision=HIGHEST
-        )
+        states[:, k, :] = entering[:, 128 * k : 128 * (k + 1)]
     states[:, 6, :] = split_scalar(running)
     states[:, 7, :] = jnp.zeros((N_EP, 128), f32)
 

time: 175 us -> 174 us (level)
  no operation moved by 1% of the time
where the time goes in v5:
time: 174 us; the launch traced here: 173 us
  starting transfers between devices  62 us (36%)
  blocking collectives  52.1 us (30%)
  waiting for transfers between devices  40.5 us (23%)
  Pallas kernels  15.4 us (9%)
  local copies, waits for them, and re-layouts  2.09 us (1%)
    all_to_all x2, blocking collectives, exchange(): return lax.all_to_all(array, axis, split_axis=0, concat_axis=0, tiled=True)  52.1 us
    ppermute x8, starting transfers between devices, swap(): return lax.ppermute(array, 'c', [(0, 1), (1, 0)])  30.2 us
    all_to_all x2, waiting for transfers between devices, exchange(): return lax.all_to_all(array, axis, split_axis=0, concat_axis=0, tiled=True)  27.6 us
    all_to_all x2, starting transfers between devices, exchange(): return lax.all_to_all(array, axis, split_axis=0, concat_axis=0, tiled=True)  23.3 us
    pallas_call x7, Pallas kernels, call(): pl.pallas_call(body, out_shape=outs, in_specs=ins, out_specs=spaces, scra...  15.4 us
    ppermute x3, waiting for transfers between devices, reach_over(): return lax.ppermute(array, 'y', [(k, k ^ 1) for k in range(N_Y)])  10.7 us
    ppermute x3, starting transfers between devices, reach_over(): return lax.ppermute(array, 'y', [(k, k ^ 1) for k in range(N_Y)])  8.48 us
  transfers between devices with their start and end apart: 13, of which 6 were waited for; matrix products, arithmetic and copies ran while one was open for 0% of the time, Pallas kernels for 1%

profile of v5, /device:TPU:1, one launch (start us, length us, event | category | flops | bytes accessed | tf_op | source)
XLA Modules:
  0.0 173.5 jit_solution(9064973730238938103)
XLA Ops:
  0.6 4.0 %shard_map.176 = (bf16[256,2176]{1,0:T(8,128)(2,1)}, bf16[256,256]{1,0:T(8,128)(2,1)}, bf16[256,256]{1,0:T(8,128)(2,1)}) custom-call(bf16[256,2048]{1,0:T(8,128)(2,1)} %x.2, f32[1,2048]{1,0:T(1,128)} %bitcast.22, s32[4,256]{1,0:T(4,128)} %bitcast.40, f32[4,256]{1,0:T(4,128)} %bitcast.41, bf16[128,512]{1,0:T(8,128)(2,1)} %keys.3, bf16[64,128]{1,0:T(8,128)(2,1)} %bitcast.20, ...), custom_call_target="tpu_custom_call" | custom-call | flops 268435456 | bytes 1048576 | tf_op jit(solution)/shard_map/pallas_call | solution.py:38
  4.6 0.0 copy-start.15
  4.6 0.0 copy-start.16
  4.6 0.0 copy-start.14
  4.6 14.0 %all-to-all-start = ((bf16[32,8,2176]{2,1,0:T(8,128)(2,1)}), bf16[32,8,2176]{2,1,0:T(8,128)(2,1)}, u32[]{:S(2)}, u32[]{:S(2)}) async-start(bf16[32,8,2176]{2,1,0:T(8,128)(2,1)} %bitcast.30), calls=%async_computation | async-start | bytes 2228224 | tf_op jit(solution)/shard_map/all_to_all | solution.py:334
  18.6 3.2 %collective-permute-start.4 = (bf16[2048,128]{1,0:T(8,128)(2,1)S(1)}, bf16[2048,128]{1,0:T(8,128)(2,1)S(1)}, u32[]{:S(2)}, u32[]{:S(2)}) collective-permute-start(bf16[2048,128]{1,0:T(8,128)(2,1)S(1)} %bitcast.35), channel_id=1, source_target_pairs={{0,2},{2,0},{4,6},{6,4},{8,10},{10,8},{12,14},{14,12},{1,3},{3,1},... | collective-permute-start | bytes 1572872 | tf_op jit(solution)/shard_map/ppermute | solution.py:342
  21.8 2.1 %collective-permute-start.5 = (bf16[128,2048]{1,0:T(8,128)(2,1)S(1)}, bf16[128,2048]{1,0:T(8,128)(2,1)S(1)}, u32[]{:S(2)}, u32[]{:S(2)}) collective-permute-start(bf16[128,2048]{1,0:T(8,128)(2,1)S(1)} %bitcast.38), channel_id=1, source_target_pairs={{0,2},{2,0},{4,6},{6,4},{8,10},{10,8},{12,14},{14,12},{1,3},{3,1},... | collective-permute-start | bytes 1572872 | tf_op jit(solution)/shard_map/ppermute | solution.py:342
  23.9 3.4 %collective-permute-start = (bf16[2048,128]{1,0:T(8,128)(2,1)S(1)}, bf16[2048,128]{1,0:T(8,128)(2,1)S(1)}, u32[]{:S(2)}, u32[]{:S(2)}) collective-permute-start(bf16[2048,128]{1,0:T(8,128)(2,1)S(1)} %bitcast.32), channel_id=1, source_target_pairs={{0,1},{1,0},{2,3},{3,2},{4,5},{5,4},{6,7},{7,6},{8,9},{9,8},{10,11... | collective-permute-start | bytes 1572872 | tf_op jit(solution)/shard_map/ppermute | solution.py:338
  27.4 3.2 %collective-permute-start.3 = (bf16[2048,128]{1,0:T(8,128)(2,1)S(1)}, bf16[2048,128]{1,0:T(8,128)(2,1)S(1)}, u32[]{:S(2)}, u32[]{:S(2)}) collective-permute-start(bf16[2048,128]{1,0:T(8,128)(2,1)S(1)} %bitcast.33), channel_id=1, source_target_pairs={{0,2},{2,0},{4,6},{6,4},{8,10},{10,8},{12,14},{14,12},{1,3},{3,1},... | collective-permute-start | bytes 1572872 | tf_op jit(solution)/shard_map/ppermute | solution.py:342
  30.6 2.2 %collective-permute-start.1 = (bf16[2048,128]{1,0:T(8,128)(2,1)S(1)}, bf16[2048,128]{1,0:T(8,128)(2,1)S(1)}, u32[]{:S(2)}, u32[]{:S(2)}) collective-permute-start(bf16[2048,128]{1,0:T(8,128)(2,1)S(1)} %bitcast.36), channel_id=1, source_target_pairs={{0,1},{1,0},{2,3},{3,2},{4,5},{5,4},{6,7},{7,6},{8,9},{9,8},{10,11... | collective-permute-start | bytes 1572872 | tf_op jit(solution)/shard_map/ppermute | solution.py:338
  32.8 0.3 collective-permute-done.4.refs_8_
  33.1 5.0 %collective-permute-start.2 = (bf16[128,2048]{1,0:T(8,128)(2,1)S(1)}, bf16[128,2048]{1,0:T(8,128)(2,1)S(1)}, u32[]{:S(2)}, u32[]{:S(2)}) collective-permute-start(bf16[128,2048]{1,0:T(8,128)(2,1)S(1)} %bitcast.39), channel_id=1, source_target_pairs={{0,1},{1,0},{2,3},{3,2},{4,5},{5,4},{6,7},{7,6},{8,9},{9,8},{10,11... | collective-permute-start | bytes 1572872 | tf_op jit(solution)/shard_map/ppermute | solution.py:338
  38.2 6.2 %collective-permute-done.5.refs_9_ = bf16[128,2048]{1,0:T(8,128)(2,1)S(1)} collective-permute-done((bf16[128,2048]{1,0:T(8,128)(2,1)S(1)}, bf16[128,2048]{1,0:T(8,128)(2,1)S(1)}, u32[]{:S(2)}, u32[]{:S(2)}) %collective-permute-start.5) | collective-permute-done | bytes 524320 | tf_op jit(solution)/shard_map/ppermute | solution.py:342
  44.4 5.0 %collective-permute-start.7 = (bf16[2048,128]{1,0:T(8,128)(2,1)S(1)}, bf16[2048,128]{1,0:T(8,128)(2,1)S(1)}, u32[]{:S(2)}, u32[]{:S(2)}) collective-permute-start(bf16[2048,128]{1,0:T(8,128)(2,1)S(1)} %collective-permute-done.4.refs_8_), channel_id=1, source_target_pairs={{0,1},{1,0},{2,3},{3,2},{4,5},{5,4},{6,7},{7,6},{8,9},{9,8},{10,11... | collective-permute-start | bytes 1572872 | tf_op jit(solution)/shard_map/ppermute | solution.py:338
  49.4 0.0 copy-start.19
  49.4 1.9 %collective-permute-start.8 = (bf16[128,2048]{1,0:T(8,128)(2,1)S(1)}, bf16[128,2048]{1,0:T(8,128)(2,1)S(1)}, u32[]{:S(2)}, u32[]{:S(2)}) collective-permute-start(bf16[128,2048]{1,0:T(8,128)(2,1)S(1)} %collective-permute-done.5.refs_9_), channel_id=1, source_target_pairs={{0,1},{1,0},{2,3},{3,2},{4,5},{5,4},{6,7},{7,6},{8,9},{9,8},{10,11... | collective-permute-start | bytes 1572872 | tf_op jit(solution)/shard_map/ppermute | solution.py:338
  51.3 4.1 %collective-permute-done.3.refs_7_ = bf16[2048,128]{1,0:T(8,128)(2,1)S(1)} collective-permute-done((bf16[2048,128]{1,0:T(8,128)(2,1)S(1)}, bf16[2048,128]{1,0:T(8,128)(2,1)S(1)}, u32[]{:S(2)}, u32[]{:S(2)}) %collective-permute-start.3) | collective-permute-done | bytes 524320 | tf_op jit(solution)/shard_map/ppermute | solution.py:342
  55.5 3.7 %collective-permute-start.6 = (bf16[2048,128]{1,0:T(8,128)(2,1)S(1)}, bf16[2048,128]{1,0:T(8,128)(2,1)}, u32[]{:S(2)}, u32[]{:S(2)}) collective-permute-start(bf16[2048,128]{1,0:T(8,128)(2,1)S(1)} %collective-permute-done.3.refs_7_), channel_id=1, source_target_pairs={{0,1},{1,0},{2,3},{3,2},{4,5},{5,4},{6,7},{7,6},{8,9},{9,8},{10,11... | collective-permute-start | bytes 1572872 | tf_op jit(solution)/shard_map/ppermute | solution.py:338
  59.2 0.0 copy-start.21
  59.3 0.7 copy-done.21
  60.0 0.2 copy-done.22
  60.2 0.2 copy-done.23
  60.4 0.8 copy-done.24
  61.2 6.4 %shard_map.177 = bf16[256,2176]{1,0:T(8,128)(2,1)} custom-call(bf16[256,2176]{1,0:T(8,128)(2,1)} %bitcast.7.refs_0_, bf16[2048,128]{1,0:T(8,128)(2,1)} %bitcast.31, bf16[2048,128]{1,0:T(8,128)(2,1)} %bitcast.34, bf16[128,2048]{1,0:T(8,128)(2,1)} %bitcast.37, bf16[2048,128]{1,0:T(8,128)(2,1)} %copy-done.19, bf16[2048,128]{1,0:T(8,128)(2,1)} %copy-done.21, ...), custom_call_target="tpu_custom_call" | custom-call | flops 2147483648 | bytes 1048576 | tf_op jit(solution)/shard_map/pallas_call | solution.py:38
  67.6 0.0 copy-start
  67.7 0.0 copy-start.7
  67.7 0.0 copy-start.10
  67.7 0.0 copy-start.1
  67.8 0.0 copy-start.6
  67.8 0.0 copy-start.9
  67.8 0.0 copy-start.12
  67.8 0.0 copy-start.13
  67.8 9.3 %all-to-all-start.1 = ((bf16[32,8,2176]{2,1,0:T(8,128)(2,1)}), bf16[32,8,2176]{2,1,0:T(8,128)(2,1)S(1)}, u32[]{:S(2)}, u32[]{:S(2)}) async-start(bf16[32,8,2176]{2,1,0:T(8,128)(2,1)} %bitcast.29), calls=%async_computation.1 | async-start | bytes 2228224 | tf_op jit(solution)/shard_map/all_to_all | solution.py:334
  77.2 0.9 shard_map.178.act
  78.1 27.6 %all-to-all-done.1 = bf16[32,8,2176]{2,1,0:T(8,128)(2,1)S(1)} async-done(((bf16[32,8,2176]{2,1,0:T(8,128)(2,1)}), bf16[32,8,2176]{2,1,0:T(8,128)(2,1)S(1)}, u32[]{:S(2)}, u32[]{:S(2)}) %all-to-all-start.1) | async-done | bytes 1114144 | tf_op jit(solution)/shard_map/all_to_all | solution.py:334
  105.8 1.5 shard_map.179
  107.3 3.7 %collective-permute-start.9 = (bf16[8,24,2048]{2,1,0:T(8,128)(2,1)S(1)}, bf16[8,24,2048]{2,1,0:T(8,128)(2,1)S(1)}, u32[]{:S(2)}, u32[]{:S(2)}) collective-permute-start(bf16[8,24,2048]{2,1,0:T(8,128)(2,1)S(1)} %get-tuple-element.21), channel_id=1, source_target_pairs={{0,1},{1,0},{2,3},{3,2},{4,5},{5,4},{6,7},{7,6},{8,9},{9,8},{10,11... | collective-permute-start | bytes 2359304 | tf_op jit(solution)/shard_map/ppermute | solution.py:338
  111.0 0.6 shard_map.180
  111.6 1.3 collective-permute-done.9
  112.9 0.2 add_convert_fusion
  113.0 29.0 %all_to_all.20 = bf16[8,24,2048]{2,1,0:T(8,128)(2,1)S(1)} all-to-all(bf16[8,24,2048]{2,1,0:T(8,128)(2,1)S(1)} %add_convert_fusion), channel_id=1, replica_groups=mesh['z'=8,'x'=4,'y'=8,'c'=2] {'y'}, dimensions={0} | all-to-all | bytes 1572864 | tf_op jit(solution)/shard_map/all_to_all | solution.py:334
  142.0 0.1 reduce_sum.12
  142.1 0.1 broadcast_in_dim.5
  142.2 23.1 %all_to_all.21.mine = bf16[8,24,2048]{2,1,0:T(8,128)(2,1)S(1)} all-to-all(bf16[8,24,2048]{2,1,0:T(8,128)(2,1)S(1)} %broadcast_in_dim.5), channel_id=1, replica_groups=mesh['z'=8,'x'=4,'y'=8,'c'=2] {'y'}, dimensions={0} | all-to-all | bytes 1572864 | tf_op jit(solution)/shard_map/all_to_all | solution.py:334
  165.4 5.2 %collective-permute-start.10 = (bf16[8,24,2048]{2,1,0:T(8,128)(2,1)S(1)}, bf16[8,24,2048]{2,1,0:T(8,128)(2,1)S(1)}, u32[]{:S(2)}, u32[]{:S(2)}) collective-permute-start(bf16[8,24,2048]{2,1,0:T(8,128)(2,1)S(1)} %all_to_all.21.mine), channel_id=1, source_target_pairs={{0,1},{1,0},{2,3},{3,2},{4,5},{5,4},{6,7},{7,6},{8,9},{9,8},{10,11... | collective-permute-start | bytes 2359304 | tf_op jit(solution)/shard_map/ppermute | solution.py:338
  170.6 1.0 shard_map.181
  171.6 0.9 collective-permute-done.10.other
  172.5 1.0 shard_map.182
  (40 shorter events, 0.1 us)
Async XLA Ops:
  4.6 14.0 %copy-start.15 = (bf16[1,2048,128]{2,1,0:T(8,128)(2,1)S(1)}, bf16[1,2048,128]{2,1,0:T(8,128)(2,1)}, u32[]{:S(2)}) copy-start(bf16[1,2048,128]{2,1,0:T(8,128)(2,1)} %param.29) | copy-start | bytes 1572868
  4.6 17.2 %copy-start.16 = (bf16[1,128,2048]{2,1,0:T(8,128)(2,1)S(1)}, bf16[1,128,2048]{2,1,0:T(8,128)(2,1)}, u32[]{:S(2)}) copy-start(bf16[1,128,2048]{2,1,0:T(8,128)(2,1)} %param.30) | copy-start | bytes 1572868
  4.6 19.3 %copy-start.14 = (bf16[1,2048,128]{2,1,0:T(8,128)(2,1)S(1)}, bf16[1,2048,128]{2,1,0:T(8,128)(2,1)}, u32[]{:S(2)}) copy-start(bf16[1,2048,128]{2,1,0:T(8,128)(2,1)} %param.28) | copy-start | bytes 1572868
  4.6 56.6 %all-to-all-start = ((bf16[32,8,2176]{2,1,0:T(8,128)(2,1)}), bf16[32,8,2176]{2,1,0:T(8,128)(2,1)}, u32[]{:S(2)}, u32[]{:S(2)}) async-start(bf16[32,8,2176]{2,1,0:T(8,128)(2,1)} %bitcast.30), calls=%async_computation | async-start | bytes 2228224 | tf_op jit(solution)/shard_map/all_to_all | solution.py:334
  18.6 14.5 %collective-permute-start.4 = (bf16[2048,128]{1,0:T(8,128)(2,1)S(1)}, bf16[2048,128]{1,0:T(8,128)(2,1)S(1)}, u32[]{:S(2)}, u32[]{:S(2)}) collective-permute-start(bf16[2048,128]{1,0:T(8,128)(2,1)S(1)} %bitcast.35), channel_id=1, source_target_pairs={{0,2},{2,0},{4,6},{6,4},{8,10},{10,8},{12,14},{14,12},{1,3},{3,1},... | collective-permute-start | bytes 1572872 | tf_op jit(solution)/shard_map/ppermute | solution.py:342
  21.8 22.5 %collective-permute-start.5 = (bf16[128,2048]{1,0:T(8,128)(2,1)S(1)}, bf16[128,2048]{1,0:T(8,128)(2,1)S(1)}, u32[]{:S(2)}, u32[]{:S(2)}) collective-permute-start(bf16[128,2048]{1,0:T(8,128)(2,1)S(1)} %bitcast.38), channel_id=1, source_target_pairs={{0,2},{2,0},{4,6},{6,4},{8,10},{10,8},{12,14},{14,12},{1,3},{3,1},... | collective-permute-start | bytes 1572872 | tf_op jit(solution)/shard_map/ppermute | solution.py:342
  23.9 25.5 %collective-permute-start = (bf16[2048,128]{1,0:T(8,128)(2,1)S(1)}, bf16[2048,128]{1,0:T(8,128)(2,1)S(1)}, u32[]{:S(2)}, u32[]{:S(2)}) collective-permute-start(bf16[2048,128]{1,0:T(8,128)(2,1)S(1)} %bitcast.32), channel_id=1, source_target_pairs={{0,1},{1,0},{2,3},{3,2},{4,5},{5,4},{6,7},{7,6},{8,9},{9,8},{10,11... | collective-permute-start | bytes 1572872 | tf_op jit(solution)/shard_map/ppermute | solution.py:338
  27.4 28.1 %collective-permute-start.3 = (bf16[2048,128]{1,0:T(8,128)(2,1)S(1)}, bf16[2048,128]{1,0:T(8,128)(2,1)S(1)}, u32[]{:S(2)}, u32[]{:S(2)}) collective-permute-start(bf16[2048,128]{1,0:T(8,128)(2,1)S(1)} %bitcast.33), channel_id=1, source_target_pairs={{0,2},{2,0},{4,6},{6,4},{8,10},{10,8},{12,14},{14,12},{1,3},{3,1},... | collective-permute-start | bytes 1572872 | tf_op jit(solution)/shard_map/ppermute | solution.py:342
  30.6 28.6 %collective-permute-start.1 = (bf16[2048,128]{1,0:T(8,128)(2,1)S(1)}, bf16[2048,128]{1,0:T(8,128)(2,1)S(1)}, u32[]{:S(2)}, u32[]{:S(2)}) collective-permute-start(bf16[2048,128]{1,0:T(8,128)(2,1)S(1)} %bitcast.36), channel_id=1, source_target_pairs={{0,1},{1,0},{2,3},{3,2},{4,5},{5,4},{6,7},{7,6},{8,9},{9,8},{10,11... | collective-permute-start | bytes 1572872 | tf_op jit(solution)/shard_map/ppermute | solution.py:338
  33.1 26.1 %copy-start.17 = (bf16[2048,128]{1,0:T(8,128)(2,1)}, bf16[2048,128]{1,0:T(8,128)(2,1)S(1)}, u32[]{:S(2)}) copy-start(bf16[2048,128]{1,0:T(8,128)(2,1)S(1)} %collective-permute-done.4.refs_8_) | copy-start | bytes 1572868
  33.1 26.1 %collective-permute-start.2 = (bf16[128,2048]{1,0:T(8,128)(2,1)S(1)}, bf16[128,2048]{1,0:T(8,128)(2,1)S(1)}, u32[]{:S(2)}, u32[]{:S(2)}) collective-permute-start(bf16[128,2048]{1,0:T(8,128)(2,1)S(1)} %bitcast.39), channel_id=1, source_target_pairs={{0,1},{1,0},{2,3},{3,2},{4,5},{5,4},{6,7},{7,6},{8,9},{9,8},{10,11... | collective-permute-start | bytes 1572872 | tf_op jit(solution)/shard_map/ppermute | solution.py:338
  44.4 14.9 %copy-start.18 = (bf16[128,2048]{1,0:T(8,128)(2,1)}, bf16[128,2048]{1,0:T(8,128)(2,1)S(1)}, u32[]{:S(2)}) copy-start(bf16[128,2048]{1,0:T(8,128)(2,1)S(1)} %collective-permute-done.5.refs_9_) | copy-start | bytes 1572868
  44.4 14.9 %collective-permute-start.7 = (bf16[2048,128]{1,0:T(8,128)(2,1)S(1)}, bf16[2048,128]{1,0:T(8,128)(2,1)S(1)}, u32[]{:S(2)}, u32[]{:S(2)}) collective-permute-start(bf16[2048,128]{1,0:T(8,128)(2,1)S(1)} %collective-permute-done.4.refs_8_), channel_id=1, source_target_pairs={{0,1},{1,0},{2,3},{3,2},{4,5},{5,4},{6,7},{7,6},{8,9},{9,8},{10,11... | collective-permute-start | bytes 1572872 | tf_op jit(solution)/shard_map/ppermute | solution.py:338
  49.4 9.9 %copy-start.19 = (bf16[2048,128]{1,0:T(8,128)(2,1)}, bf16[2048,128]{1,0:T(8,128)(2,1)S(1)}, u32[]{:S(2)}) copy-start(bf16[2048,128]{1,0:T(8,128)(2,1)S(1)} %collective-permute-done.refs_4_) | copy-start | bytes 1572868
  49.4 9.9 %collective-permute-start.8 = (bf16[128,2048]{1,0:T(8,128)(2,1)S(1)}, bf16[128,2048]{1,0:T(8,128)(2,1)S(1)}, u32[]{:S(2)}, u32[]{:S(2)}) collective-permute-start(bf16[128,2048]{1,0:T(8,128)(2,1)S(1)} %collective-permute-done.5.refs_9_), channel_id=1, source_target_pairs={{0,1},{1,0},{2,3},{3,2},{4,5},{5,4},{6,7},{7,6},{8,9},{9,8},{10,11... | collective-permute-start | bytes 1572872 | tf_op jit(solution)/shard_map/ppermute | solution.py:338
  55.5 3.8 %copy-start.20 = (bf16[2048,128]{1,0:T(8,128)(2,1)}, bf16[2048,128]{1,0:T(8,128)(2,1)S(1)}, u32[]{:S(2)}) copy-start(bf16[2048,128]{1,0:T(8,128)(2,1)S(1)} %collective-permute-done.3.refs_7_) | copy-start | bytes 1572868
  55.5 5.7 %collective-permute-start.6 = (bf16[2048,128]{1,0:T(8,128)(2,1)S(1)}, bf16[2048,128]{1,0:T(8,128)(2,1)}, u32[]{:S(2)}, u32[]{:S(2)}) collective-permute-start(bf16[2048,128]{1,0:T(8,128)(2,1)S(1)} %collective-permute-done.3.refs_7_), channel_id=1, source_target_pairs={{0,1},{1,0},{2,3},{3,2},{4,5},{5,4},{6,7},{7,6},{8,9},{9,8},{10,11... | collective-permute-start | bytes 1572872 | tf_op jit(solution)/shard_map/ppermute | solution.py:338
  59.2 0.8 copy-start.21
  59.3 1.0 copy-start.22
  59.3 1.1 copy-start.23
  60.4 0.8 copy-start.24
  67.6 9.5 %copy-start = (bf16[256,2048]{1,0:T(8,128)(2,1)S(1)}, bf16[256,2048]{1,0:T(8,128)(2,1)}, u32[]{:S(2)}) copy-start(bf16[256,2048]{1,0:T(8,128)(2,1)} %x.2) | copy-start | bytes 3145732
  67.7 9.5 %copy-start.7 = (bf16[2048,32]{0,1:T(8,128)(2,1)S(1)}, bf16[2048,32]{0,1:T(8,128)(2,1)}, u32[]{:S(2)}) copy-start(bf16[2048,32]{0,1:T(8,128)(2,1)} %param.31) | copy-start | bytes 393220
  67.7 9.5 %copy-start.8 = (bf16[2048,32]{0,1:T(8,128)(2,1)S(1)}, bf16[2048,32]{0,1:T(8,128)(2,1)}, u32[]{:S(2)}) copy-start(bf16[2048,32]{0,1:T(8,128)(2,1)} %param.32) | copy-start | bytes 393220
  67.7 9.5 %copy-start.10 = (f32[2048]{0:T(1024)S(1)}, f32[2048]{0:T(1024)}, u32[]{:S(2)}) copy-start(f32[2048]{0:T(1024)} %param.25) | copy-start | bytes 24580
  67.7 38.0 %copy-start.1 = (bf16[128,512]{1,0:T(8,128)(2,1)S(1)}, bf16[128,512]{1,0:T(8,128)(2,1)}, u32[]{:S(2)}) copy-start(bf16[128,512]{1,0:T(8,128)(2,1)} %keys.3) | copy-start | bytes 393220
  67.7 38.0 %copy-start.2 = (bf16[32,2048]{1,0:T(8,128)(2,1)S(1)}, bf16[32,2048]{1,0:T(8,128)(2,1)}, u32[]{:S(2)}) copy-start(bf16[32,2048]{1,0:T(8,128)(2,1)} %down.3) | copy-start | bytes 393220
  67.7 38.0 %copy-start.3 = (bf16[256,256]{1,0:T(8,128)(2,1)S(1)}, bf16[256,256]{1,0:T(8,128)(2,1)}, u32[]{:S(2)}) copy-start(bf16[256,256]{1,0:T(8,128)(2,1)} %get-tuple-element.14.w_high) | copy-start | bytes 393220
  67.7 38.0 %copy-start.4 = (bf16[256,256]{1,0:T(8,128)(2,1)S(1)}, bf16[256,256]{1,0:T(8,128)(2,1)}, u32[]{:S(2)}) copy-start(bf16[256,256]{1,0:T(8,128)(2,1)} %get-tuple-element.18.w_low) | copy-start | bytes 393220
  67.7 38.0 %copy-start.5 = (bf16[64,2048]{1,0:T(8,128)(2,1)S(1)}, bf16[64,2048]{1,0:T(8,128)(2,1)}, u32[]{:S(2)}) copy-start(bf16[64,2048]{1,0:T(8,128)(2,1)} %mix.1) | copy-start | bytes 786436
  67.8 38.0 %copy-start.6 = (bf16[128,512]{1,0:T(8,128)(2,1)S(1)}, bf16[128,512]{1,0:T(8,128)(2,1)}, u32[]{:S(2)}) copy-start(bf16[128,512]{1,0:T(8,128)(2,1)} %queries.1) | copy-start | bytes 393220
  67.8 38.0 %copy-start.9 = (bf16[128,64]{0,1:T(8,128)(2,1)S(1)}, bf16[128,64]{0,1:T(8,128)(2,1)}, u32[]{:S(2)}) copy-start(bf16[128,64]{0,1:T(8,128)(2,1)} %param.19) | copy-start | bytes 49156
  67.8 38.0 %copy-start.11 = (bf16[128,64]{0,1:T(8,128)(2,1)S(1)}, bf16[128,64]{0,1:T(8,128)(2,1)}, u32[]{:S(2)}) copy-start(bf16[128,64]{0,1:T(8,128)(2,1)} %param.20) | copy-start | bytes 49156
  67.8 38.0 %copy-start.12 = (f32[128,2]{0,1:T(2,128)S(1)}, f32[128,2]{0,1:T(2,128)}, u32[]{:S(2)}) copy-start(f32[128,2]{0,1:T(2,128)} %param.21) | copy-start | bytes 3076
  67.8 38.0 %copy-start.13 = (f32[128,2]{0,1:T(2,128)S(1)}, f32[128,2]{0,1:T(2,128)}, u32[]{:S(2)}) copy-start(f32[128,2]{0,1:T(2,128)} %param.22) | copy-start | bytes 3076
  67.8 37.9 %all-to-all-start.1 = ((bf16[32,8,2176]{2,1,0:T(8,128)(2,1)}), bf16[32,8,2176]{2,1,0:T(8,128)(2,1)S(1)}, u32[]{:S(2)}, u32[]{:S(2)}) async-start(bf16[32,8,2176]{2,1,0:T(8,128)(2,1)} %bitcast.29), calls=%async_computation.1 | async-start | bytes 2228224 | tf_op jit(solution)/shard_map/all_to_all | solution.py:334
  107.3 5.6 %collective-permute-start.9 = (bf16[8,24,2048]{2,1,0:T(8,128)(2,1)S(1)}, bf16[8,24,2048]{2,1,0:T(8,128)(2,1)S(1)}, u32[]{:S(2)}, u32[]{:S(2)}) collective-permute-start(bf16[8,24,2048]{2,1,0:T(8,128)(2,1)S(1)} %get-tuple-element.21), channel_id=1, source_target_pairs={{0,1},{1,0},{2,3},{3,2},{4,5},{5,4},{6,7},{7,6},{8,9},{9,8},{10,11... | collective-permute-start | bytes 2359304 | tf_op jit(solution)/shard_map/ppermute | solution.py:338
  165.4 7.1 %collective-permute-start.10 = (bf16[8,24,2048]{2,1,0:T(8,128)(2,1)S(1)}, bf16[8,24,2048]{2,1,0:T(8,128)(2,1)S(1)}, u32[]{:S(2)}, u32[]{:S(2)}) collective-permute-start(bf16[8,24,2048]{2,1,0:T(8,128)(2,1)S(1)} %all_to_all.21.mine), channel_id=1, source_target_pairs={{0,1},{1,0},{2,3},{3,2},{4,5},{5,4},{6,7},{7,6},{8,9},{9,8},{10,11... | collective-permute-start | bytes 2359304 | tf_op jit(solution)/shard_map/ppermute | solution.py:338
